TPU v7x, 512 devices: a whole 4x8x8 slice. The times are simulated.
512 devices in a mesh: sp: 64 (over z, y), tp: 8 (over x, core).
Axes of the slice: x: 4, y: 8, z: 8, core: 2. Of those that a mesh axis runs over, the one named last changes fastest.
Arguments:
- activations: bfloat16 [65536, 2048], P(('sp', 'tp')), may hold values from -6 to 6
- input_norm_scale: float32 [2048], replicated, may hold values from 0.1 to 1.9
- value_weight_matrix: bfloat16 [2048, 1024], P(None, 'tp'), may hold values from -0.125 to 0.125
- gate_weight_matrix: bfloat16 [2048, 1024], P(None, 'tp'), may hold values from -0.125 to 0.125
- write_weight_matrix: bfloat16 [2048, 1024], P(None, 'tp'), may hold values from -0.125 to 0.125
- read_weight_matrix: bfloat16 [2048, 1024], P(None, 'tp'), may hold values from -0.125 to 0.125
- step_weight_matrix: bfloat16 [2048, 16], replicated, may hold values from -0.125 to 0.125
- pooling_input_matrix: bfloat16 [2048, 1024], P(None, 'tp'), may hold values from -0.125 to 0.125
- value_filter_weight: float32 [4, 1024], P(None, 'tp'), may hold values from -3 to 3
- write_filter_weight: float32 [4, 1024], P(None, 'tp'), may hold values from -3 to 3
- read_filter_weight: float32 [4, 1024], P(None, 'tp'), may hold values from -3 to 3
- head_log_decay_rate: float32 [16], replicated, may hold values from -12 to 0, as said below
- step_bias_offset: float32 [16, 65536], P('tp', 'sp'), may hold values from -3 to 0, as said below
- position_log_decay: float32 [16, 65536], P('tp', 'sp'), may hold values from -2 to 0, as said below
- gated_norm_scale: float32 [1024], P('tp'), may hold values from 0.1 to 1.9
- pooling_group_matrix: bfloat16 [16, 64, 64], P('tp'), may hold values from -0.75 to 0.75
- pooling_channel_scale: float32 [1024], P('tp'), may hold values from 0.1 to 1.9
- state_output_matrix: bfloat16 [1024, 2048], P('tp'), may hold values from -0.125 to 0.125
- pooling_output_matrix: bfloat16 [1024, 2048], P('tp'), may hold values from -0.125 to 0.125
Outputs:
- mixed: bfloat16 [65536, 2048], P(('sp', 'tp'))
Inputs may be any that keep to these rules, and one draw needn't show every extreme that they name: `head_log_decay_rate`: each head's logarithmic decay rate. `step_bias_offset`: constant over each block of 128 positions. `position_log_decay`: zero except at a few positions of the sequence.
All inputs are finite; a program needn't handle non-finite values.
Results may differ from a plain program's by a relative error of at most 0.017.
Values may be sent and summed in bfloat16 or wider, within the bound.
No kernel may reach another device: no remote copies, remote signals or barrier semaphores. Data moves between devices by JAX's collectives and lax.ppermute only.
A program may use at most 64 MiB of HBM per device.

v0:
```python
import jax
import jax.numpy as jnp
from jax import lax
from jax.experimental import pallas as pl
from jax.experimental.pallas import tpu as pltpu
from jax.sharding import Mesh
from jax.sharding import PartitionSpec as P

HEAD_DIM = 64
STATE = 128
BLOCK = 128
POOL_DIM = 64
HALO = 16
SP = ("sp_0", "sp_1")
TP = ("x", "core")
SP_TP = ("sp_0", "sp_1", "x", "core")
EPS = 1e-06
F32 = jnp.float32
BF16 = jnp.bfloat16
STEP_ROWS = 256
PACKED = STATE + 16


def silu(x):
    return x / (1.0 + jnp.exp(-x))


def by_head(first, second, shape):
    lane = lax.broadcasted_iota(jnp.int32, shape, len(shape) - 1)
    return jnp.where(lane < HEAD_DIM, first, second)


def norm_kernel(x_ref, scale_ref, out_ref, tail_ref):
    rows = normalize(x_ref[...], scale_ref[...])
    out_ref[...] = rows
    tail_ref[...] = rows[rows.shape[0] - HALO :]


def prepare_kernel(
    place_ref,
    rate_ref,
    value_ref,
    write_ref,
    read_ref,
    pool_ref,
    gate_ref,
    step_ref,
    value_taps_ref,
    write_taps_ref,
    read_taps_ref,
    bias_ref,
    pld_ref,
    group_ref,
    channel_ref,
    state_output_ref,
    pool_output_ref,
    w_ref,
    taps_ref,
    lanes_ref,
    pool_matrix_ref,
    output_ref,
):
    rank = place_ref[1] * 2 + place_ref[2]
    heads, length = bias_ref.shape
    for k, ref in enumerate((value_ref, write_ref, read_ref, pool_ref, gate_ref)):
        w_ref[:, k * STATE : (k + 1) * STATE] = ref[...]
    shape = (step_ref.shape[1], STATE)
    row, lane = (lax.broadcasted_iota(jnp.int32, shape, k) for k in range(2))
    chosen = jnp.where((lane < heads) & (row == rank * heads + lane), 1.0, 0.0).astype(BF16)
    w_ref[:, 5 * STATE :] = jnp.dot(
        step_ref[...], chosen, preferred_element_type=F32
    ).astype(BF16)
    for k, ref in enumerate((value_taps_ref, write_taps_ref, read_taps_ref)):
        taps_ref[0:4, k * STATE : (k + 1) * STATE] = ref[...]
    blocks = length // BLOCK
    pairs = heads * blocks
    for b in range(blocks):
        at = slice(b * BLOCK, (b + 1) * BLOCK)
        lanes_ref[b * heads : (b + 1) * heads] = bias_ref[:, at]
        lanes_ref[pairs + b * heads : pairs + (b + 1) * heads] = pld_ref[:, at]
    odd = lax.broadcasted_iota(jnp.int32, (pairs, BLOCK), 0) % 2 == 1
    lanes_ref[2 * pairs : 3 * pairs] = jnp.exp(
        jnp.where(odd, rate_ref[rank * heads + 1], rate_ref[rank * heads])
    )
    at_lane = lax.broadcasted_iota(jnp.int32, (1, STATE), 1)
    level = (rank * 2 + at_lane // POOL_DIM) % 4
    window = jnp.where(
        level == 0, 2.0, jnp.where(level == 1, 4.0, jnp.where(level == 2, 8.0, 16.0))
    )
    lanes_ref[3 * pairs : 3 * pairs + 1] = window
    lanes_ref[3 * pairs + 1 : 3 * pairs + 2] = channel_ref[...]
    shape = (POOL_DIM, STATE)
    row, lane = (lax.broadcasted_iota(jnp.int32, shape, k) for k in range(2))
    for k in range(2):
        place = jnp.where(lane == row + k * POOL_DIM, 1.0, 0.0).astype(BF16)
        pool_matrix_ref[k * POOL_DIM : (k + 1) * POOL_DIM] = jnp.dot(
            group_ref[k], place, preferred_element_type=F32
        ).astype(BF16)
    count = state_output_ref.shape[0]
    output_ref[:count] = state_output_ref[...]
    output_ref[count:] = pool_output_ref[...]


def halves_kernel(prior_ref, next_ref, first_ref, second_ref):
    half = first_ref.shape[0]
    first_ref[...] = prior_ref[:half]
    second_ref[...] = next_ref[half:]


def project_kernel(*refs):
    *row_refs, w_ref, other_ref, own_out, other_out, rows_ref = refs
    at = 0
    tails = [ref[...] for ref in row_refs if ref.shape[0] == HALO]
    for ref in row_refs:
        if ref.shape[0] != HALO:
            rows_ref[at : at + ref.shape[0]] = ref[...]
            at += ref.shape[0]
    if tails:
        tail = tails[0]
        for other in tails[1:]:
            tail = tail + other
        rows_ref[at:] = tail
    rows = rows_ref[...]
    own_out[...] = jnp.dot(rows, w_ref[...], preferred_element_type=F32).astype(BF16)
    other_out[...] = jnp.dot(rows, other_ref[...], preferred_element_type=F32).astype(BF16)


def mix_kernel(
    place_ref,
    own_near_ref,
    own_far_ref,
    other_near_ref,
    other_far_ref,
    taps_ref,
    lanes_ref,
    pool_matrix_ref,
    y_ref,
    reads_ref,
    reach_ref,
    gate_ref,
    pool_ref,
    state_ref,
    conv_in,
    pool_in,
    step_in,
    mixed_ref,
):
    length = y_ref.shape[0]
    chunks = length // STEP_ROWS
    blocks = length // BLOCK
    pairs = 2 * blocks
    bias, pld, rate = (lanes_ref[k * pairs : (k + 1) * pairs] for k in range(3))
    window = lanes_ref[3 * pairs : 3 * pairs + 1]
    pool_scale = lanes_ref[3 * pairs + 1 : 3 * pairs + 2]
    base, x, core = place_ref[0], place_ref[1], place_ref[2]
    near = own_near_ref.shape[0] - HALO
    halo = jnp.where(
        core == 0, own_near_ref[near:].astype(F32), other_near_ref[near:].astype(F32)
    )
    conv_in[:HALO] = halo[:, : 3 * STATE]
    pool_in[:HALO] = halo[:, 3 * STATE : 4 * STATE]
    ring = blocks // 2
    for side, near_ref, far_ref in ((core, own_near_ref, own_far_ref), (1 - core, other_near_ref, other_far_ref)):
        for away, source in ((0, near_ref[:BLOCK]), (ring - 1, near_ref[BLOCK : 2 * BLOCK]), (1, near_ref[2 * BLOCK : 3 * BLOCK]), (2, far_ref[...])):
            first = pl.multiple_of(((x + away) % ring * 2 + side) * BLOCK, BLOCK)
            wide = source.astype(F32)
            conv_in[pl.ds(HALO + first, BLOCK)] = wide[:, : 3 * STATE]
            pool_in[pl.ds(HALO + first, BLOCK)] = wide[:, 3 * STATE : 4 * STATE]
            gate_ref[pl.ds(first, BLOCK)] = silu(wide[:, 4 * STATE : 5 * STATE])
            step_in[pl.ds(first, BLOCK)] = wide[:, 5 * STATE :]
    for c in range(chunks):
        first = c * STEP_ROWS
        at = slice(first, first + STEP_ROWS)
        reached = slice(first, first + HALO + STEP_ROWS)
        extended = conv_in[reached]
        summed = extended * taps_ref[3:4, :]
        for back in range(1, 4):
            summed = summed + pltpu.roll(extended, back, 0) * taps_ref[3 - back : 4 - back, :]
        convolved = silu(summed[HALO:]).astype(BF16)
        mixed_ref[at] = convolved[:, : 2 * STATE]
        reads_ref[at] = convolved[:, 2 * STATE :]

        wide = pool_in[reached]
        sum_two = wide + pltpu.roll(wide, 1, 0)
        sum_four = sum_two + pltpu.roll(sum_two, 2, 0)
        sum_eight = sum_four + pltpu.roll(sum_four, 4, 0)
        sum_sixteen = sum_eight + pltpu.roll(sum_eight, 8, 0)
        window_sum = jnp.where(
            window == 2.0,
            sum_two,
            jnp.where(window == 4.0, sum_four, jnp.where(window == 8.0, sum_eight, sum_sixteen)),
        )[HALO:]
        position = (
            base + first + 1 + lax.broadcasted_iota(jnp.int32, (STEP_ROWS, 1), 0)
        ).astype(F32)
        difference = (window_sum / jnp.minimum(position, window) - wide[HALO:]).astype(BF16)
        pooled = jnp.dot(difference, pool_matrix_ref[...], preferred_element_type=F32)
        pool_ref[at] = (pooled * pool_scale).astype(BF16)

    square = (BLOCK, BLOCK)
    row_at = lax.broadcasted_iota(jnp.int32, square, 0)
    col_at = lax.broadcasted_iota(jnp.int32, square, 1)
    upper = (row_at <= col_at).astype(F32)
    causal = row_at >= col_at
    spread = step_in[:BLOCK]
    for b in range(1, blocks):
        spread = spread + pltpu.roll(step_in[b * BLOCK : (b + 1) * BLOCK], 2 * b, 1)
    step = jax.nn.softplus(spread.T[:pairs] + bias)
    cum = jnp.dot(
        pld - rate * step,
        upper,
        precision=lax.Precision.HIGHEST,
        preferred_element_type=F32,
    )
    total = jnp.broadcast_to(cum[:, BLOCK - 1 :], (pairs, BLOCK))
    prefix = jnp.zeros((2, BLOCK), F32)
    prefixes = []
    for b in range(blocks):
        prefixes.append(prefix)
        prefix = prefix + total[2 * b : 2 * b + 2]
    columns = jnp.concatenate(
        [
            cum,
            jnp.exp(total - cum) * step,
            jnp.exp(cum),
            jnp.exp(jnp.concatenate(prefixes, axis=0) + cum),
            jnp.zeros((BLOCK - 4 * pairs, BLOCK), F32),
        ],
        axis=0,
    ).T

    def column(kind, b, h):
        j = kind * pairs + 2 * b + h
        return columns[:, j : j + 1]

    carried = jnp.zeros((STATE, STATE), F32)
    for b in range(blocks):
        at = slice(b * BLOCK, (b + 1) * BLOCK)
        values = mixed_ref[at, :STATE]
        writes = mixed_ref[at, STATE:]
        reads = reads_ref[at]
        affinity = lax.dot_general(
            reads, writes, (((1,), (1,)), ((), ())), preferred_element_type=F32
        )
        inside = []
        for h in range(2):
            row = 2 * b + h
            spacing = column(0, b, h) - cum[row : row + 1]
            within = affinity * jnp.exp(jnp.where(causal, spacing, -jnp.inf)) * step[row : row + 1]
            inside.append(jnp.dot(within.astype(BF16), values, preferred_element_type=F32))
        weighted = (
            values.astype(F32) * by_head(column(1, b, 0), column(1, b, 1), square)
        ).astype(BF16)
        contrib = lax.dot_general(
            writes, weighted, (((0,), (0,)), ((), ())), preferred_element_type=F32
        )
        local = jnp.dot(reads, carried.astype(BF16), preferred_element_type=F32)
        y_ref[at] = by_head(inside[0], inside[1], square) + local * by_head(
            column(2, b, 0), column(2, b, 1), square
        )
        reach_ref[at] = by_head(column(3, b, 0), column(3, b, 1), square)
        decay = by_head(total[2 * b : 2 * b + 1], total[2 * b + 1 : 2 * b + 2], (1, STATE))
        carried = carried * jnp.exp(decay) + contrib
    packed = pack(carried, by_head(prefix[0:1], prefix[1:2], (1, STATE)))
    for k in range(state_ref.shape[0]):
        state_ref[k] = packed


def pack(state, total):
    high = total.astype(BF16)
    low = (total - high.astype(F32)).astype(BF16)
    row = lax.broadcasted_iota(jnp.int32, (PACKED - STATE, STATE), 0)
    tail = jnp.where(row == 0, high.astype(F32), jnp.where(row == 1, low.astype(F32), 0.0))
    return jnp.concatenate([state.astype(BF16), tail.astype(BF16)], axis=0)


def scan_pieces(pieces_ref, here):
    state = before_state = jnp.zeros((STATE, STATE), F32)
    total = before_total = jnp.zeros((1, STATE), F32)
    for k in range(pieces_ref.shape[0]):
        tail = pieces_ref[k, STATE:, :].astype(F32)
        decay = tail[0:1, :] + tail[1:2, :]
        state = state * jnp.exp(decay) + pieces_ref[k, :STATE, :].astype(F32)
        total = total + decay
        passed = k < here
        before_state = jnp.where(passed, state, before_state)
        before_total = jnp.where(passed, total, before_total)
    return state, total, before_state, before_total


def row_scan_kernel(here_ref, pieces_ref, before_ref, packed_ref):
    state, total, before_state, before_total = scan_pieces(pieces_ref, here_ref[0])
    before_ref[:STATE, :] = before_state
    before_ref[STATE:, :] = jnp.broadcast_to(before_total, (8, STATE))
    packed = pack(state, total)
    for k in range(packed_ref.shape[0]):
        packed_ref[k] = packed


def finish_kernel(
    here_ref,
    pieces_ref,
    before_ref,
    y_ref,
    reads_ref,
    reach_ref,
    gate_ref,
    pool_ref,
    scale_ref,
    out_ref,
):
    _, _, rows_before, _ = scan_pieces(pieces_ref, here_ref[0])
    incoming = rows_before * jnp.exp(before_ref[STATE : STATE + 1, :]) + before_ref[:STATE, :]
    crossed = jnp.dot(reads_ref[...], incoming.astype(BF16), preferred_element_type=F32)
    gated = (y_ref[...] + crossed * reach_ref[...]) * gate_ref[...]
    norm = lax.rsqrt(jnp.mean(gated * gated, axis=-1, keepdims=True) + EPS)
    out_ref[:, :STATE] = (gated * norm * scale_ref[...]).astype(BF16)
    out_ref[:, STATE:] = pool_ref[...]


def output_kernel(place_ref, rows_ref, own_ref, prior_ref, next_ref, far_a_ref, far_b_ref, keep_ref, send_ref, total_ref):
    x, core = place_ref[1], place_ref[2]
    ring = rows_ref.shape[0]
    half = far_a_ref.shape[0]
    total = jnp.dot(rows_ref[x], own_ref[...], preferred_element_type=F32)
    total = total + jnp.dot(rows_ref[(x + ring - 1) % ring], prior_ref[...], preferred_element_type=F32)
    total = total + jnp.dot(rows_ref[(x + 1) % ring], next_ref[...], preferred_element_type=F32)
    far = rows_ref[(x + 2) % ring]
    total = total + jnp.dot(far[:, :half], far_a_ref[...], preferred_element_type=F32)
    total_ref[...] = total + jnp.dot(far[:, half:], far_b_ref[...], preferred_element_type=F32)
    count = keep_ref.shape[0]
    keep_ref[...] = total_ref[pl.ds(pl.multiple_of(core * count, count), count)]
    send_ref[...] = total_ref[pl.ds(pl.multiple_of((1 - core) * count, count), count)].astype(BF16)


def join_kernel(keep_ref, other_ref, out_ref):
    out_ref[...] = (keep_ref[...] + other_ref[...].astype(F32)).astype(BF16)


def limits(mebibytes):
    return pltpu.CompilerParams(vmem_limit_bytes=mebibytes * 2**20)


def whole(shape):
    return pl.BlockSpec(shape, lambda *_: (0,) * len(shape))


def normalize(rows, scale):
    wide = rows.astype(F32)
    return (wide * lax.rsqrt(jnp.mean(wide * wide, axis=-1, keepdims=True) + EPS) * scale).astype(
        BF16
    )


def rows_before(rows, ring):
    ranges = lax.axis_size(SP)
    members = 2 * ring
    return [
        lax.ppermute(
            rows,
            SP_TP,
            [(i * members + members - 1, (i + 1) * members + 2 * k) for i in range(ranges - 1)],
        )
        for k in range(ring)
    ]


def around(array, away):
    ring = lax.axis_size("x")
    return lax.ppermute(array, "x", [(i, (i + away) % ring) for i in range(ring)])


def swapped(array):
    return lax.ppermute(array, "core", [(0, 1), (1, 0)])


def kernel_call(body, out_shape, *arrays, scratch=(), mebibytes=16):
    def spec(array):
        if array.ndim == 1:
            return pl.BlockSpec(memory_space=pltpu.SMEM)
        return whole(array.shape)

    return pl.pallas_call(
        body,
        grid=(1,),
        in_specs=[spec(array) for array in arrays],
        out_specs=jax.tree.map(lambda out: whole(out.shape), out_shape),
        out_shape=out_shape,
        scratch_shapes=list(scratch),
        compiler_params=limits(mebibytes),
    )(*arrays)


def held(shape, dtype):
    return jax.ShapeDtypeStruct(shape, dtype)


def shards(
    activations,
    input_norm_scale,
    value_weight_matrix,
    gate_weight_matrix,
    write_weight_matrix,
    read_weight_matrix,
    step_weight_matrix,
    pooling_input_matrix,
    value_filter_weight,
    write_filter_weight,
    read_filter_weight,
    head_log_decay_rate,
    step_bias_offset,
    position_log_decay,
    gated_norm_scale,
    pooling_group_matrix,
    pooling_channel_scale,
    state_output_matrix,
    pooling_output_matrix,
):
    x, core = lax.axis_index("x"), lax.axis_index("core")
    ring = lax.axis_size("x")
    sp_rank = lax.axis_index(SP)
    own_rows, width = activations.shape
    length = own_rows * ring * 2
    blocks = length // BLOCK
    scale = input_norm_scale.reshape(1, width)

    place = jnp.stack([sp_rank * length, x, core]).astype(jnp.int32)
    normed, tail = kernel_call(
        norm_kernel, [held((own_rows, width), BF16), held((HALO, width), BF16)], activations, scale
    )
    prior = around(normed, 1)
    following = around(normed, -1)
    found = rows_before(tail, ring)
    output_rows = state_output_matrix.shape[0] + pooling_output_matrix.shape[0]
    weights, taps, lanes, pool_matrix, own_output = kernel_call(
        prepare_kernel,
        [
            held((width, 6 * STATE), BF16),
            held((8, 3 * STATE), F32),
            held((6 * blocks + 8, STATE), F32),
            held((STATE, STATE), BF16),
            held((output_rows, width), BF16),
        ],
        place,
        head_log_decay_rate,
        value_weight_matrix,
        write_weight_matrix,
        read_weight_matrix,
        pooling_input_matrix,
        gate_weight_matrix,
        step_weight_matrix,
        value_filter_weight,
        write_filter_weight,
        read_filter_weight,
        step_bias_offset,
        position_log_decay,
        pooling_group_matrix,
        pooling_channel_scale.reshape(1, STATE),
        state_output_matrix,
        pooling_output_matrix,
        mebibytes=24,
    )
    other_weights = swapped(weights)
    half = own_rows // 2
    far = kernel_call(halves_kernel, [held((half, width), BF16)] * 2, prior, following)
    far_first = around(far[0], 1)
    far_second = around(far[1], -1)

    def project(*pieces):
        count = sum(piece.shape[0] for piece in pieces if piece.shape[0] > HALO)
        count += HALO * any(piece.shape[0] == HALO for piece in pieces)
        return kernel_call(
            project_kernel,
            [held((count, weights.shape[1]), BF16)] * 2,
            *pieces,
            weights,
            other_weights,
            scratch=[pltpu.VMEM((count, width), BF16)],
            mebibytes=24,
        )

    own_near, send_near = project(normed, prior, following, *found)
    other_near = swapped(send_near)
    own_far, send_far = project(far_first, far_second)
    other_far = swapped(send_far)

    columns, inner = lax.axis_size("sp_0"), lax.axis_size("sp_1")
    y, reads, reach, gate, pool, packed = kernel_call(
        mix_kernel,
        [
            held((length, STATE), F32),
            held((length, STATE), BF16),
            held((length, STATE), F32),
            held((length, STATE), F32),
            held((length, STATE), BF16),
            held((inner, PACKED, STATE), BF16),
        ],
        place,
        own_near,
        own_far,
        other_near,
        other_far,
        taps,
        lanes,
        pool_matrix,
        scratch=[
            pltpu.VMEM((HALO + length, 3 * STATE), F32),
            pltpu.VMEM((HALO + length, STATE), F32),
            pltpu.VMEM((length, STATE), F32),
            pltpu.VMEM((length, 2 * STATE), BF16),
        ],
        mebibytes=24,
    )

    packed, own_output = lax.optimization_barrier((packed, own_output))
    prior_output = around(own_output, 1)
    next_output = around(own_output, -1)
    pieces = lax.all_to_all(packed, "sp_1", 0, 0, tiled=True)
    before, packed = kernel_call(
        row_scan_kernel,
        [held((STATE + 8, STATE), F32), held((columns, PACKED, STATE), BF16)],
        lax.axis_index("sp_1").astype(jnp.int32).reshape(1),
        pieces,
        mebibytes=8,
    )
    pieces = lax.all_to_all(packed, "sp_0", 0, 0, tiled=True)
    prior_output, next_output, pieces = lax.optimization_barrier(
        (prior_output, next_output, pieces)
    )
    half = output_rows // 2
    far = kernel_call(halves_kernel, [held((half, width), BF16)] * 2, prior_output, next_output)
    far_output = (around(far[0], 1), around(far[1], -1))
    branches = kernel_call(
        finish_kernel,
        held((length, 2 * STATE), BF16),
        lax.axis_index("sp_0").astype(jnp.int32).reshape(1),
        pieces,
        before,
        y,
        reads,
        reach,
        gate,
        pool,
        gated_norm_scale.reshape(1, STATE),
    )
    branches = lax.all_to_all(
        branches.reshape(ring, 2 * own_rows, 2 * STATE), "x", 0, 0, tiled=True
    )
    keep, send = kernel_call(
        output_kernel,
        [held((own_rows, width), F32), held((own_rows, width), BF16)],
        place,
        branches,
        own_output,
        prior_output,
        next_output,
        *far_output,
        scratch=[pltpu.VMEM((2 * own_rows, width), F32)],
        mebibytes=24,
    )
    return kernel_call(join_kernel, held((own_rows, width), BF16), keep, swapped(send), mebibytes=8)


def solution(mesh):
    ranges = mesh.shape["sp"]
    inner = 8 if ranges % 8 == 0 else 2
    shape = (ranges // inner, inner, mesh.shape["tp"] // 2, 2)
    torus = Mesh(mesh.devices.reshape(shape), SP_TP)
    in_specs = (
        P(SP_TP, None),
        P(),
        P(None, TP),
        P(None, TP),
        P(None, TP),
        P(None, TP),
        P(),
        P(None, TP),
        P(None, TP),
        P(None, TP),
        P(None, TP),
        P(),
        P(TP, SP),
        P(TP, SP),
        P(TP),
        P(TP, None, None),
        P(TP),
        P(TP, None),
        P(TP, None),
    )

    return jax.shard_map(
        shards, mesh=torus, in_specs=in_specs, out_specs=P(SP_TP, None), check_vma=False
    )
```

profile of v0, /device:TPU:7, one launch (start us, length us, event | category | flops | bytes accessed | tf_op | source)
XLA Modules:
  0.0 139.8 jit_solution(14023899958303804536)
XLA Ops:
  0.0 1.2 copy.20.step_ref
  1.2 0.1 pad_add_fusion.place_ref
  1.3 1.0 copy-done.1
  2.3 1.0 copy-done.2
  3.4 1.0 copy-done.3
  4.4 1.0 copy-done.4
  5.4 1.0 copy-done.5
  6.5 1.0 copy-done.6
  7.5 1.0 copy-done.7
  8.6 0.8 copy-done.8
  9.3 0.7 copy-done.9
  10.0 0.7 copy-done.10
  10.7 0.7 copy-done.12
  11.4 0.7 copy-done.13
  12.1 0.7 copy-done.14
  12.8 0.7 copy-done.16
  13.4 0.7 copy-done.17
  14.1 1.3 shard_map.182
  15.4 2.6 %collective-permute-start.6 = (bf16[2048,768]{1,0:T(8,128)(2,1)S(1)}, bf16[2048,768]{1,0:T(8,128)(2,1)S(1)}, u32[]{:S(2)}, u32[]{:S(2)}) collective-permute-start(bf16[2048,768]{1,0:T(8,128)(2,1)S(1)} %get-tuple-element.37.refs_7_.refs_2_), channel_id=1, source_target_pairs={{0,1},{1,0},{2,3},{3,2},{4,5},{5,4},{6,7},{7,6},{8,9},{9,8},{10,11... | collective-permute-start | bytes 9437192 | tf_op jit(solution)/shard_map/ppermute | solution.py:374
  18.0 0.2 shard_map.181
  18.2 7.4 %collective-permute-start = (bf16[128,2048]{1,0:T(8,128)(2,1)S(1)}, bf16[128,2048]{1,0:T(8,128)(2,1)S(1)}, u32[]{:S(2)}, u32[]{:S(2)}) collective-permute-start(bf16[128,2048]{1,0:T(8,128)(2,1)S(1)} %get-tuple-element.35.refs_0_), channel_id=1, source_target_pairs={{0,2},{2,4},{4,6},{6,0},{1,3},{3,5},{5,7},{7,1},{8,10},{10,12},{12... | collective-permute-start | bytes 1572872 | tf_op jit(solution)/shard_map/ppermute | solution.py:370
  25.7 1.9 %collective-permute-start.1 = (bf16[128,2048]{1,0:T(8,128)(2,1)S(1)}, bf16[128,2048]{1,0:T(8,128)(2,1)S(1)}, u32[]{:S(2)}, u32[]{:S(2)}) collective-permute-start(bf16[128,2048]{1,0:T(8,128)(2,1)S(1)} %get-tuple-element.35.refs_0_), channel_id=1, source_target_pairs={{0,6},{2,0},{4,2},{6,4},{1,7},{3,1},{5,3},{7,5},{8,14},{10,8},{12,... | collective-permute-start | bytes 1572872 | tf_op jit(solution)/shard_map/ppermute | solution.py:370
  27.6 1.3 collective-permute-start.2
  28.9 1.3 collective-permute-start.3
  30.2 0.0 collective-permute-done.2.refs_3_
  30.2 1.3 collective-permute-start.4
  31.5 0.0 collective-permute-done.3.refs_4_
  31.5 1.3 collective-permute-start.5
  32.8 0.0 collective-permute-done.4.refs_5_
  32.8 1.3 collective-permute-done.5.refs_6_
  34.1 2.8 %collective-permute-done.refs_1_.prior_ref = bf16[128,2048]{1,0:T(8,128)(2,1)S(1)} collective-permute-done((bf16[128,2048]{1,0:T(8,128)(2,1)S(1)}, bf16[128,2048]{1,0:T(8,128)(2,1)S(1)}, u32[]{:S(2)}, u32[]{:S(2)}) %collective-permute-start) | collective-permute-done | bytes 524320 | tf_op jit(solution)/shard_map/ppermute | solution.py:370
  36.9 5.0 %collective-permute-done.1.refs_2_.next_ref = bf16[128,2048]{1,0:T(8,128)(2,1)S(1)} collective-permute-done((bf16[128,2048]{1,0:T(8,128)(2,1)S(1)}, bf16[128,2048]{1,0:T(8,128)(2,1)S(1)}, u32[]{:S(2)}, u32[]{:S(2)}) %collective-permute-start.1) | collective-permute-done | bytes 524320 | tf_op jit(solution)/shard_map/ppermute | solution.py:370
  42.0 0.0 collective-permute-done.6.refs_8_.refs_3_
  42.0 2.7 %shard_map.183 = (bf16[400,768]{1,0:T(8,128)(2,1)S(1)}, bf16[400,768]{1,0:T(8,128)(2,1)S(1)}) custom-call(bf16[128,2048]{1,0:T(8,128)(2,1)S(1)} %get-tuple-element.35.refs_0_, bf16[128,2048]{1,0:T(8,128)(2,1)S(1)} %collective-permute-done.refs_1_.prior_ref, bf16[128,2048]{1,0:T(8,128)(2,1)S(1)} %collective-permute-done.1.refs_2_.next_ref, ...), custom_call_target="tpu_custom_call" | custom-call | tf_op jit(solution)/shard_map/pallas_call | solution.py:383
  44.7 3.1 %collective-permute-start.9 = (bf16[400,768]{1,0:T(8,128)(2,1)S(1)}, bf16[400,768]{1,0:T(8,128)(2,1)S(1)}, u32[]{:S(2)}, u32[]{:S(2)}) collective-permute-start(bf16[400,768]{1,0:T(8,128)(2,1)S(1)} %get-tuple-element.42), channel_id=1, source_target_pairs={{0,1},{1,0},{2,3},{3,2},{4,5},{5,4},{6,7},{7,6},{8,9},{9,8},{10,11... | collective-permute-start | bytes 1843208 | tf_op jit(solution)/shard_map/ppermute | solution.py:374
  47.8 1.9 %collective-permute-start.7 = (bf16[64,2048]{1,0:T(8,128)(2,1)S(1)}, bf16[64,2048]{1,0:T(8,128)(2,1)S(1)}, u32[]{:S(2)}, u32[]{:S(2)}) collective-permute-start(bf16[64,2048]{1,0:T(8,128)(2,1)S(1)} %get-tuple-element.39), channel_id=1, source_target_pairs={{0,2},{2,4},{4,6},{6,0},{1,3},{3,5},{5,7},{7,1},{8,10},{10,12},{12... | collective-permute-start | bytes 786440 | tf_op jit(solution)/shard_map/ppermute | solution.py:370
  49.7 3.4 %collective-permute-start.8 = (bf16[64,2048]{1,0:T(8,128)(2,1)S(1)}, bf16[64,2048]{1,0:T(8,128)(2,1)S(1)}, u32[]{:S(2)}, u32[]{:S(2)}) collective-permute-start(bf16[64,2048]{1,0:T(8,128)(2,1)S(1)} %get-tuple-element.40), channel_id=1, source_target_pairs={{0,6},{2,0},{4,2},{6,4},{1,7},{3,1},{5,3},{7,5},{8,14},{10,8},{12,... | collective-permute-start | bytes 786440 | tf_op jit(solution)/shard_map/ppermute | solution.py:370
  53.1 4.4 %collective-permute-done.7.refs_0_ = bf16[64,2048]{1,0:T(8,128)(2,1)S(1)} collective-permute-done((bf16[64,2048]{1,0:T(8,128)(2,1)S(1)}, bf16[64,2048]{1,0:T(8,128)(2,1)S(1)}, u32[]{:S(2)}, u32[]{:S(2)}) %collective-permute-start.7) | collective-permute-done | bytes 262176 | tf_op jit(solution)/shard_map/ppermute | solution.py:370
  57.5 3.1 %collective-permute-done.8.refs_1_ = bf16[64,2048]{1,0:T(8,128)(2,1)S(1)} collective-permute-done((bf16[64,2048]{1,0:T(8,128)(2,1)S(1)}, bf16[64,2048]{1,0:T(8,128)(2,1)S(1)}, u32[]{:S(2)}, u32[]{:S(2)}) %collective-permute-start.8) | collective-permute-done | bytes 262176 | tf_op jit(solution)/shard_map/ppermute | solution.py:370
  60.7 1.0 shard_map.185
  61.7 0.0 copy-start.15
  61.7 2.8 %collective-permute-start.10 = (bf16[128,768]{1,0:T(8,128)(2,1)S(1)}, bf16[128,768]{1,0:T(8,128)(2,1)S(1)}, u32[]{:S(2)}, u32[]{:S(2)}) collective-permute-start(bf16[128,768]{1,0:T(8,128)(2,1)S(1)} %get-tuple-element.43), channel_id=1, source_target_pairs={{0,1},{1,0},{2,3},{3,2},{4,5},{5,4},{6,7},{7,6},{8,9},{9,8},{10,11... | collective-permute-start | bytes 589832 | tf_op jit(solution)/shard_map/ppermute | solution.py:374
  64.5 1.0 collective-permute-done.10.other_far_ref
  65.5 0.0 collective-permute-done.9.other_near_ref
  65.5 3.7 %shard_map.186 = (f32[1024,128]{1,0:T(8,128)S(1)}, bf16[1024,128]{1,0:T(8,128)(2,1)S(1)}, f32[1024,128]{1,0:T(8,128)S(1)}, f32[1024,128]{1,0:T(8,128)S(1)}, bf16...) custom-call(s32[3]{0:T(128)S(1)} %pad_add_fusion.place_ref, ...), custom_call_target="tpu_custom_call" | custom-call | tf_op jit(solution)/shard_map/pallas_call | solution.py:383
  69.3 1.9 %collective-permute-start.11 = (bf16[256,2048]{1,0:T(8,128)(2,1)S(1)}, bf16[256,2048]{1,0:T(8,128)(2,1)S(1)}, u32[]{:S(2)}, u32[]{:S(2)}) collective-permute-start(bf16[256,2048]{1,0:T(8,128)(2,1)S(1)} %get-tuple-element.49.own_ref), channel_id=1, source_target_pairs={{0,2},{2,4},{4,6},{6,0},{1,3},{3,5},{5,7},{7,1},{8,10},{10,12},{12... | collective-permute-start | bytes 3145736 | tf_op jit(solution)/shard_map/ppermute | solution.py:370
  71.2 3.4 %collective-permute-start.12 = (bf16[256,2048]{1,0:T(8,128)(2,1)S(1)}, bf16[256,2048]{1,0:T(8,128)(2,1)S(1)}, u32[]{:S(2)}, u32[]{:S(2)}) collective-permute-start(bf16[256,2048]{1,0:T(8,128)(2,1)S(1)} %get-tuple-element.49.own_ref), channel_id=1, source_target_pairs={{0,6},{2,0},{4,2},{6,4},{1,7},{3,1},{5,3},{7,5},{8,14},{10,8},{12,... | collective-permute-start | bytes 3145736 | tf_op jit(solution)/shard_map/ppermute | solution.py:370
  74.5 13.4 %all_to_all.15.pieces_ref = bf16[8,144,128]{2,1,0:T(8,128)(2,1)S(1)} all-to-all(bf16[8,144,128]{2,1,0:T(8,128)(2,1)S(1)} %get-tuple-element.50), channel_id=1, replica_groups=mesh['sp_0'=8,'sp_1'=8,'x'=4,'core'=2] {'sp_1'}, dimensions={0} | all-to-all | bytes 589824 | tf_op jit(solution)/shard_map/all_to_all | solution.py:518
  88.0 0.1 shard_map.187
  88.1 18.1 %all_to_all.16.pieces_ref = bf16[8,144,128]{2,1,0:T(8,128)(2,1)S(1)} all-to-all(bf16[8,144,128]{2,1,0:T(8,128)(2,1)S(1)} %get-tuple-element.51), channel_id=1, replica_groups=mesh['sp_0'=8,'sp_1'=8,'x'=4,'core'=2] {'sp_0'}, dimensions={0} | all-to-all | bytes 589824 | tf_op jit(solution)/shard_map/all_to_all | solution.py:526
  106.2 0.0 collective-permute-done.11.prior_ref
  106.2 0.0 collective-permute-done.12.next_ref
  106.2 0.1 shard_map.189
  106.2 4.0 %collective-permute-start.13 = (bf16[128,2048]{1,0:T(8,128)(2,1)S(1)}, bf16[128,2048]{1,0:T(8,128)(2,1)S(1)}, u32[]{:S(2)}, u32[]{:S(2)}) collective-permute-start(bf16[128,2048]{1,0:T(8,128)(2,1)S(1)} %get-tuple-element.61), channel_id=1, source_target_pairs={{0,2},{2,4},{4,6},{6,0},{1,3},{3,5},{5,7},{7,1},{8,10},{10,12},{12... | collective-permute-start | bytes 1572872 | tf_op jit(solution)/shard_map/ppermute | solution.py:370
  110.2 1.9 %collective-permute-start.14 = (bf16[128,2048]{1,0:T(8,128)(2,1)S(1)}, bf16[128,2048]{1,0:T(8,128)(2,1)S(1)}, u32[]{:S(2)}, u32[]{:S(2)}) collective-permute-start(bf16[128,2048]{1,0:T(8,128)(2,1)S(1)} %get-tuple-element.62), channel_id=1, source_target_pairs={{0,6},{2,0},{4,2},{6,4},{1,7},{3,1},{5,3},{7,5},{8,14},{10,8},{12,... | collective-permute-start | bytes 1572872 | tf_op jit(solution)/shard_map/ppermute | solution.py:370
  112.2 0.0 copy-done.15
  112.2 0.5 shard_map.188
  112.7 13.7 %all_to_all.17.rows_ref = bf16[4,256,256]{2,1,0:T(8,128)(2,1)S(1)} all-to-all(bf16[4,256,256]{2,1,0:T(8,128)(2,1)S(1)} %bitcast.9), channel_id=1, replica_groups=mesh['sp_0'=8,'sp_1'=8,'x'=4,'core'=2] {'x'}, dimensions={0} | all-to-all | bytes 1048576 | tf_op jit(solution)/shard_map/all_to_all | solution.py:546
  126.4 0.0 collective-permute-done.13.far_a_ref
  126.4 0.0 collective-permute-done.14.far_b_ref
  126.4 2.2 %shard_map.190 = (f32[128,2048]{1,0:T(8,128)S(1)}, bf16[128,2048]{1,0:T(8,128)(2,1)S(1)}) custom-call(s32[3]{0:T(128)S(1)} %pad_add_fusion.place_ref, bf16[4,256,256]{2,1,0:T(8,128)(2,1)S(1)} %all_to_all.17.rows_ref, bf16[256,2048]{1,0:T(8,128)(2,1)S(1)} %get-tuple-element.49.own_ref, bf16[256,2048]{1,0:T(8,128)(2,1)S(1)} %collective-permute-done.11.prior_ref, ...), custom_call_target="tpu_custom_call" | custom-call | tf_op jit(solution)/shard_map/pallas_call | solution.py:383
  128.6 8.8 %collective-permute-start.15 = (bf16[128,2048]{1,0:T(8,128)(2,1)S(1)}, bf16[128,2048]{1,0:T(8,128)(2,1)S(1)}, u32[]{:S(2)}, u32[]{:S(2)}) collective-permute-start(bf16[128,2048]{1,0:T(8,128)(2,1)S(1)} %get-tuple-element.64), channel_id=1, source_target_pairs={{0,1},{1,0},{2,3},{3,2},{4,5},{5,4},{6,7},{7,6},{8,9},{9,8},{10,11... | collective-permute-start | bytes 1572872 | tf_op jit(solution)/shard_map/ppermute | solution.py:374
  137.4 1.5 %collective-permute-done.15.other_ref = bf16[128,2048]{1,0:T(8,128)(2,1)S(1)} collective-permute-done((bf16[128,2048]{1,0:T(8,128)(2,1)S(1)}, bf16[128,2048]{1,0:T(8,128)(2,1)S(1)}, u32[]{:S(2)}, u32[]{:S(2)}) %collective-permute-start.15) | collective-permute-done | bytes 524320 | tf_op jit(solution)/shard_map/ppermute | solution.py:374
  138.9 0.9 shard_map.191
  (20 shorter events, 0.1 us)
Async XLA Ops:
  0.0 18.0 %copy-start.11 = (f32[2048]{0:T(1024)S(1)}, f32[2048]{0:T(1024)}, u32[]{:S(2)}) copy-start(f32[2048]{0:T(1024)} %param.20) | copy-start | bytes 24580
  0.0 18.0 %copy-start = (bf16[128,2048]{1,0:T(8,128)(2,1)S(1)}, bf16[128,2048]{1,0:T(8,128)(2,1)}, u32[]{:S(2)}) copy-start(bf16[128,2048]{1,0:T(8,128)(2,1)} %x_ref.1) | copy-start | bytes 1572868
  1.3 1.0 copy-start.1
  2.3 1.0 copy-start.2
  3.4 1.0 copy-start.3
  4.4 1.0 copy-start.4
  5.4 1.0 copy-start.5
  6.5 1.0 copy-start.6
  7.5 1.0 copy-start.7
  8.6 0.8 copy-start.8
  9.3 0.7 copy-start.9
  10.0 0.7 copy-start.10
  10.7 0.7 copy-start.12
  11.4 0.7 copy-start.13
  12.1 0.7 copy-start.14
  12.8 0.7 copy-start.16
  13.4 0.7 copy-start.17
  15.4 26.6 %collective-permute-start.6 = (bf16[2048,768]{1,0:T(8,128)(2,1)S(1)}, bf16[2048,768]{1,0:T(8,128)(2,1)S(1)}, u32[]{:S(2)}, u32[]{:S(2)}) collective-permute-start(bf16[2048,768]{1,0:T(8,128)(2,1)S(1)} %get-tuple-element.37.refs_7_.refs_2_), channel_id=1, source_target_pairs={{0,1},{1,0},{2,3},{3,2},{4,5},{5,4},{6,7},{7,6},{8,9},{9,8},{10,11... | collective-permute-start | bytes 9437192 | tf_op jit(solution)/shard_map/ppermute | solution.py:374
  18.2 18.7 %collective-permute-start = (bf16[128,2048]{1,0:T(8,128)(2,1)S(1)}, bf16[128,2048]{1,0:T(8,128)(2,1)S(1)}, u32[]{:S(2)}, u32[]{:S(2)}) collective-permute-start(bf16[128,2048]{1,0:T(8,128)(2,1)S(1)} %get-tuple-element.35.refs_0_), channel_id=1, source_target_pairs={{0,2},{2,4},{4,6},{6,0},{1,3},{3,5},{5,7},{7,1},{8,10},{10,12},{12... | collective-permute-start | bytes 1572872 | tf_op jit(solution)/shard_map/ppermute | solution.py:370
  25.7 16.3 %collective-permute-start.1 = (bf16[128,2048]{1,0:T(8,128)(2,1)S(1)}, bf16[128,2048]{1,0:T(8,128)(2,1)S(1)}, u32[]{:S(2)}, u32[]{:S(2)}) collective-permute-start(bf16[128,2048]{1,0:T(8,128)(2,1)S(1)} %get-tuple-element.35.refs_0_), channel_id=1, source_target_pairs={{0,6},{2,0},{4,2},{6,4},{1,7},{3,1},{5,3},{7,5},{8,14},{10,8},{12,... | collective-permute-start | bytes 1572872 | tf_op jit(solution)/shard_map/ppermute | solution.py:370
  27.6 2.6 %collective-permute-start.2 = (bf16[16,2048]{1,0:T(8,128)(2,1)S(1)}, bf16[16,2048]{1,0:T(8,128)(2,1)S(1)}, u32[]{:S(2)}, u32[]{:S(2)}) collective-permute-start(bf16[16,2048]{1,0:T(8,128)(2,1)S(1)} %get-tuple-element.36), channel_id=1, source_target_pairs={{7,8},{15,16},{23,24},{31,32},{39,40},{47,48},{55,56},{63,64},{71,... | collective-permute-start | bytes 196616 | tf_op jit(solution)/shard_map/ppermute | solution.py:359
  28.9 2.6 %collective-permute-start.3 = (bf16[16,2048]{1,0:T(8,128)(2,1)S(1)}, bf16[16,2048]{1,0:T(8,128)(2,1)S(1)}, u32[]{:S(2)}, u32[]{:S(2)}) collective-permute-start(bf16[16,2048]{1,0:T(8,128)(2,1)S(1)} %get-tuple-element.36), channel_id=1, source_target_pairs={{7,10},{15,18},{23,26},{31,34},{39,42},{47,50},{55,58},{63,66},{71... | collective-permute-start | bytes 196616 | tf_op jit(solution)/shard_map/ppermute | solution.py:359
  30.2 2.6 %collective-permute-start.4 = (bf16[16,2048]{1,0:T(8,128)(2,1)S(1)}, bf16[16,2048]{1,0:T(8,128)(2,1)S(1)}, u32[]{:S(2)}, u32[]{:S(2)}) collective-permute-start(bf16[16,2048]{1,0:T(8,128)(2,1)S(1)} %get-tuple-element.36), channel_id=1, source_target_pairs={{7,12},{15,20},{23,28},{31,36},{39,44},{47,52},{55,60},{63,68},{71... | collective-permute-start | bytes 196616 | tf_op jit(solution)/shard_map/ppermute | solution.py:359
  31.5 2.6 %collective-permute-start.5 = (bf16[16,2048]{1,0:T(8,128)(2,1)S(1)}, bf16[16,2048]{1,0:T(8,128)(2,1)S(1)}, u32[]{:S(2)}, u32[]{:S(2)}) collective-permute-start(bf16[16,2048]{1,0:T(8,128)(2,1)S(1)} %get-tuple-element.36), channel_id=1, source_target_pairs={{7,14},{15,22},{23,30},{31,38},{39,46},{47,54},{55,62},{63,70},{71... | collective-permute-start | bytes 196616 | tf_op jit(solution)/shard_map/ppermute | solution.py:359
  44.7 20.8 %collective-permute-start.9 = (bf16[400,768]{1,0:T(8,128)(2,1)S(1)}, bf16[400,768]{1,0:T(8,128)(2,1)S(1)}, u32[]{:S(2)}, u32[]{:S(2)}) collective-permute-start(bf16[400,768]{1,0:T(8,128)(2,1)S(1)} %get-tuple-element.42), channel_id=1, source_target_pairs={{0,1},{1,0},{2,3},{3,2},{4,5},{5,4},{6,7},{7,6},{8,9},{9,8},{10,11... | collective-permute-start | bytes 1843208 | tf_op jit(solution)/shard_map/ppermute | solution.py:374
  47.8 9.7 %collective-permute-start.7 = (bf16[64,2048]{1,0:T(8,128)(2,1)S(1)}, bf16[64,2048]{1,0:T(8,128)(2,1)S(1)}, u32[]{:S(2)}, u32[]{:S(2)}) collective-permute-start(bf16[64,2048]{1,0:T(8,128)(2,1)S(1)} %get-tuple-element.39), channel_id=1, source_target_pairs={{0,2},{2,4},{4,6},{6,0},{1,3},{3,5},{5,7},{7,1},{8,10},{10,12},{12... | collective-permute-start | bytes 786440 | tf_op jit(solution)/shard_map/ppermute | solution.py:370
  49.7 11.0 %collective-permute-start.8 = (bf16[64,2048]{1,0:T(8,128)(2,1)S(1)}, bf16[64,2048]{1,0:T(8,128)(2,1)S(1)}, u32[]{:S(2)}, u32[]{:S(2)}) collective-permute-start(bf16[64,2048]{1,0:T(8,128)(2,1)S(1)} %get-tuple-element.40), channel_id=1, source_target_pairs={{0,6},{2,0},{4,2},{6,4},{1,7},{3,1},{5,3},{7,5},{8,14},{10,8},{12,... | collective-permute-start | bytes 786440 | tf_op jit(solution)/shard_map/ppermute | solution.py:370
  61.7 50.5 %copy-start.15 = (f32[128]{0:T(128)S(1)}, f32[128]{0:T(128)}, u32[]{:S(2)}) copy-start(f32[128]{0:T(128)} %param.33) | copy-start | bytes 1540
  61.7 3.8 %collective-permute-start.10 = (bf16[128,768]{1,0:T(8,128)(2,1)S(1)}, bf16[128,768]{1,0:T(8,128)(2,1)S(1)}, u32[]{:S(2)}, u32[]{:S(2)}) collective-permute-start(bf16[128,768]{1,0:T(8,128)(2,1)S(1)} %get-tuple-element.43), channel_id=1, source_target_pairs={{0,1},{1,0},{2,3},{3,2},{4,5},{5,4},{6,7},{7,6},{8,9},{9,8},{10,11... | collective-permute-start | bytes 589832 | tf_op jit(solution)/shard_map/ppermute | solution.py:374
  69.3 36.9 %collective-permute-start.11 = (bf16[256,2048]{1,0:T(8,128)(2,1)S(1)}, bf16[256,2048]{1,0:T(8,128)(2,1)S(1)}, u32[]{:S(2)}, u32[]{:S(2)}) collective-permute-start(bf16[256,2048]{1,0:T(8,128)(2,1)S(1)} %get-tuple-element.49.own_ref), channel_id=1, source_target_pairs={{0,2},{2,4},{4,6},{6,0},{1,3},{3,5},{5,7},{7,1},{8,10},{10,12},{12... | collective-permute-start | bytes 3145736 | tf_op jit(solution)/shard_map/ppermute | solution.py:370
  71.2 35.0 %collective-permute-start.12 = (bf16[256,2048]{1,0:T(8,128)(2,1)S(1)}, bf16[256,2048]{1,0:T(8,128)(2,1)S(1)}, u32[]{:S(2)}, u32[]{:S(2)}) collective-permute-start(bf16[256,2048]{1,0:T(8,128)(2,1)S(1)} %get-tuple-element.49.own_ref), channel_id=1, source_target_pairs={{0,6},{2,0},{4,2},{6,4},{1,7},{3,1},{5,3},{7,5},{8,14},{10,8},{12,... | collective-permute-start | bytes 3145736 | tf_op jit(solution)/shard_map/ppermute | solution.py:370
  106.2 20.1 %collective-permute-start.13 = (bf16[128,2048]{1,0:T(8,128)(2,1)S(1)}, bf16[128,2048]{1,0:T(8,128)(2,1)S(1)}, u32[]{:S(2)}, u32[]{:S(2)}) collective-permute-start(bf16[128,2048]{1,0:T(8,128)(2,1)S(1)} %get-tuple-element.61), channel_id=1, source_target_pairs={{0,2},{2,4},{4,6},{6,0},{1,3},{3,5},{5,7},{7,1},{8,10},{10,12},{12... | collective-permute-start | bytes 1572872 | tf_op jit(solution)/shard_map/ppermute | solution.py:370
  110.2 16.2 %collective-permute-start.14 = (bf16[128,2048]{1,0:T(8,128)(2,1)S(1)}, bf16[128,2048]{1,0:T(8,128)(2,1)S(1)}, u32[]{:S(2)}, u32[]{:S(2)}) collective-permute-start(bf16[128,2048]{1,0:T(8,128)(2,1)S(1)} %get-tuple-element.62), channel_id=1, source_target_pairs={{0,6},{2,0},{4,2},{6,4},{1,7},{3,1},{5,3},{7,5},{8,14},{10,8},{12,... | collective-permute-start | bytes 1572872 | tf_op jit(solution)/shard_map/ppermute | solution.py:370
  128.6 10.3 %collective-permute-start.15 = (bf16[128,2048]{1,0:T(8,128)(2,1)S(1)}, bf16[128,2048]{1,0:T(8,128)(2,1)S(1)}, u32[]{:S(2)}, u32[]{:S(2)}) collective-permute-start(bf16[128,2048]{1,0:T(8,128)(2,1)S(1)} %get-tuple-element.64), channel_id=1, source_target_pairs={{0,1},{1,0},{2,3},{3,2},{4,5},{5,4},{6,7},{7,6},{8,9},{9,8},{10,11... | collective-permute-start | bytes 1572872 | tf_op jit(solution)/shard_map/ppermute | solution.py:374
where the time goes:
time: 141 us; the launch traced here: 140 us
  starting transfers between devices  48.3 us (34%)
  blocking collectives  45.2 us (32%)
  waiting for transfers between devices  19.3 us (14%)
  local copies, waits for them, and re-layouts  14 us (10%)
  Pallas kernels  12.7 us (9%)
    ppermute x8, starting transfers between devices, around(): lax.ppermute(array, 'x', [(i, (i + away) % ring) for i in range(ring)])  25.8 us
    all_to_all x1, blocking collectives, shards(): pieces = lax.all_to_all(packed, 'sp_0', 0, 0, tiled=True)  18.1 us
    ppermute x4, starting transfers between devices, swapped(): return lax.ppermute(array, 'core', [(0, 1), (1, 0)])  17.3 us
    ppermute x8, waiting for transfers between devices, around(): lax.ppermute(array, 'x', [(i, (i + away) % ring) for i in range(ring)])  15.4 us
    unnamed x37, local copies, waits for them, and re-layouts  14 us
    all_to_all x1, blocking collectives, shards(): lax.all_to_all(branches.reshape(ring, 2 * own_rows, 2 * STATE), 'x', 0, 0...  13.7 us
    all_to_all x1, blocking collectives, shards(): pieces = lax.all_to_all(packed, 'sp_1', 0, 0, tiled=True)  13.4 us
    pallas_call x11, Pallas kernels, kernel_call(): pl.pallas_call(body, grid=(1,), in_specs=[spec(array) for array in arrays...  12.7 us
  transfers between devices with their start and end apart: 16, of which 7 were waited for; matrix products, arithmetic and copies ran while one was open for 0% of the time, Pallas kernels for 1%

commit v1 on v0

--- a/solution.py
+++ b/solution.py
@@ -30,7 +30,19 @@
     return jnp.where(lane < HEAD_DIM, first, second)
 
 
-def norm_kernel(x_ref, scale_ref, out_ref, tail_ref):
+def fetch(pairs, arrived):
+    copies = [
+        pltpu.make_async_copy(source, target, arrived.at[k])
+        for k, (source, target) in enumerate(pairs)
+    ]
+    for copy in copies:
+        copy.start()
+    for copy in copies:
+        copy.wait()
+
+
+def norm_kernel(x_hbm, scale_hbm, out_ref, tail_ref, x_ref, scale_ref, arrived):
+    fetch(((x_hbm, x_ref), (scale_hbm, scale_ref)), arrived)
     rows = normalize(x_ref[...], scale_ref[...])
     out_ref[...] = rows
     tail_ref[...] = rows[rows.shape[0] - HALO :]
@@ -38,39 +50,40 @@
 
 def prepare_kernel(
     place_ref,
-    rate_ref,
-    value_ref,
-    write_ref,
-    read_ref,
-    pool_ref,
-    gate_ref,
-    step_ref,
-    value_taps_ref,
-    write_taps_ref,
-    read_taps_ref,
-    bias_ref,
-    pld_ref,
-    group_ref,
-    channel_ref,
-    state_output_ref,
-    pool_output_ref,
-    w_ref,
-    taps_ref,
-    lanes_ref,
-    pool_matrix_ref,
-    output_ref,
+    value_hbm,
+    write_hbm,
+    read_hbm,
+    pool_hbm,
+    gate_hbm,
+    state_output_hbm,
+    pool_output_hbm,
+    *refs,
 ):
+    small_hbm, (w_ref, output_hbm, taps_ref, lanes_ref, pool_matrix_ref), small = (
+        refs[:9],
+        refs[9:14],
+        refs[14:23],
+    )
+    arrived = refs[23]
+    step_ref, value_taps, write_taps, read_taps, bias_ref, pld_ref, rate_ref = small[:7]
+    group_ref, channel_ref = small[7:]
+    count = state_output_hbm.shape[0]
+    large = [
+        (ref, w_ref.at[:, k * STATE : (k + 1) * STATE])
+        for k, ref in enumerate((value_hbm, write_hbm, read_hbm, pool_hbm, gate_hbm))
+    ]
+    large.append((state_output_hbm, output_hbm.at[:count]))
+    large.append((pool_output_hbm, output_hbm.at[count:]))
+    fetch(large + list(zip(small_hbm, small)), arrived)
     rank = place_ref[1] * 2 + place_ref[2]
     heads, length = bias_ref.shape
-    for k, ref in enumerate((value_ref, write_ref, read_ref, pool_ref, gate_ref)):
-        w_ref[:, k * STATE : (k + 1) * STATE] = ref[...]
-    shape = (step_ref.shape[1], STATE)
+    shape = (step_ref.shape[0], STATE)
     row, lane = (lax.broadcasted_iota(jnp.int32, shape, k) for k in range(2))
     chosen = jnp.where((lane < heads) & (row == rank * heads + lane), 1.0, 0.0).astype(BF16)
-    w_ref[:, 5 * STATE :] = jnp.dot(
-        step_ref[...], chosen, preferred_element_type=F32
+    w_ref[:, 5 * STATE :] = lax.dot_general(
+        step_ref[...], chosen, (((0,), (0,)), ((), ())), preferred_element_type=F32
     ).astype(BF16)
-    for k, ref in enumerate((value_taps_ref, write_taps_ref, read_taps_ref)):
+    for k, ref in enumerate((value_taps, write_taps, read_taps)):
         taps_ref[0:4, k * STATE : (k + 1) * STATE] = ref[...]
     blocks = length // BLOCK
     pairs = heads * blocks
@@ -78,10 +91,14 @@
         at = slice(b * BLOCK, (b + 1) * BLOCK)
         lanes_ref[b * heads : (b + 1) * heads] = bias_ref[:, at]
         lanes_ref[pairs + b * heads : pairs + (b + 1) * heads] = pld_ref[:, at]
+    rates = rate_ref[...]
+    at_head = lax.broadcasted_iota(jnp.int32, rates.shape, 1)
+    own = [
+        jnp.sum(jnp.where(at_head == rank * heads + h, rates, 0.0), axis=1, keepdims=True)
+        for h in range(2)
+    ]
     odd = lax.broadcasted_iota(jnp.int32, (pairs, BLOCK), 0) % 2 == 1
-    lanes_ref[2 * pairs : 3 * pairs] = jnp.exp(
-        jnp.where(odd, rate_ref[rank * heads + 1], rate_ref[rank * heads])
-    )
+    lanes_ref[2 * pairs : 3 * pairs] = jnp.exp(jnp.where(odd, own[1], own[0]))
     at_lane = lax.broadcasted_iota(jnp.int32, (1, STATE), 1)
     level = (rank * 2 + at_lane // POOL_DIM) % 4
     window = jnp.where(
@@ -96,9 +113,6 @@
         pool_matrix_ref[k * POOL_DIM : (k + 1) * POOL_DIM] = jnp.dot(
             group_ref[k], place, preferred_element_type=F32
         ).astype(BF16)
-    count = state_output_ref.shape[0]
-    output_ref[:count] = state_output_ref[...]
-    output_ref[count:] = pool_output_ref[...]
 
 
 def halves_kernel(prior_ref, next_ref, first_ref, second_ref):
@@ -318,23 +332,19 @@
     out_ref[:, STATE:] = pool_ref[...]
 
 
-def output_kernel(place_ref, rows_ref, own_ref, prior_ref, next_ref, far_a_ref, far_b_ref, keep_ref, send_ref, total_ref):
-    x, core = place_ref[1], place_ref[2]
-    ring = rows_ref.shape[0]
-    half = far_a_ref.shape[0]
-    total = jnp.dot(rows_ref[x], own_ref[...], preferred_element_type=F32)
-    total = total + jnp.dot(rows_ref[(x + ring - 1) % ring], prior_ref[...], preferred_element_type=F32)
-    total = total + jnp.dot(rows_ref[(x + 1) % ring], next_ref[...], preferred_element_type=F32)
-    far = rows_ref[(x + 2) % ring]
-    total = total + jnp.dot(far[:, :half], far_a_ref[...], preferred_element_type=F32)
-    total_ref[...] = total + jnp.dot(far[:, half:], far_b_ref[...], preferred_element_type=F32)
-    count = keep_ref.shape[0]
-    keep_ref[...] = total_ref[pl.ds(pl.multiple_of(core * count, count), count)]
-    send_ref[...] = total_ref[pl.ds(pl.multiple_of((1 - core) * count, count), count)].astype(BF16)
-
-
-def join_kernel(keep_ref, other_ref, out_ref):
-    out_ref[...] = (keep_ref[...] + other_ref[...].astype(F32)).astype(BF16)
+def output_kernel(rows_ref, w_ref, out_ref, weights_ref, arrived):
+    parts = rows_ref.shape[0]
+    incoming = [
+        pltpu.make_async_copy(w_ref.at[k], weights_ref.at[k], arrived.at[k]) for k in range(parts)
+    ]
+    for copy in incoming:
+        copy.start()
+    total = None
+    for k in range(parts):
+        incoming[k].wait()
+        part = jnp.dot(rows_ref[k], weights_ref[k], preferred_element_type=F32)
+        total = part if total is None else total + part
+    out_ref[...] = total.astype(BF16)
 
 
 def limits(mebibytes):
@@ -374,8 +384,16 @@
     return lax.ppermute(array, "core", [(0, 1), (1, 0)])
 
 
-def kernel_call(body, out_shape, *arrays, scratch=(), mebibytes=16):
+class Stored:
+    def __init__(self, array):
+        self.array = pltpu.with_memory_space_constraint(array, pltpu.HBM)
+        self.shape, self.dtype = array.shape, array.dtype
+
+
+def kernel_call(body, out_shape, *arrays, scratch=(), mebibytes=16, stored_outputs=()):
     def spec(array):
+        if isinstance(array, Stored):
+            return pl.BlockSpec(memory_space=pltpu.HBM)
         if array.ndim == 1:
             return pl.BlockSpec(memory_space=pltpu.SMEM)
         return whole(array.shape)
@@ -384,11 +402,14 @@
         body,
         grid=(1,),
         in_specs=[spec(array) for array in arrays],
-        out_specs=jax.tree.map(lambda out: whole(out.shape), out_shape),
+        out_specs=[
+            pl.BlockSpec(memory_space=pltpu.HBM) if k in stored_outputs else whole(out.shape)
+            for k, out in enumerate(out_shape)
+        ],
         out_shape=out_shape,
         scratch_shapes=list(scratch),
         compiler_params=limits(mebibytes),
-    )(*arrays)
+    )(*(array.array if isinstance(array, Stored) else array for array in arrays))
 
 
 def held(shape, dtype):
@@ -426,39 +447,54 @@
 
     place = jnp.stack([sp_rank * length, x, core]).astype(jnp.int32)
     normed, tail = kernel_call(
-        norm_kernel, [held((own_rows, width), BF16), held((HALO, width), BF16)], activations, scale
+        norm_kernel,
+        [held((own_rows, width), BF16), held((HALO, width), BF16)],
+        Stored(activations),
+        Stored(scale),
+        scratch=[
+            pltpu.VMEM((own_rows, width), BF16),
+            pltpu.VMEM((1, width), F32),
+            pltpu.SemaphoreType.DMA((2,)),
+        ],
     )
     prior = around(normed, 1)
     following = around(normed, -1)
     found = rows_before(tail, ring)
     output_rows = state_output_matrix.shape[0] + pooling_output_matrix.shape[0]
-    weights, taps, lanes, pool_matrix, own_output = kernel_call(
-        prepare_kernel,
-        [
-            held((width, 6 * STATE), BF16),
-            held((8, 3 * STATE), F32),
-            held((6 * blocks + 8, STATE), F32),
-            held((STATE, STATE), BF16),
-            held((output_rows, width), BF16),
-        ],
-        place,
-        head_log_decay_rate,
+    small = [
+        step_weight_matrix.T,
+        value_filter_weight,
+        write_filter_weight,
+        read_filter_weight,
+        step_bias_offset,
+        position_log_decay,
+        head_log_decay_rate.reshape(1, -1),
+        pooling_group_matrix,
+        pooling_channel_scale.reshape(1, STATE),
+    ]
+    large = [
         value_weight_matrix,
         write_weight_matrix,
         read_weight_matrix,
         pooling_input_matrix,
         gate_weight_matrix,
-        step_weight_matrix,
-        value_filter_weight,
-        write_filter_weight,
-        read_filter_weight,
-        step_bias_offset,
-        position_log_decay,
-        pooling_group_matrix,
-        pooling_channel_scale.reshape(1, STATE),
         state_output_matrix,
         pooling_output_matrix,
-        mebibytes=24,
+    ]
+    weights, own_output, taps, lanes, pool_matrix = kernel_call(
+        prepare_kernel,
+        [
+            held((width, 6 * STATE), BF16),
+            held((output_rows, width), BF16),
+            held((8, 3 * STATE), F32),
+            held((6 * blocks + 8, STATE), F32),
+            held((STATE, STATE), BF16),
+        ],
+        place,
+        *(Stored(array) for array in large + small),
+        scratch=[pltpu.VMEM(array.shape, array.dtype) for array in small]
+        + [pltpu.SemaphoreType.DMA((len(large) + len(small),))],
+        stored_outputs=(1,),
     )
     other_weights = swapped(weights)
     half = own_rows // 2
@@ -482,6 +518,8 @@
     own_near, send_near = project(normed, prior, following, *found)
     other_near = swapped(send_near)
     own_far, send_far = project(far_first, far_second)
+    own_far, own_output = lax.optimization_barrier((own_far, own_output))
+    output_weights = lax.all_gather(own_output, TP, axis=0)
     other_far = swapped(send_far)
 
     columns, inner = lax.axis_size("sp_0"), lax.axis_size("sp_1")
@@ -512,9 +550,6 @@
         mebibytes=24,
     )
 
-    packed, own_output = lax.optimization_barrier((packed, own_output))
-    prior_output = around(own_output, 1)
-    next_output = around(own_output, -1)
     pieces = lax.all_to_all(packed, "sp_1", 0, 0, tiled=True)
     before, packed = kernel_call(
         row_scan_kernel,
@@ -524,15 +559,9 @@
         mebibytes=8,
     )
     pieces = lax.all_to_all(packed, "sp_0", 0, 0, tiled=True)
-    prior_output, next_output, pieces = lax.optimization_barrier(
-        (prior_output, next_output, pieces)
-    )
-    half = output_rows // 2
-    far = kernel_call(halves_kernel, [held((half, width), BF16)] * 2, prior_output, next_output)
-    far_output = (around(far[0], 1), around(far[1], -1))
-    branches = kernel_call(
+    (branches,) = kernel_call(
         finish_kernel,
-        held((length, 2 * STATE), BF16),
+        [held((length, 2 * STATE), BF16)],
         lax.axis_index("sp_0").astype(jnp.int32).reshape(1),
         pieces,
         before,
@@ -543,22 +572,22 @@
         pool,
         gated_norm_scale.reshape(1, STATE),
     )
+    members = 2 * ring
     branches = lax.all_to_all(
-        branches.reshape(ring, 2 * own_rows, 2 * STATE), "x", 0, 0, tiled=True
-    )
-    keep, send = kernel_call(
+        branches.reshape(members, own_rows, 2 * STATE), TP, 0, 0, tiled=True
+    )
+    (mixed,) = kernel_call(
         output_kernel,
-        [held((own_rows, width), F32), held((own_rows, width), BF16)],
-        place,
+        [held((own_rows, width), BF16)],
         branches,
-        own_output,
-        prior_output,
-        next_output,
-        *far_output,
-        scratch=[pltpu.VMEM((2 * own_rows, width), F32)],
-        mebibytes=24,
-    )
-    return kernel_call(join_kernel, held((own_rows, width), BF16), keep, swapped(send), mebibytes=8)
+        Stored(output_weights),
+        scratch=[
+            pltpu.VMEM((members, 2 * STATE, width), BF16),
+            pltpu.SemaphoreType.DMA((members,)),
+        ],
+        mebibytes=20,
+    )
+    return mixed
 
 
 def solution(mesh):

time: 141 us -> 146 us (1.035)
  the two profiles are of different devices: /device:TPU:7 before, /device:TPU:1 now
where the time goes in v1:
time: 146 us; the launch traced here: 145 us
  blocking collectives  59.5 us (41%)
  starting transfers between devices  31 us (21%)
  Pallas kernels  16.9 us (12%)
  waiting for transfers between devices  16.1 us (11%)
  between operations  13.6 us (9%)
  local copies, waits for them, and re-layouts  8.16 us (6%)
    all_to_all x1, blocking collectives, shards(): pieces = lax.all_to_all(packed, 'sp_1', 0, 0, tiled=True)  21.3 us
    all_to_all x1, blocking collectives, shards(): pieces = lax.all_to_all(packed, 'sp_0', 0, 0, tiled=True)  20.6 us
    all_to_all x1, blocking collectives, shards(): lax.all_to_all(branches.reshape(members, own_rows, 2 * STATE), TP, 0, 0,...  17.6 us
    pallas_call x9, Pallas kernels, kernel_call(): pl.pallas_call(body, grid=(1,), in_specs=[spec(array) for array in arrays...  16.9 us
    ppermute x4, waiting for transfers between devices, around(): lax.ppermute(array, 'x', [(i, (i + away) % ring) for i in range(ring)])  14.7 us
    ppermute x3, starting transfers between devices, swapped(): return lax.ppermute(array, 'core', [(0, 1), (1, 0)])  14.6 us
    ppermute x4, starting transfers between devices, around(): lax.ppermute(array, 'x', [(i, (i + away) % ring) for i in range(ring)])  13.7 us
    unnamed x24, local copies, waits for them, and re-layouts  8.16 us
  transfers between devices with their start and end apart: 12, of which 5 were waited for; matrix products, arithmetic and copies ran while one was open for 0% of the time, Pallas kernels for 6%

profile of v1, /device:TPU:1, one launch (start us, length us, event | category | flops | bytes accessed | tf_op | source)
XLA Modules:
  0.0 145.3 jit_solution(1562525708490400451)
XLA Ops:
  6.5 0.0 all-gather.3.cloned.1.call-start
  6.5 0.1 pad_add_fusion.place_ref
  6.6 3.1 %shard_map.182 = (bf16[2048,768]{1,0:T(8,128)(2,1)S(1)}, bf16[256,2048]{1,0:T(8,128)(2,1)S(1)}, f32[8,384]{1,0:T(8,128)S(1)}, f32[56,128]{1,0:T(8,128)S(1)}, bf16[128,128]{1,0:T(8,128)(2,1)S(1)}) custom-call(s32[3]{0:T(128)S(1)} %pad_add_fusion.place_ref, bf16[2048,128]{1,0:T(8,128)(2,1)} %value_hbm.1, bf16[2048,128]{1,0:T(8,128)(2,1)} %write_hbm.1, ...), custom_call_target="tpu_custom_call" | custom-call | tf_op jit(solution)/shard_map/pallas_call | solution.py:401
  9.7 0.0 copy-start.6
  9.7 1.0 copy-done.6
  10.7 8.7 %collective-permute-start.6 = (bf16[2048,768]{1,0:T(8,128)(2,1)S(1)}, bf16[2048,768]{1,0:T(8,128)(2,1)S(1)}, u32[]{:S(2)}, u32[]{:S(2)}) collective-permute-start(bf16[2048,768]{1,0:T(8,128)(2,1)S(1)} %get-tuple-element.30.refs_7_.refs_2_), channel_id=1, source_target_pairs={{0,1},{1,0},{2,3},{3,2},{4,5},{5,4},{6,7},{7,6},{8,9},{9,8},{10,11... | collective-permute-start | bytes 9437192 | tf_op jit(solution)/shard_map/ppermute | solution.py:384
  19.4 1.3 shard_map.181
  20.7 1.9 %collective-permute-start = (bf16[128,2048]{1,0:T(8,128)(2,1)S(1)}, bf16[128,2048]{1,0:T(8,128)(2,1)S(1)}, u32[]{:S(2)}, u32[]{:S(2)}) collective-permute-start(bf16[128,2048]{1,0:T(8,128)(2,1)S(1)} %get-tuple-element.28.refs_0_), channel_id=1, source_target_pairs={{0,2},{2,4},{4,6},{6,0},{1,3},{3,5},{5,7},{7,1},{8,10},{10,12},{12... | collective-permute-start | bytes 1572872 | tf_op jit(solution)/shard_map/ppermute | solution.py:380
  22.7 4.6 %collective-permute-start.1 = (bf16[128,2048]{1,0:T(8,128)(2,1)S(1)}, bf16[128,2048]{1,0:T(8,128)(2,1)S(1)}, u32[]{:S(2)}, u32[]{:S(2)}) collective-permute-start(bf16[128,2048]{1,0:T(8,128)(2,1)S(1)} %get-tuple-element.28.refs_0_), channel_id=1, source_target_pairs={{0,6},{2,0},{4,2},{6,4},{1,7},{3,1},{5,3},{7,5},{8,14},{10,8},{12,... | collective-permute-start | bytes 1572872 | tf_op jit(solution)/shard_map/ppermute | solution.py:380
  27.2 0.0 copy-start.7
  27.3 0.8 copy-done.7
  28.0 9.3 %collective-permute-done.refs_1_.prior_ref = bf16[128,2048]{1,0:T(8,128)(2,1)S(1)} collective-permute-done((bf16[128,2048]{1,0:T(8,128)(2,1)S(1)}, bf16[128,2048]{1,0:T(8,128)(2,1)S(1)}, u32[]{:S(2)}, u32[]{:S(2)}) %collective-permute-start) | collective-permute-done | bytes 524320 | tf_op jit(solution)/shard_map/ppermute | solution.py:380
  37.3 0.0 copy-start.2
  37.3 0.9 collective-permute-done.1.refs_2_.next_ref
  38.2 0.0 copy-start.4
  38.3 1.9 %collective-permute-start.7 = (bf16[64,2048]{1,0:T(8,128)(2,1)S(1)}, bf16[64,2048]{1,0:T(8,128)(2,1)S(1)}, u32[]{:S(2)}, u32[]{:S(2)}) collective-permute-start(bf16[64,2048]{1,0:T(8,128)(2,1)S(1)} %get-tuple-element.32), channel_id=1, source_target_pairs={{0,2},{2,4},{4,6},{6,0},{1,3},{3,5},{5,7},{7,1},{8,10},{10,12},{12... | collective-permute-start | bytes 786440 | tf_op jit(solution)/shard_map/ppermute | solution.py:380
  40.2 5.3 %collective-permute-start.8 = (bf16[64,2048]{1,0:T(8,128)(2,1)S(1)}, bf16[64,2048]{1,0:T(8,128)(2,1)S(1)}, u32[]{:S(2)}, u32[]{:S(2)}) collective-permute-start(bf16[64,2048]{1,0:T(8,128)(2,1)S(1)} %get-tuple-element.33), channel_id=1, source_target_pairs={{0,6},{2,0},{4,2},{6,4},{1,7},{3,1},{5,3},{7,5},{8,14},{10,8},{12,... | collective-permute-start | bytes 786440 | tf_op jit(solution)/shard_map/ppermute | solution.py:380
  45.5 3.6 %collective-permute-done.7.refs_0_ = bf16[64,2048]{1,0:T(8,128)(2,1)S(1)} collective-permute-done((bf16[64,2048]{1,0:T(8,128)(2,1)S(1)}, bf16[64,2048]{1,0:T(8,128)(2,1)S(1)}, u32[]{:S(2)}, u32[]{:S(2)}) %collective-permute-start.7) | collective-permute-done | bytes 262176 | tf_op jit(solution)/shard_map/ppermute | solution.py:380
  49.1 0.0 copy-done.2
  49.1 0.9 collective-permute-done.8.refs_1_
  50.0 0.0 copy-done.4
  50.0 0.0 collective-permute-done.6.refs_8_.refs_3_
  50.0 0.0 copy-start
  50.0 1.0 shard_map.185
  51.0 0.7 copy-done
  51.7 0.0 copy-start.10
  51.7 0.7 copy-done.10
  52.3 0.0 all-gather.3.cloned.1.call-update
  52.4 0.7 collective-permute-start.2
  53.0 0.7 collective-permute-start.3
  53.7 0.7 collective-permute-start.4
  54.4 0.7 collective-permute-start.5
  55.1 0.0 collective-permute-done.2.refs_3_
  55.1 0.0 collective-permute-done.3.refs_4_
  55.1 0.0 collective-permute-done.4.refs_5_
  55.1 0.0 collective-permute-done.5.refs_6_
  55.1 0.0 copy-start.1
  55.1 1.9 %copy-done.1 = bf16[2048,768]{1,0:T(8,128)(2,1)S(1)} copy-done((bf16[2048,768]{1,0:T(8,128)(2,1)S(1)}, bf16[2048,768]{1,0:T(8,128)(2,1)}, u32[]{:S(2)}) %copy-start.1) | copy-done | bytes 3145752
  57.0 0.0 copy-start.3
  57.0 1.0 copy-done.3
  58.0 0.0 copy-start.5
  58.0 1.0 copy-done.5
  59.1 0.0 copy-start.8
  59.1 1.0 copy-done.8
  60.1 0.0 copy-start.11
  60.1 2.7 %shard_map.183 = (bf16[400,768]{1,0:T(8,128)(2,1)S(1)}, bf16[400,768]{1,0:T(8,128)(2,1)S(1)}) custom-call(bf16[128,2048]{1,0:T(8,128)(2,1)S(1)} %copy-done.8, bf16[128,2048]{1,0:T(8,128)(2,1)S(1)} %copy-done.3, bf16[128,2048]{1,0:T(8,128)(2,1)S(1)} %copy-done.5, bf16[16,2048]{1,0:T(8,128)(2,1)S(1)} %collective-permute-done.2.refs_3_, ...), custom_call_target="tpu_custom_call" | custom-call | tf_op jit(solution)/shard_map/pallas_call | solution.py:401
  62.8 0.0 copy-start.9
  62.8 3.9 %collective-permute-start.9 = (bf16[400,768]{1,0:T(8,128)(2,1)S(1)}, bf16[400,768]{1,0:T(8,128)(2,1)S(1)}, u32[]{:S(2)}, u32[]{:S(2)}) collective-permute-start(bf16[400,768]{1,0:T(8,128)(2,1)S(1)} %get-tuple-element.37), channel_id=1, source_target_pairs={{0,1},{1,0},{2,3},{3,2},{4,5},{5,4},{6,7},{7,6},{8,9},{9,8},{10,11... | collective-permute-start | bytes 1843208 | tf_op jit(solution)/shard_map/ppermute | solution.py:384
  66.8 0.0 copy-done.11
  66.8 1.9 %collective-permute-start.10 = (bf16[128,768]{1,0:T(8,128)(2,1)S(1)}, bf16[128,768]{1,0:T(8,128)(2,1)S(1)}, u32[]{:S(2)}, u32[]{:S(2)}) collective-permute-start(bf16[128,768]{1,0:T(8,128)(2,1)S(1)} %copy-done.11), channel_id=1, source_target_pairs={{0,1},{1,0},{2,3},{3,2},{4,5},{5,4},{6,7},{7,6},{8,9},{9,8},{10,11... | collective-permute-start | bytes 589832 | tf_op jit(solution)/shard_map/ppermute | solution.py:384
  68.7 1.4 collective-permute-done.10.other_far_ref
  70.1 0.0 collective-permute-done.9.other_near_ref
  70.1 3.7 %shard_map.186 = (f32[1024,128]{1,0:T(8,128)S(1)}, bf16[1024,128]{1,0:T(8,128)(2,1)S(1)}, f32[1024,128]{1,0:T(8,128)S(1)}, f32[1024,128]{1,0:T(8,128)S(1)}, bf16...) custom-call(s32[3]{0:T(128)S(1)} %pad_add_fusion.place_ref, ...), custom_call_target="tpu_custom_call" | custom-call | tf_op jit(solution)/shard_map/pallas_call | solution.py:401
  73.8 21.3 %all_to_all.15.pieces_ref = bf16[8,144,128]{2,1,0:T(8,128)(2,1)S(1)} all-to-all(bf16[8,144,128]{2,1,0:T(8,128)(2,1)S(1)} %get-tuple-element.42), channel_id=1, replica_groups=mesh['sp_0'=8,'sp_1'=8,'x'=4,'core'=2] {'sp_1'}, dimensions={0} | all-to-all | bytes 589824 | tf_op jit(solution)/shard_map/all_to_all | solution.py:553
  95.1 0.1 shard_map.187
  95.2 20.6 %all_to_all.16.pieces_ref = bf16[8,144,128]{2,1,0:T(8,128)(2,1)S(1)} all-to-all(bf16[8,144,128]{2,1,0:T(8,128)(2,1)S(1)} %get-tuple-element.43), channel_id=1, replica_groups=mesh['sp_0'=8,'sp_1'=8,'x'=4,'core'=2] {'sp_0'}, dimensions={0} | all-to-all | bytes 589824 | tf_op jit(solution)/shard_map/all_to_all | solution.py:561
  115.8 0.0 copy-done.9
  115.8 0.5 shard_map.188
  116.3 17.6 %all_to_all.17.rows_ref = bf16[8,128,256]{2,1,0:T(8,128)(2,1)S(1)} all-to-all(bf16[8,128,256]{2,1,0:T(8,128)(2,1)S(1)} %bitcast.12), channel_id=1, replica_groups=mesh['sp_0'=8,'sp_1'=8,'x'=4,'core'=2] {'x','core'}, dimensions={0} | all-to-all | bytes 1048576 | tf_op jit(solution)/shard_map/all_to_all | solution.py:576
  133.9 0.0 all-gather.3.cloned.1.call-done
  133.9 4.6 %shard_map.189 = bf16[128,2048]{1,0:T(8,128)(2,1)} custom-call(bf16[8,128,256]{2,1,0:T(8,128)(2,1)S(1)} %all_to_all.17.rows_ref, bf16[8,256,2048]{2,1,0:T(8,128)(2,1)} %bitcast.14), custom_call_target="tpu_custom_call" | custom-call | tf_op jit(solution)/shard_map/pallas_call | solution.py:401
  (1 shorter events, 0.0 us)
Async XLA Ops:
  6.5 127.3 %all-gather.3.cloned.1.call-start = ((), (), s32[]{:S(2)}) async-start(), calls=%async_computation.3 | async-start | bytes 9437184 | tf_op jit(solution)/shard_map/all_gather | solution.py:522
  9.7 1.0 copy-start.6
  10.7 39.3 %collective-permute-start.6 = (bf16[2048,768]{1,0:T(8,128)(2,1)S(1)}, bf16[2048,768]{1,0:T(8,128)(2,1)S(1)}, u32[]{:S(2)}, u32[]{:S(2)}) collective-permute-start(bf16[2048,768]{1,0:T(8,128)(2,1)S(1)} %get-tuple-element.30.refs_7_.refs_2_), channel_id=1, source_target_pairs={{0,1},{1,0},{2,3},{3,2},{4,5},{5,4},{6,7},{7,6},{8,9},{9,8},{10,11... | collective-permute-start | bytes 9437192 | tf_op jit(solution)/shard_map/ppermute | solution.py:384
  20.7 16.6 %collective-permute-start = (bf16[128,2048]{1,0:T(8,128)(2,1)S(1)}, bf16[128,2048]{1,0:T(8,128)(2,1)S(1)}, u32[]{:S(2)}, u32[]{:S(2)}) collective-permute-start(bf16[128,2048]{1,0:T(8,128)(2,1)S(1)} %get-tuple-element.28.refs_0_), channel_id=1, source_target_pairs={{0,2},{2,4},{4,6},{6,0},{1,3},{3,5},{5,7},{7,1},{8,10},{10,12},{12... | collective-permute-start | bytes 1572872 | tf_op jit(solution)/shard_map/ppermute | solution.py:380
  22.7 15.5 %collective-permute-start.1 = (bf16[128,2048]{1,0:T(8,128)(2,1)S(1)}, bf16[128,2048]{1,0:T(8,128)(2,1)S(1)}, u32[]{:S(2)}, u32[]{:S(2)}) collective-permute-start(bf16[128,2048]{1,0:T(8,128)(2,1)S(1)} %get-tuple-element.28.refs_0_), channel_id=1, source_target_pairs={{0,6},{2,0},{4,2},{6,4},{1,7},{3,1},{5,3},{7,5},{8,14},{10,8},{12,... | collective-permute-start | bytes 1572872 | tf_op jit(solution)/shard_map/ppermute | solution.py:380
  27.2 0.8 copy-start.7
  37.3 11.8 %copy-start.2 = (bf16[128,2048]{1,0:T(8,128)(2,1)}, bf16[128,2048]{1,0:T(8,128)(2,1)S(1)}, u32[]{:S(2)}) copy-start(bf16[128,2048]{1,0:T(8,128)(2,1)S(1)} %collective-permute-done.refs_1_.prior_ref) | copy-start | bytes 1572868
  38.2 11.8 %copy-start.4 = (bf16[128,2048]{1,0:T(8,128)(2,1)}, bf16[128,2048]{1,0:T(8,128)(2,1)S(1)}, u32[]{:S(2)}) copy-start(bf16[128,2048]{1,0:T(8,128)(2,1)S(1)} %collective-permute-done.1.refs_2_.next_ref) | copy-start | bytes 1572868
  38.3 10.8 %collective-permute-start.7 = (bf16[64,2048]{1,0:T(8,128)(2,1)S(1)}, bf16[64,2048]{1,0:T(8,128)(2,1)S(1)}, u32[]{:S(2)}, u32[]{:S(2)}) collective-permute-start(bf16[64,2048]{1,0:T(8,128)(2,1)S(1)} %get-tuple-element.32), channel_id=1, source_target_pairs={{0,2},{2,4},{4,6},{6,0},{1,3},{3,5},{5,7},{7,1},{8,10},{10,12},{12... | collective-permute-start | bytes 786440 | tf_op jit(solution)/shard_map/ppermute | solution.py:380
  40.2 9.8 %collective-permute-start.8 = (bf16[64,2048]{1,0:T(8,128)(2,1)S(1)}, bf16[64,2048]{1,0:T(8,128)(2,1)S(1)}, u32[]{:S(2)}, u32[]{:S(2)}) collective-permute-start(bf16[64,2048]{1,0:T(8,128)(2,1)S(1)} %get-tuple-element.33), channel_id=1, source_target_pairs={{0,6},{2,0},{4,2},{6,4},{1,7},{3,1},{5,3},{7,5},{8,14},{10,8},{12,... | collective-permute-start | bytes 786440 | tf_op jit(solution)/shard_map/ppermute | solution.py:380
  50.0 1.7 %copy-start = (bf16[2048,768]{1,0:T(8,128)(2,1)}, bf16[2048,768]{1,0:T(8,128)(2,1)S(1)}, u32[]{:S(2)}) copy-start(bf16[2048,768]{1,0:T(8,128)(2,1)S(1)} %collective-permute-done.6.refs_8_.refs_3_) | copy-start | bytes 9437188
  51.7 0.7 copy-start.10
  52.4 2.7 %collective-permute-start.2 = (bf16[16,2048]{1,0:T(8,128)(2,1)S(1)}, bf16[16,2048]{1,0:T(8,128)(2,1)S(1)}, u32[]{:S(2)}, u32[]{:S(2)}) collective-permute-start(bf16[16,2048]{1,0:T(8,128)(2,1)S(1)} %get-tuple-element.29), channel_id=1, source_target_pairs={{7,8},{15,16},{23,24},{31,32},{39,40},{47,48},{55,56},{63,64},{71,... | collective-permute-start | bytes 196616 | tf_op jit(solution)/shard_map/ppermute | solution.py:369
  53.0 2.0 %collective-permute-start.3 = (bf16[16,2048]{1,0:T(8,128)(2,1)S(1)}, bf16[16,2048]{1,0:T(8,128)(2,1)S(1)}, u32[]{:S(2)}, u32[]{:S(2)}) collective-permute-start(bf16[16,2048]{1,0:T(8,128)(2,1)S(1)} %get-tuple-element.29), channel_id=1, source_target_pairs={{7,10},{15,18},{23,26},{31,34},{39,42},{47,50},{55,58},{63,66},{71... | collective-permute-start | bytes 196616 | tf_op jit(solution)/shard_map/ppermute | solution.py:369
  53.7 1.4 collective-permute-start.4
  54.4 0.7 collective-permute-start.5
  55.1 1.9 %copy-start.1 = (bf16[2048,768]{1,0:T(8,128)(2,1)S(1)}, bf16[2048,768]{1,0:T(8,128)(2,1)}, u32[]{:S(2)}) copy-start(bf16[2048,768]{1,0:T(8,128)(2,1)} %copy-done) | copy-start | bytes 9437188
  57.0 1.0 copy-start.3
  58.0 1.0 copy-start.5
  59.1 1.0 copy-start.8
  60.1 6.6 %copy-start.11 = (bf16[128,768]{1,0:T(8,128)(2,1)S(1)}, bf16[128,768]{1,0:T(8,128)(2,1)}, u32[]{:S(2)}) copy-start(bf16[128,768]{1,0:T(8,128)(2,1)} %copy-done.10) | copy-start | bytes 589828
  62.8 53.0 %copy-start.9 = (f32[128]{0:T(128)S(1)}, f32[128]{0:T(128)}, u32[]{:S(2)}) copy-start(f32[128]{0:T(128)} %param.33) | copy-start | bytes 1540
  62.8 7.3 %collective-permute-start.9 = (bf16[400,768]{1,0:T(8,128)(2,1)S(1)}, bf16[400,768]{1,0:T(8,128)(2,1)S(1)}, u32[]{:S(2)}, u32[]{:S(2)}) collective-permute-start(bf16[400,768]{1,0:T(8,128)(2,1)S(1)} %get-tuple-element.37), channel_id=1, source_target_pairs={{0,1},{1,0},{2,3},{3,2},{4,5},{5,4},{6,7},{7,6},{8,9},{9,8},{10,11... | collective-permute-start | bytes 1843208 | tf_op jit(solution)/shard_map/ppermute | solution.py:384
  66.8 3.3 %collective-permute-start.10 = (bf16[128,768]{1,0:T(8,128)(2,1)S(1)}, bf16[128,768]{1,0:T(8,128)(2,1)S(1)}, u32[]{:S(2)}, u32[]{:S(2)}) collective-permute-start(bf16[128,768]{1,0:T(8,128)(2,1)S(1)} %copy-done.11), channel_id=1, source_target_pairs={{0,1},{1,0},{2,3},{3,2},{4,5},{5,4},{6,7},{7,6},{8,9},{9,8},{10,11... | collective-permute-start | bytes 589832 | tf_op jit(solution)/shard_map/ppermute | solution.py:384
Sparse Core Ops, SparseCore 0:
  52.5 56.6 all-gather.2

commit v2 on v1

--- a/solution.py
+++ b/solution.py
@@ -59,7 +59,7 @@
     pool_output_hbm,
     *refs,
 ):
-    small_hbm, (w_ref, output_hbm, taps_ref, lanes_ref, pool_matrix_ref), small = (
+    small_hbm, (w_ref, output_ref, taps_ref, lanes_ref, pool_matrix_ref), small = (
         refs[:9],
         refs[9:14],
         refs[14:23],
@@ -72,8 +72,8 @@
         (ref, w_ref.at[:, k * STATE : (k + 1) * STATE])
         for k, ref in enumerate((value_hbm, write_hbm, read_hbm, pool_hbm, gate_hbm))
     ]
-    large.append((state_output_hbm, output_hbm.at[:count]))
-    large.append((pool_output_hbm, output_hbm.at[count:]))
+    large.append((state_output_hbm, output_ref.at[:count]))
+    large.append((pool_output_hbm, output_ref.at[count:]))
     fetch(large + list(zip(small_hbm, small)), arrived)
     rank = place_ref[1] * 2 + place_ref[2]
     heads, length = bias_ref.shape
@@ -390,7 +390,7 @@
         self.shape, self.dtype = array.shape, array.dtype
 
 
-def kernel_call(body, out_shape, *arrays, scratch=(), mebibytes=16, stored_outputs=()):
+def kernel_call(body, out_shape, *arrays, scratch=(), mebibytes=16):
     def spec(array):
         if isinstance(array, Stored):
             return pl.BlockSpec(memory_space=pltpu.HBM)
@@ -402,10 +402,7 @@
         body,
         grid=(1,),
         in_specs=[spec(array) for array in arrays],
-        out_specs=[
-            pl.BlockSpec(memory_space=pltpu.HBM) if k in stored_outputs else whole(out.shape)
-            for k, out in enumerate(out_shape)
-        ],
+        out_specs=[whole(out.shape) for out in out_shape],
         out_shape=out_shape,
         scratch_shapes=list(scratch),
         compiler_params=limits(mebibytes),
@@ -494,7 +491,6 @@
         *(Stored(array) for array in large + small),
         scratch=[pltpu.VMEM(array.shape, array.dtype) for array in small]
         + [pltpu.SemaphoreType.DMA((len(large) + len(small),))],
-        stored_outputs=(1,),
     )
     other_weights = swapped(weights)
     half = own_rows // 2

time: 146 us -> 146 us (level)
  no operation moved by 1% of the time
where the time goes in v2:
time: 146 us; the launch traced here: 145 us
  blocking collectives  59.5 us (41%)
  starting transfers between devices  31 us (21%)
  Pallas kernels  16.9 us (12%)
  waiting for transfers between devices  16.1 us (11%)
  between operations  13.6 us (9%)
  local copies, waits for them, and re-layouts  8.16 us (6%)
    all_to_all x1, blocking collectives, shards(): pieces = lax.all_to_all(packed, 'sp_1', 0, 0, tiled=True)  21.3 us
    all_to_all x1, blocking collectives, shards(): pieces = lax.all_to_all(packed, 'sp_0', 0, 0, tiled=True)  20.6 us
    all_to_all x1, blocking collectives, shards(): lax.all_to_all(branches.reshape(members, own_rows, 2 * STATE), TP, 0, 0,...  17.6 us
    pallas_call x9, Pallas kernels, kernel_call(): pl.pallas_call(body, grid=(1,), in_specs=[spec(array) for array in arrays...  16.9 us
    ppermute x4, waiting for transfers between devices, around(): lax.ppermute(array, 'x', [(i, (i + away) % ring) for i in range(ring)])  14.7 us
    ppermute x3, starting transfers between devices, swapped(): return lax.ppermute(array, 'core', [(0, 1), (1, 0)])  14.6 us
    ppermute x4, starting transfers between devices, around(): lax.ppermute(array, 'x', [(i, (i + away) % ring) for i in range(ring)])  13.7 us
    unnamed x24, local copies, waits for them, and re-layouts  8.16 us
  transfers between devices with their start and end apart: 12, of which 5 were waited for; matrix products, arithmetic and copies ran while one was open for 0% of the time, Pallas kernels for 6%

profile of v2, /device:TPU:1, one launch (start us, length us, event | category | flops | bytes accessed | tf_op | source)
XLA Modules:
  0.0 145.3 jit_solution(1562525708490400451)
XLA Ops:
  6.5 0.0 all-gather.3.cloned.1.call-start
  6.5 0.1 pad_add_fusion.place_ref
  6.6 3.1 %shard_map.182 = (bf16[2048,768]{1,0:T(8,128)(2,1)S(1)}, bf16[256,2048]{1,0:T(8,128)(2,1)S(1)}, f32[8,384]{1,0:T(8,128)S(1)}, f32[56,128]{1,0:T(8,128)S(1)}, bf16[128,128]{1,0:T(8,128)(2,1)S(1)}) custom-call(s32[3]{0:T(128)S(1)} %pad_add_fusion.place_ref, bf16[2048,128]{1,0:T(8,128)(2,1)} %value_hbm.1, bf16[2048,128]{1,0:T(8,128)(2,1)} %write_hbm.1, ...), custom_call_target="tpu_custom_call" | custom-call | tf_op jit(solution)/shard_map/pallas_call | solution.py:401
  9.7 0.0 copy-start.6
  9.7 1.0 copy-done.6
  10.7 8.7 %collective-permute-start.6 = (bf16[2048,768]{1,0:T(8,128)(2,1)S(1)}, bf16[2048,768]{1,0:T(8,128)(2,1)S(1)}, u32[]{:S(2)}, u32[]{:S(2)}) collective-permute-start(bf16[2048,768]{1,0:T(8,128)(2,1)S(1)} %get-tuple-element.30.refs_7_.refs_2_), channel_id=1, source_target_pairs={{0,1},{1,0},{2,3},{3,2},{4,5},{5,4},{6,7},{7,6},{8,9},{9,8},{10,11... | collective-permute-start | bytes 9437192 | tf_op jit(solution)/shard_map/ppermute | solution.py:384
  19.4 1.3 shard_map.181
  20.7 1.9 %collective-permute-start = (bf16[128,2048]{1,0:T(8,128)(2,1)S(1)}, bf16[128,2048]{1,0:T(8,128)(2,1)S(1)}, u32[]{:S(2)}, u32[]{:S(2)}) collective-permute-start(bf16[128,2048]{1,0:T(8,128)(2,1)S(1)} %get-tuple-element.28.refs_0_), channel_id=1, source_target_pairs={{0,2},{2,4},{4,6},{6,0},{1,3},{3,5},{5,7},{7,1},{8,10},{10,12},{12... | collective-permute-start | bytes 1572872 | tf_op jit(solution)/shard_map/ppermute | solution.py:380
  22.7 4.6 %collective-permute-start.1 = (bf16[128,2048]{1,0:T(8,128)(2,1)S(1)}, bf16[128,2048]{1,0:T(8,128)(2,1)S(1)}, u32[]{:S(2)}, u32[]{:S(2)}) collective-permute-start(bf16[128,2048]{1,0:T(8,128)(2,1)S(1)} %get-tuple-element.28.refs_0_), channel_id=1, source_target_pairs={{0,6},{2,0},{4,2},{6,4},{1,7},{3,1},{5,3},{7,5},{8,14},{10,8},{12,... | collective-permute-start | bytes 1572872 | tf_op jit(solution)/shard_map/ppermute | solution.py:380
  27.2 0.0 copy-start.7
  27.3 0.8 copy-done.7
  28.0 9.3 %collective-permute-done.refs_1_.prior_ref = bf16[128,2048]{1,0:T(8,128)(2,1)S(1)} collective-permute-done((bf16[128,2048]{1,0:T(8,128)(2,1)S(1)}, bf16[128,2048]{1,0:T(8,128)(2,1)S(1)}, u32[]{:S(2)}, u32[]{:S(2)}) %collective-permute-start) | collective-permute-done | bytes 524320 | tf_op jit(solution)/shard_map/ppermute | solution.py:380
  37.3 0.0 copy-start.2
  37.3 0.9 collective-permute-done.1.refs_2_.next_ref
  38.2 0.0 copy-start.4
  38.3 1.9 %collective-permute-start.7 = (bf16[64,2048]{1,0:T(8,128)(2,1)S(1)}, bf16[64,2048]{1,0:T(8,128)(2,1)S(1)}, u32[]{:S(2)}, u32[]{:S(2)}) collective-permute-start(bf16[64,2048]{1,0:T(8,128)(2,1)S(1)} %get-tuple-element.32), channel_id=1, source_target_pairs={{0,2},{2,4},{4,6},{6,0},{1,3},{3,5},{5,7},{7,1},{8,10},{10,12},{12... | collective-permute-start | bytes 786440 | tf_op jit(solution)/shard_map/ppermute | solution.py:380
  40.2 5.3 %collective-permute-start.8 = (bf16[64,2048]{1,0:T(8,128)(2,1)S(1)}, bf16[64,2048]{1,0:T(8,128)(2,1)S(1)}, u32[]{:S(2)}, u32[]{:S(2)}) collective-permute-start(bf16[64,2048]{1,0:T(8,128)(2,1)S(1)} %get-tuple-element.33), channel_id=1, source_target_pairs={{0,6},{2,0},{4,2},{6,4},{1,7},{3,1},{5,3},{7,5},{8,14},{10,8},{12,... | collective-permute-start | bytes 786440 | tf_op jit(solution)/shard_map/ppermute | solution.py:380
  45.5 3.6 %collective-permute-done.7.refs_0_ = bf16[64,2048]{1,0:T(8,128)(2,1)S(1)} collective-permute-done((bf16[64,2048]{1,0:T(8,128)(2,1)S(1)}, bf16[64,2048]{1,0:T(8,128)(2,1)S(1)}, u32[]{:S(2)}, u32[]{:S(2)}) %collective-permute-start.7) | collective-permute-done | bytes 262176 | tf_op jit(solution)/shard_map/ppermute | solution.py:380
  49.1 0.0 copy-done.2
  49.1 0.9 collective-permute-done.8.refs_1_
  50.0 0.0 copy-done.4
  50.0 0.0 collective-permute-done.6.refs_8_.refs_3_
  50.0 0.0 copy-start
  50.0 1.0 shard_map.185
  51.0 0.7 copy-done
  51.7 0.0 copy-start.10
  51.7 0.7 copy-done.10
  52.3 0.0 all-gather.3.cloned.1.call-update
  52.4 0.7 collective-permute-start.2
  53.0 0.7 collective-permute-start.3
  53.7 0.7 collective-permute-start.4
  54.4 0.7 collective-permute-start.5
  55.1 0.0 collective-permute-done.2.refs_3_
  55.1 0.0 collective-permute-done.3.refs_4_
  55.1 0.0 collective-permute-done.4.refs_5_
  55.1 0.0 collective-permute-done.5.refs_6_
  55.1 0.0 copy-start.1
  55.1 1.9 %copy-done.1 = bf16[2048,768]{1,0:T(8,128)(2,1)S(1)} copy-done((bf16[2048,768]{1,0:T(8,128)(2,1)S(1)}, bf16[2048,768]{1,0:T(8,128)(2,1)}, u32[]{:S(2)}) %copy-start.1) | copy-done | bytes 3145752
  57.0 0.0 copy-start.3
  57.0 1.0 copy-done.3
  58.0 0.0 copy-start.5
  58.0 1.0 copy-done.5
  59.1 0.0 copy-start.8
  59.1 1.0 copy-done.8
  60.1 0.0 copy-start.11
  60.1 2.7 %shard_map.183 = (bf16[400,768]{1,0:T(8,128)(2,1)S(1)}, bf16[400,768]{1,0:T(8,128)(2,1)S(1)}) custom-call(bf16[128,2048]{1,0:T(8,128)(2,1)S(1)} %copy-done.8, bf16[128,2048]{1,0:T(8,128)(2,1)S(1)} %copy-done.3, bf16[128,2048]{1,0:T(8,128)(2,1)S(1)} %copy-done.5, bf16[16,2048]{1,0:T(8,128)(2,1)S(1)} %collective-permute-done.2.refs_3_, ...), custom_call_target="tpu_custom_call" | custom-call | tf_op jit(solution)/shard_map/pallas_call | solution.py:401
  62.8 0.0 copy-start.9
  62.8 3.9 %collective-permute-start.9 = (bf16[400,768]{1,0:T(8,128)(2,1)S(1)}, bf16[400,768]{1,0:T(8,128)(2,1)S(1)}, u32[]{:S(2)}, u32[]{:S(2)}) collective-permute-start(bf16[400,768]{1,0:T(8,128)(2,1)S(1)} %get-tuple-element.37), channel_id=1, source_target_pairs={{0,1},{1,0},{2,3},{3,2},{4,5},{5,4},{6,7},{7,6},{8,9},{9,8},{10,11... | collective-permute-start | bytes 1843208 | tf_op jit(solution)/shard_map/ppermute | solution.py:384
  66.8 0.0 copy-done.11
  66.8 1.9 %collective-permute-start.10 = (bf16[128,768]{1,0:T(8,128)(2,1)S(1)}, bf16[128,768]{1,0:T(8,128)(2,1)S(1)}, u32[]{:S(2)}, u32[]{:S(2)}) collective-permute-start(bf16[128,768]{1,0:T(8,128)(2,1)S(1)} %copy-done.11), channel_id=1, source_target_pairs={{0,1},{1,0},{2,3},{3,2},{4,5},{5,4},{6,7},{7,6},{8,9},{9,8},{10,11... | collective-permute-start | bytes 589832 | tf_op jit(solution)/shard_map/ppermute | solution.py:384
  68.7 1.4 collective-permute-done.10.other_far_ref
  70.1 0.0 collective-permute-done.9.other_near_ref
  70.1 3.7 %shard_map.186 = (f32[1024,128]{1,0:T(8,128)S(1)}, bf16[1024,128]{1,0:T(8,128)(2,1)S(1)}, f32[1024,128]{1,0:T(8,128)S(1)}, f32[1024,128]{1,0:T(8,128)S(1)}, bf16...) custom-call(s32[3]{0:T(128)S(1)} %pad_add_fusion.place_ref, ...), custom_call_target="tpu_custom_call" | custom-call | tf_op jit(solution)/shard_map/pallas_call | solution.py:401
  73.8 21.3 %all_to_all.15.pieces_ref = bf16[8,144,128]{2,1,0:T(8,128)(2,1)S(1)} all-to-all(bf16[8,144,128]{2,1,0:T(8,128)(2,1)S(1)} %get-tuple-element.42), channel_id=1, replica_groups=mesh['sp_0'=8,'sp_1'=8,'x'=4,'core'=2] {'sp_1'}, dimensions={0} | all-to-all | bytes 589824 | tf_op jit(solution)/shard_map/all_to_all | solution.py:549
  95.1 0.1 shard_map.187
  95.2 20.6 %all_to_all.16.pieces_ref = bf16[8,144,128]{2,1,0:T(8,128)(2,1)S(1)} all-to-all(bf16[8,144,128]{2,1,0:T(8,128)(2,1)S(1)} %get-tuple-element.43), channel_id=1, replica_groups=mesh['sp_0'=8,'sp_1'=8,'x'=4,'core'=2] {'sp_0'}, dimensions={0} | all-to-all | bytes 589824 | tf_op jit(solution)/shard_map/all_to_all | solution.py:557
  115.8 0.0 copy-done.9
  115.8 0.5 shard_map.188
  116.3 17.6 %all_to_all.17.rows_ref = bf16[8,128,256]{2,1,0:T(8,128)(2,1)S(1)} all-to-all(bf16[8,128,256]{2,1,0:T(8,128)(2,1)S(1)} %bitcast.12), channel_id=1, replica_groups=mesh['sp_0'=8,'sp_1'=8,'x'=4,'core'=2] {'x','core'}, dimensions={0} | all-to-all | bytes 1048576 | tf_op jit(solution)/shard_map/all_to_all | solution.py:572
  133.9 0.0 all-gather.3.cloned.1.call-done
  133.9 4.6 %shard_map.189 = bf16[128,2048]{1,0:T(8,128)(2,1)} custom-call(bf16[8,128,256]{2,1,0:T(8,128)(2,1)S(1)} %all_to_all.17.rows_ref, bf16[8,256,2048]{2,1,0:T(8,128)(2,1)} %bitcast.14), custom_call_target="tpu_custom_call" | custom-call | tf_op jit(solution)/shard_map/pallas_call | solution.py:401
  (1 shorter events, 0.0 us)
Async XLA Ops:
  6.5 127.3 %all-gather.3.cloned.1.call-start = ((), (), s32[]{:S(2)}) async-start(), calls=%async_computation.3 | async-start | bytes 9437184 | tf_op jit(solution)/shard_map/all_gather | solution.py:518
  9.7 1.0 copy-start.6
  10.7 39.3 %collective-permute-start.6 = (bf16[2048,768]{1,0:T(8,128)(2,1)S(1)}, bf16[2048,768]{1,0:T(8,128)(2,1)S(1)}, u32[]{:S(2)}, u32[]{:S(2)}) collective-permute-start(bf16[2048,768]{1,0:T(8,128)(2,1)S(1)} %get-tuple-element.30.refs_7_.refs_2_), channel_id=1, source_target_pairs={{0,1},{1,0},{2,3},{3,2},{4,5},{5,4},{6,7},{7,6},{8,9},{9,8},{10,11... | collective-permute-start | bytes 9437192 | tf_op jit(solution)/shard_map/ppermute | solution.py:384
  20.7 16.6 %collective-permute-start = (bf16[128,2048]{1,0:T(8,128)(2,1)S(1)}, bf16[128,2048]{1,0:T(8,128)(2,1)S(1)}, u32[]{:S(2)}, u32[]{:S(2)}) collective-permute-start(bf16[128,2048]{1,0:T(8,128)(2,1)S(1)} %get-tuple-element.28.refs_0_), channel_id=1, source_target_pairs={{0,2},{2,4},{4,6},{6,0},{1,3},{3,5},{5,7},{7,1},{8,10},{10,12},{12... | collective-permute-start | bytes 1572872 | tf_op jit(solution)/shard_map/ppermute | solution.py:380
  22.7 15.5 %collective-permute-start.1 = (bf16[128,2048]{1,0:T(8,128)(2,1)S(1)}, bf16[128,2048]{1,0:T(8,128)(2,1)S(1)}, u32[]{:S(2)}, u32[]{:S(2)}) collective-permute-start(bf16[128,2048]{1,0:T(8,128)(2,1)S(1)} %get-tuple-element.28.refs_0_), channel_id=1, source_target_pairs={{0,6},{2,0},{4,2},{6,4},{1,7},{3,1},{5,3},{7,5},{8,14},{10,8},{12,... | collective-permute-start | bytes 1572872 | tf_op jit(solution)/shard_map/ppermute | solution.py:380
  27.2 0.8 copy-start.7
  37.3 11.8 %copy-start.2 = (bf16[128,2048]{1,0:T(8,128)(2,1)}, bf16[128,2048]{1,0:T(8,128)(2,1)S(1)}, u32[]{:S(2)}) copy-start(bf16[128,2048]{1,0:T(8,128)(2,1)S(1)} %collective-permute-done.refs_1_.prior_ref) | copy-start | bytes 1572868
  38.2 11.8 %copy-start.4 = (bf16[128,2048]{1,0:T(8,128)(2,1)}, bf16[128,2048]{1,0:T(8,128)(2,1)S(1)}, u32[]{:S(2)}) copy-start(bf16[128,2048]{1,0:T(8,128)(2,1)S(1)} %collective-permute-done.1.refs_2_.next_ref) | copy-start | bytes 1572868
  38.3 10.8 %collective-permute-start.7 = (bf16[64,2048]{1,0:T(8,128)(2,1)S(1)}, bf16[64,2048]{1,0:T(8,128)(2,1)S(1)}, u32[]{:S(2)}, u32[]{:S(2)}) collective-permute-start(bf16[64,2048]{1,0:T(8,128)(2,1)S(1)} %get-tuple-element.32), channel_id=1, source_target_pairs={{0,2},{2,4},{4,6},{6,0},{1,3},{3,5},{5,7},{7,1},{8,10},{10,12},{12... | collective-permute-start | bytes 786440 | tf_op jit(solution)/shard_map/ppermute | solution.py:380
  40.2 9.8 %collective-permute-start.8 = (bf16[64,2048]{1,0:T(8,128)(2,1)S(1)}, bf16[64,2048]{1,0:T(8,128)(2,1)S(1)}, u32[]{:S(2)}, u32[]{:S(2)}) collective-permute-start(bf16[64,2048]{1,0:T(8,128)(2,1)S(1)} %get-tuple-element.33), channel_id=1, source_target_pairs={{0,6},{2,0},{4,2},{6,4},{1,7},{3,1},{5,3},{7,5},{8,14},{10,8},{12,... | collective-permute-start | bytes 786440 | tf_op jit(solution)/shard_map/ppermute | solution.py:380
  50.0 1.7 %copy-start = (bf16[2048,768]{1,0:T(8,128)(2,1)}, bf16[2048,768]{1,0:T(8,128)(2,1)S(1)}, u32[]{:S(2)}) copy-start(bf16[2048,768]{1,0:T(8,128)(2,1)S(1)} %collective-permute-done.6.refs_8_.refs_3_) | copy-start | bytes 9437188
  51.7 0.7 copy-start.10
  52.4 2.7 %collective-permute-start.2 = (bf16[16,2048]{1,0:T(8,128)(2,1)S(1)}, bf16[16,2048]{1,0:T(8,128)(2,1)S(1)}, u32[]{:S(2)}, u32[]{:S(2)}) collective-permute-start(bf16[16,2048]{1,0:T(8,128)(2,1)S(1)} %get-tuple-element.29), channel_id=1, source_target_pairs={{7,8},{15,16},{23,24},{31,32},{39,40},{47,48},{55,56},{63,64},{71,... | collective-permute-start | bytes 196616 | tf_op jit(solution)/shard_map/ppermute | solution.py:369
  53.0 2.0 %collective-permute-start.3 = (bf16[16,2048]{1,0:T(8,128)(2,1)S(1)}, bf16[16,2048]{1,0:T(8,128)(2,1)S(1)}, u32[]{:S(2)}, u32[]{:S(2)}) collective-permute-start(bf16[16,2048]{1,0:T(8,128)(2,1)S(1)} %get-tuple-element.29), channel_id=1, source_target_pairs={{7,10},{15,18},{23,26},{31,34},{39,42},{47,50},{55,58},{63,66},{71... | collective-permute-start | bytes 196616 | tf_op jit(solution)/shard_map/ppermute | solution.py:369
  53.7 1.4 collective-permute-start.4
  54.4 0.7 collective-permute-start.5
  55.1 1.9 %copy-start.1 = (bf16[2048,768]{1,0:T(8,128)(2,1)S(1)}, bf16[2048,768]{1,0:T(8,128)(2,1)}, u32[]{:S(2)}) copy-start(bf16[2048,768]{1,0:T(8,128)(2,1)} %copy-done) | copy-start | bytes 9437188
  57.0 1.0 copy-start.3
  58.0 1.0 copy-start.5
  59.1 1.0 copy-start.8
  60.1 6.6 %copy-start.11 = (bf16[128,768]{1,0:T(8,128)(2,1)S(1)}, bf16[128,768]{1,0:T(8,128)(2,1)}, u32[]{:S(2)}) copy-start(bf16[128,768]{1,0:T(8,128)(2,1)} %copy-done.10) | copy-start | bytes 589828
  62.8 53.0 %copy-start.9 = (f32[128]{0:T(128)S(1)}, f32[128]{0:T(128)}, u32[]{:S(2)}) copy-start(f32[128]{0:T(128)} %param.33) | copy-start | bytes 1540
  62.8 7.3 %collective-permute-start.9 = (bf16[400,768]{1,0:T(8,128)(2,1)S(1)}, bf16[400,768]{1,0:T(8,128)(2,1)S(1)}, u32[]{:S(2)}, u32[]{:S(2)}) collective-permute-start(bf16[400,768]{1,0:T(8,128)(2,1)S(1)} %get-tuple-element.37), channel_id=1, source_target_pairs={{0,1},{1,0},{2,3},{3,2},{4,5},{5,4},{6,7},{7,6},{8,9},{9,8},{10,11... | collective-permute-start | bytes 1843208 | tf_op jit(solution)/shard_map/ppermute | solution.py:384
  66.8 3.3 %collective-permute-start.10 = (bf16[128,768]{1,0:T(8,128)(2,1)S(1)}, bf16[128,768]{1,0:T(8,128)(2,1)S(1)}, u32[]{:S(2)}, u32[]{:S(2)}) collective-permute-start(bf16[128,768]{1,0:T(8,128)(2,1)S(1)} %copy-done.11), channel_id=1, source_target_pairs={{0,1},{1,0},{2,3},{3,2},{4,5},{5,4},{6,7},{7,6},{8,9},{9,8},{10,11... | collective-permute-start | bytes 589832 | tf_op jit(solution)/shard_map/ppermute | solution.py:384
Sparse Core Ops, SparseCore 0:
  52.5 56.6 all-gather.2

commit v3 on v2

--- a/solution.py
+++ b/solution.py
@@ -115,10 +115,12 @@
         ).astype(BF16)
 
 
-def halves_kernel(prior_ref, next_ref, first_ref, second_ref):
-    half = first_ref.shape[0]
-    first_ref[...] = prior_ref[:half]
-    second_ref[...] = next_ref[half:]
+def first_half_kernel(rows_ref, half_ref):
+    half_ref[...] = rows_ref[: half_ref.shape[0]]
+
+
+def second_half_kernel(rows_ref, half_ref):
+    half_ref[...] = rows_ref[half_ref.shape[0] :]
 
 
 def project_kernel(*refs):
@@ -174,8 +176,18 @@
     conv_in[:HALO] = halo[:, : 3 * STATE]
     pool_in[:HALO] = halo[:, 3 * STATE : 4 * STATE]
     ring = blocks // 2
-    for side, near_ref, far_ref in ((core, own_near_ref, own_far_ref), (1 - core, other_near_ref, other_far_ref)):
-        for away, source in ((0, near_ref[:BLOCK]), (ring - 1, near_ref[BLOCK : 2 * BLOCK]), (1, near_ref[2 * BLOCK : 3 * BLOCK]), (2, far_ref[...])):
+    for side, near_ref, far_ref in (
+        (core, own_near_ref, own_far_ref),
+        (1 - core, other_near_ref, other_far_ref),
+    ):
+        ahead = ring + 1 - 2 * side
+        behind = ring - 1 + 2 * side
+        for away, source in (
+            (0, near_ref[:BLOCK]),
+            (behind, near_ref[BLOCK : 2 * BLOCK]),
+            (ahead, near_ref[2 * BLOCK : 3 * BLOCK]),
+            (2, far_ref[...]),
+        ):
             first = pl.multiple_of(((x + away) % ring * 2 + side) * BLOCK, BLOCK)
             wide = source.astype(F32)
             conv_in[pl.ds(HALO + first, BLOCK)] = wide[:, : 3 * STATE]
@@ -332,19 +344,38 @@
     out_ref[:, STATE:] = pool_ref[...]
 
 
-def output_kernel(rows_ref, w_ref, out_ref, weights_ref, arrived):
-    parts = rows_ref.shape[0]
-    incoming = [
-        pltpu.make_async_copy(w_ref.at[k], weights_ref.at[k], arrived.at[k]) for k in range(parts)
-    ]
-    for copy in incoming:
-        copy.start()
-    total = None
-    for k in range(parts):
-        incoming[k].wait()
-        part = jnp.dot(rows_ref[k], weights_ref[k], preferred_element_type=F32)
-        total = part if total is None else total + part
-    out_ref[...] = total.astype(BF16)
+def output_kernel(
+    place_ref,
+    rows_ref,
+    own_ref,
+    behind_ref,
+    ahead_ref,
+    far_first_ref,
+    far_second_ref,
+    keep_ref,
+    send_ref,
+    total_ref,
+):
+    x, core = place_ref[1], place_ref[2]
+    ring = rows_ref.shape[0]
+    half = far_first_ref.shape[0]
+    total = jnp.dot(rows_ref[x], own_ref[...], preferred_element_type=F32)
+    behind = rows_ref[(x + ring - 1 + 2 * core) % ring]
+    total = total + jnp.dot(behind, behind_ref[...], preferred_element_type=F32)
+    ahead = rows_ref[(x + ring + 1 - 2 * core) % ring]
+    total = total + jnp.dot(ahead, ahead_ref[...], preferred_element_type=F32)
+    far = rows_ref[(x + 2) % ring]
+    total = total + jnp.dot(far[:, :half], far_first_ref[...], preferred_element_type=F32)
+    total_ref[...] = total + jnp.dot(
+        far[:, half:], far_second_ref[...], preferred_element_type=F32
+    )
+    count = keep_ref.shape[0]
+    keep_ref[...] = total_ref[pl.ds(pl.multiple_of(core * count, count), count)]
+    send_ref[...] = total_ref[pl.ds(pl.multiple_of((1 - core) * count, count), count)].astype(BF16)
+
+
+def join_kernel(keep_ref, other_ref, out_ref):
+    out_ref[...] = (keep_ref[...] + other_ref[...].astype(F32)).astype(BF16)
 
 
 def limits(mebibytes):
@@ -377,7 +408,12 @@
 
 def around(array, away):
     ring = lax.axis_size("x")
-    return lax.ppermute(array, "x", [(i, (i + away) % ring) for i in range(ring)])
+    route = [
+        (2 * i + side, 2 * ((i + away * (1 - 2 * side)) % ring) + side)
+        for i in range(ring)
+        for side in range(2)
+    ]
+    return lax.ppermute(array, TP, route)
 
 
 def swapped(array):
@@ -494,9 +530,11 @@
     )
     other_weights = swapped(weights)
     half = own_rows // 2
-    far = kernel_call(halves_kernel, [held((half, width), BF16)] * 2, prior, following)
-    far_first = around(far[0], 1)
-    far_second = around(far[1], -1)
+    half_rows = [held((half, width), BF16)]
+    (prior_half,) = kernel_call(first_half_kernel, half_rows, prior)
+    far_first = around(prior_half, 1)
+    (next_half,) = kernel_call(second_half_kernel, half_rows, following)
+    far_second = around(next_half, -1)
 
     def project(*pieces):
         count = sum(piece.shape[0] for piece in pieces if piece.shape[0] > HALO)
@@ -514,9 +552,9 @@
     own_near, send_near = project(normed, prior, following, *found)
     other_near = swapped(send_near)
     own_far, send_far = project(far_first, far_second)
-    own_far, own_output = lax.optimization_barrier((own_far, own_output))
-    output_weights = lax.all_gather(own_output, TP, axis=0)
+    send_far, own_output = lax.optimization_barrier((send_far, own_output))
     other_far = swapped(send_far)
+    output_behind = around(own_output, 1)
 
     columns, inner = lax.axis_size("sp_0"), lax.axis_size("sp_1")
     y, reads, reach, gate, pool, packed = kernel_call(
@@ -547,6 +585,8 @@
     )
 
     pieces = lax.all_to_all(packed, "sp_1", 0, 0, tiled=True)
+    pieces, own_output = lax.optimization_barrier((pieces, own_output))
+    output_ahead = around(own_output, -1)
     before, packed = kernel_call(
         row_scan_kernel,
         [held((STATE + 8, STATE), F32), held((columns, PACKED, STATE), BF16)],
@@ -554,7 +594,16 @@
         pieces,
         mebibytes=8,
     )
+    packed, output_behind = lax.optimization_barrier((packed, output_behind))
     pieces = lax.all_to_all(packed, "sp_0", 0, 0, tiled=True)
+    output_behind, output_ahead, pieces = lax.optimization_barrier(
+        (output_behind, output_ahead, pieces)
+    )
+    half_outputs = [held((output_rows // 2, width), BF16)]
+    (half,) = kernel_call(first_half_kernel, half_outputs, output_behind)
+    far_outputs = [around(half, 1)]
+    (half,) = kernel_call(second_half_kernel, half_outputs, output_ahead)
+    far_outputs.append(around(half, -1))
     (branches,) = kernel_call(
         finish_kernel,
         [held((length, 2 * STATE), BF16)],
@@ -568,20 +617,23 @@
         pool,
         gated_norm_scale.reshape(1, STATE),
     )
-    members = 2 * ring
     branches = lax.all_to_all(
-        branches.reshape(members, own_rows, 2 * STATE), TP, 0, 0, tiled=True
+        branches.reshape(ring, 2 * own_rows, 2 * STATE), "x", 0, 0, tiled=True
+    )
+    keep, send = kernel_call(
+        output_kernel,
+        [held((own_rows, width), F32), held((own_rows, width), BF16)],
+        place,
+        branches,
+        own_output,
+        output_behind,
+        output_ahead,
+        *far_outputs,
+        scratch=[pltpu.VMEM((2 * own_rows, width), F32)],
+        mebibytes=24,
     )
     (mixed,) = kernel_call(
-        output_kernel,
-        [held((own_rows, width), BF16)],
-        branches,
-        Stored(output_weights),
-        scratch=[
-            pltpu.VMEM((members, 2 * STATE, width), BF16),
-            pltpu.SemaphoreType.DMA((members,)),
-        ],
-        mebibytes=20,
+        join_kernel, [held((own_rows, width), BF16)], keep, swapped(send), mebibytes=8
     )
     return mixed
 

time: 146 us -> 129 us (0.88)
  between operations: 13.6 us -> 0.3 us
  starting transfers between devices: 31 us -> 44.1 us
  blocking collectives: 59.5 us -> 50.7 us
  local copies, waits for them, and re-layouts: 8.16 us -> 0.01 us
  waiting for transfers between devices: 16.1 us -> 17.9 us
    ppermute x4 -> x8, starting transfers between devices: 13.7 us -> 26.9 us  [around(): return lax.ppermute(array, TP, route)]
    unnamed x24 -> x2, local copies, waits for them, and re-layouts: 8.16 us -> 0.01 us
    all_to_all x1, blocking collectives: 21.3 us -> 13.7 us  [shards(): pieces = lax.all_to_all(packed, 'sp_1', 0, 0, tiled=True)]
    pallas_call x9 -> x13, Pallas kernels: 16.9 us -> 15.5 us  [kernel_call(): pl.pallas_call(body, grid=(1,), in_specs=[spec(array) for array in arrays...]
    ppermute x4 -> x8, waiting for transfers between devices: 14.7 us -> 16 us  [around(): return lax.ppermute(array, TP, route)]
    ppermute x3 -> x4, starting transfers between devices: 14.6 us -> 14.5 us  [swapped(): return lax.ppermute(array, 'core', [(0, 1), (1, 0)])]
  transfers between devices with their start and end apart: 12 -> 16, of which waited for: 5 -> 5; matrix products, arithmetic and copies ran while one was open for 0% -> 0% of each run, Pallas kernels for 6% -> 5%
where the time goes in v3:
time: 129 us
  blocking collectives  50.7 us (39%)
  starting transfers between devices  44.1 us (34%)
  waiting for transfers between devices  17.9 us (14%)
  Pallas kernels  15.5 us (12%)
    ppermute x8, starting transfers between devices, around(): return lax.ppermute(array, TP, route)  26.9 us
    all_to_all x1, blocking collectives, shards(): pieces = lax.all_to_all(packed, 'sp_0', 0, 0, tiled=True)  19.6 us
    all_to_all x1, blocking collectives, shards(): lax.all_to_all(branches.reshape(ring, 2 * own_rows, 2 * STATE), 'x', 0, 0...  17.3 us
    ppermute x8, waiting for transfers between devices, around(): return lax.ppermute(array, TP, route)  16 us
    pallas_call x13, Pallas kernels, kernel_call(): pl.pallas_call(body, grid=(1,), in_specs=[spec(array) for array in arrays...  15.5 us
    ppermute x4, starting transfers between devices, swapped(): return lax.ppermute(array, 'core', [(0, 1), (1, 0)])  14.5 us
    all_to_all x1, blocking collectives, shards(): pieces = lax.all_to_all(packed, 'sp_1', 0, 0, tiled=True)  13.7 us
    ppermute x4, starting transfers between devices, rows_before(): lax.ppermute(rows, SP_TP, [(i * members + members - 1, (i + 1) * members...  2.66 us
  transfers between devices with their start and end apart: 16, of which 5 were waited for; matrix products, arithmetic and copies ran while one was open for 0% of the time, Pallas kernels for 5%

profile of v3, /device:TPU:1, one launch (start us, length us, event | category | flops | bytes accessed | tf_op | source)
XLA Modules:
  0.0 128.5 jit_solution(8499501336239680340)
XLA Ops:
  0.0 0.1 pad_add_fusion.place_ref
  0.1 3.1 %shard_map.182 = (bf16[2048,768]{1,0:T(8,128)(2,1)S(1)}, bf16[256,2048]{1,0:T(8,128)(2,1)S(1)}, f32[8,384]{1,0:T(8,128)S(1)}, f32[56,128]{1,0:T(8,128)S(1)}, bf16[128,128]{1,0:T(8,128)(2,1)S(1)}) custom-call(s32[3]{0:T(128)S(1)} %pad_add_fusion.place_ref, bf16[2048,128]{1,0:T(8,128)(2,1)} %value_hbm.1, bf16[2048,128]{1,0:T(8,128)(2,1)} %write_hbm.1, ...), custom_call_target="tpu_custom_call" | custom-call | tf_op jit(solution)/shard_map/pallas_call | solution.py:437
  3.1 8.7 %collective-permute-start.6 = (bf16[2048,768]{1,0:T(8,128)(2,1)S(1)}, bf16[2048,768]{1,0:T(8,128)(2,1)S(1)}, u32[]{:S(2)}, u32[]{:S(2)}) collective-permute-start(bf16[2048,768]{1,0:T(8,128)(2,1)S(1)} %get-tuple-element.37.refs_7_.refs_2_), channel_id=1, source_target_pairs={{0,1},{1,0},{2,3},{3,2},{4,5},{5,4},{6,7},{7,6},{8,9},{9,8},{10,11... | collective-permute-start | bytes 9437192 | tf_op jit(solution)/shard_map/ppermute | solution.py:420
  11.9 1.3 %shard_map.181 = (bf16[128,2048]{1,0:T(8,128)(2,1)S(1)}, bf16[16,2048]{1,0:T(8,128)(2,1)S(1)}) custom-call(bf16[128,2048]{1,0:T(8,128)(2,1)} %x_hbm.1, f32[1,2048]{1,0:T(1,128)} %bitcast.14), custom_call_target="tpu_custom_call" | custom-call | tf_op jit(solution)/shard_map/pallas_call | solution.py:437
  13.2 1.9 %collective-permute-start = (bf16[128,2048]{1,0:T(8,128)(2,1)S(1)}, bf16[128,2048]{1,0:T(8,128)(2,1)S(1)}, u32[]{:S(2)}, u32[]{:S(2)}) collective-permute-start(bf16[128,2048]{1,0:T(8,128)(2,1)S(1)} %get-tuple-element.35.refs_0_), channel_id=1, source_target_pairs={{0,2},{1,7},{2,4},{3,1},{4,6},{5,3},{6,0},{7,5},{8,10},{9,15},{10,... | collective-permute-start | bytes 1572872 | tf_op jit(solution)/shard_map/ppermute | solution.py:416
  15.1 3.4 %collective-permute-start.1 = (bf16[128,2048]{1,0:T(8,128)(2,1)S(1)}, bf16[128,2048]{1,0:T(8,128)(2,1)S(1)}, u32[]{:S(2)}, u32[]{:S(2)}) collective-permute-start(bf16[128,2048]{1,0:T(8,128)(2,1)S(1)} %get-tuple-element.35.refs_0_), channel_id=1, source_target_pairs={{0,6},{1,3},{2,0},{3,5},{4,2},{5,7},{6,4},{7,1},{8,14},{9,11},{10,... | collective-permute-start | bytes 1572872 | tf_op jit(solution)/shard_map/ppermute | solution.py:416
  18.5 0.7 collective-permute-start.2
  19.2 0.7 collective-permute-start.3
  19.8 0.0 collective-permute-done.2.refs_3_
  19.9 0.7 collective-permute-start.4
  20.5 0.0 collective-permute-done.3.refs_4_
  20.5 0.7 collective-permute-start.5
  21.2 0.0 collective-permute-done.4.refs_5_
  21.2 0.0 collective-permute-done.5.refs_6_
  21.2 5.4 %collective-permute-done.refs_1_.rows_ref = bf16[128,2048]{1,0:T(8,128)(2,1)S(1)} collective-permute-done((bf16[128,2048]{1,0:T(8,128)(2,1)S(1)}, bf16[128,2048]{1,0:T(8,128)(2,1)S(1)}, u32[]{:S(2)}, u32[]{:S(2)}) %collective-permute-start) | collective-permute-done | bytes 524320 | tf_op jit(solution)/shard_map/ppermute | solution.py:416
  26.6 3.8 %collective-permute-done.1.refs_2_.rows_ref = bf16[128,2048]{1,0:T(8,128)(2,1)S(1)} collective-permute-done((bf16[128,2048]{1,0:T(8,128)(2,1)S(1)}, bf16[128,2048]{1,0:T(8,128)(2,1)S(1)}, u32[]{:S(2)}, u32[]{:S(2)}) %collective-permute-start.1) | collective-permute-done | bytes 524320 | tf_op jit(solution)/shard_map/ppermute | solution.py:416
  30.4 0.0 collective-permute-done.6.refs_8_.refs_3_
  30.4 2.7 %shard_map.183 = (bf16[400,768]{1,0:T(8,128)(2,1)S(1)}, bf16[400,768]{1,0:T(8,128)(2,1)S(1)}) custom-call(bf16[128,2048]{1,0:T(8,128)(2,1)S(1)} %get-tuple-element.35.refs_0_, bf16[128,2048]{1,0:T(8,128)(2,1)S(1)} %collective-permute-done.refs_1_.rows_ref, bf16[128,2048]{1,0:T(8,128)(2,1)S(1)} %collective-permute-done.1.refs_2_.rows_ref, ...), custom_call_target="tpu_custom_call" | custom-call | tf_op jit(solution)/shard_map/pallas_call | solution.py:437
  33.1 1.9 %collective-permute-start.9 = (bf16[400,768]{1,0:T(8,128)(2,1)S(1)}, bf16[400,768]{1,0:T(8,128)(2,1)S(1)}, u32[]{:S(2)}, u32[]{:S(2)}) collective-permute-start(bf16[400,768]{1,0:T(8,128)(2,1)S(1)} %get-tuple-element.40), channel_id=1, source_target_pairs={{0,1},{1,0},{2,3},{3,2},{4,5},{5,4},{6,7},{7,6},{8,9},{9,8},{10,11... | collective-permute-start | bytes 1843208 | tf_op jit(solution)/shard_map/ppermute | solution.py:420
  35.1 2.1 %collective-permute-start.7 = (bf16[64,2048]{1,0:T(8,128)(2,1)S(1)}, bf16[64,2048]{1,0:T(8,128)(2,1)S(1)}, u32[]{:S(2)}, u32[]{:S(2)}) collective-permute-start(bf16[64,2048]{1,0:T(8,128)(2,1)S(1)} %shard_map.184), channel_id=1, source_target_pairs={{0,2},{1,7},{2,4},{3,1},{4,6},{5,3},{6,0},{7,5},{8,10},{9,15},{10,... | collective-permute-start | bytes 786440 | tf_op jit(solution)/shard_map/ppermute | solution.py:416
  37.2 3.2 %collective-permute-start.8 = (bf16[64,2048]{1,0:T(8,128)(2,1)S(1)}, bf16[64,2048]{1,0:T(8,128)(2,1)S(1)}, u32[]{:S(2)}, u32[]{:S(2)}) collective-permute-start(bf16[64,2048]{1,0:T(8,128)(2,1)S(1)} %shard_map.185), channel_id=1, source_target_pairs={{0,6},{1,3},{2,0},{3,5},{4,2},{5,7},{6,4},{7,1},{8,14},{9,11},{10,... | collective-permute-start | bytes 786440 | tf_op jit(solution)/shard_map/ppermute | solution.py:416
  40.4 2.1 %collective-permute-done.7.refs_0_ = bf16[64,2048]{1,0:T(8,128)(2,1)S(1)} collective-permute-done((bf16[64,2048]{1,0:T(8,128)(2,1)S(1)}, bf16[64,2048]{1,0:T(8,128)(2,1)S(1)}, u32[]{:S(2)}, u32[]{:S(2)}) %collective-permute-start.7) | collective-permute-done | bytes 262176 | tf_op jit(solution)/shard_map/ppermute | solution.py:416
  42.5 4.7 %collective-permute-done.8.refs_1_ = bf16[64,2048]{1,0:T(8,128)(2,1)S(1)} collective-permute-done((bf16[64,2048]{1,0:T(8,128)(2,1)S(1)}, bf16[64,2048]{1,0:T(8,128)(2,1)S(1)}, u32[]{:S(2)}, u32[]{:S(2)}) %collective-permute-start.8) | collective-permute-done | bytes 262176 | tf_op jit(solution)/shard_map/ppermute | solution.py:416
  47.2 1.0 shard_map.186
  48.2 1.9 %collective-permute-start.10 = (bf16[128,768]{1,0:T(8,128)(2,1)S(1)}, bf16[128,768]{1,0:T(8,128)(2,1)S(1)}, u32[]{:S(2)}, u32[]{:S(2)}) collective-permute-start(bf16[128,768]{1,0:T(8,128)(2,1)S(1)} %get-tuple-element.43), channel_id=1, source_target_pairs={{0,1},{1,0},{2,3},{3,2},{4,5},{5,4},{6,7},{7,6},{8,9},{9,8},{10,11... | collective-permute-start | bytes 589832 | tf_op jit(solution)/shard_map/ppermute | solution.py:420
  50.1 4.7 %collective-permute-start.11 = (bf16[256,2048]{1,0:T(8,128)(2,1)S(1)}, bf16[256,2048]{1,0:T(8,128)(2,1)S(1)}, u32[]{:S(2)}, u32[]{:S(2)}) collective-permute-start(bf16[256,2048]{1,0:T(8,128)(2,1)S(1)} %get-tuple-element.52.own_ref), channel_id=1, source_target_pairs={{0,2},{1,7},{2,4},{3,1},{4,6},{5,3},{6,0},{7,5},{8,10},{9,15},{10,... | collective-permute-start | bytes 3145736 | tf_op jit(solution)/shard_map/ppermute | solution.py:416
  54.8 0.0 collective-permute-done.10.other_far_ref
  54.8 0.0 collective-permute-done.9.other_near_ref
  54.8 0.0 copy-start
  54.8 3.7 %shard_map.187 = (f32[1024,128]{1,0:T(8,128)S(1)}, bf16[1024,128]{1,0:T(8,128)(2,1)S(1)}, f32[1024,128]{1,0:T(8,128)S(1)}, f32[1024,128]{1,0:T(8,128)S(1)}, bf16...) custom-call(s32[3]{0:T(128)S(1)} %pad_add_fusion.place_ref, ...), custom_call_target="tpu_custom_call" | custom-call | tf_op jit(solution)/shard_map/pallas_call | solution.py:437
  58.5 13.7 %all_to_all.15.pieces_ref = bf16[8,144,128]{2,1,0:T(8,128)(2,1)S(1)} all-to-all(bf16[8,144,128]{2,1,0:T(8,128)(2,1)S(1)} %get-tuple-element.47), channel_id=1, replica_groups=mesh['sp_0'=8,'sp_1'=8,'x'=4,'core'=2] {'sp_1'}, dimensions={0} | all-to-all | bytes 589824 | tf_op jit(solution)/shard_map/all_to_all | solution.py:587
  72.3 2.0 %collective-permute-start.12 = (bf16[256,2048]{1,0:T(8,128)(2,1)S(1)}, bf16[256,2048]{1,0:T(8,128)(2,1)S(1)}, u32[]{:S(2)}, u32[]{:S(2)}) collective-permute-start(bf16[256,2048]{1,0:T(8,128)(2,1)S(1)} %get-tuple-element.52.own_ref), channel_id=1, source_target_pairs={{0,6},{1,3},{2,0},{3,5},{4,2},{5,7},{6,4},{7,1},{8,14},{9,11},{10,... | collective-permute-start | bytes 3145736 | tf_op jit(solution)/shard_map/ppermute | solution.py:416
  74.2 0.1 shard_map.188
  74.3 0.0 collective-permute-done.11.rows_ref.behind_ref
  74.4 19.6 %all_to_all.16.pieces_ref = bf16[8,144,128]{2,1,0:T(8,128)(2,1)S(1)} all-to-all(bf16[8,144,128]{2,1,0:T(8,128)(2,1)S(1)} %get-tuple-element.53), channel_id=1, replica_groups=mesh['sp_0'=8,'sp_1'=8,'x'=4,'core'=2] {'sp_0'}, dimensions={0} | all-to-all | bytes 589824 | tf_op jit(solution)/shard_map/all_to_all | solution.py:598
  94.0 0.0 collective-permute-done.12.rows_ref.ahead_ref
  94.0 7.8 %collective-permute-start.13 = (bf16[128,2048]{1,0:T(8,128)(2,1)S(1)}, bf16[128,2048]{1,0:T(8,128)(2,1)S(1)}, u32[]{:S(2)}, u32[]{:S(2)}) collective-permute-start(bf16[128,2048]{1,0:T(8,128)(2,1)S(1)} %shard_map.190), channel_id=1, source_target_pairs={{0,2},{1,7},{2,4},{3,1},{4,6},{5,3},{6,0},{7,5},{8,10},{9,15},{10,... | collective-permute-start | bytes 1572872 | tf_op jit(solution)/shard_map/ppermute | solution.py:416
  101.9 1.9 %collective-permute-start.14 = (bf16[128,2048]{1,0:T(8,128)(2,1)S(1)}, bf16[128,2048]{1,0:T(8,128)(2,1)S(1)}, u32[]{:S(2)}, u32[]{:S(2)}) collective-permute-start(bf16[128,2048]{1,0:T(8,128)(2,1)S(1)} %shard_map.191), channel_id=1, source_target_pairs={{0,6},{1,3},{2,0},{3,5},{4,2},{5,7},{6,4},{7,1},{8,14},{9,11},{10,... | collective-permute-start | bytes 1572872 | tf_op jit(solution)/shard_map/ppermute | solution.py:416
  103.8 0.0 copy-done
  103.8 0.5 shard_map.189
  104.3 17.3 %all_to_all.17.rows_ref = bf16[4,256,256]{2,1,0:T(8,128)(2,1)S(1)} all-to-all(bf16[4,256,256]{2,1,0:T(8,128)(2,1)S(1)} %bitcast.11), channel_id=1, replica_groups=mesh['sp_0'=8,'sp_1'=8,'x'=4,'core'=2] {'x'}, dimensions={0} | all-to-all | bytes 1048576 | tf_op jit(solution)/shard_map/all_to_all | solution.py:620
  121.6 0.0 collective-permute-done.13.far_first_ref
  121.6 0.0 collective-permute-done.14.far_second_ref
  121.6 2.2 %shard_map.192 = (f32[128,2048]{1,0:T(8,128)S(1)}, bf16[128,2048]{1,0:T(8,128)(2,1)S(1)}) custom-call(s32[3]{0:T(128)S(1)} %pad_add_fusion.place_ref, bf16[4,256,256]{2,1,0:T(8,128)(2,1)S(1)} %all_to_all.17.rows_ref, bf16[256,2048]{1,0:T(8,128)(2,1)S(1)} %get-tuple-element.52.own_ref, bf16[256,2048]{1,0:T(8,128)(2,1)S(1)} %collective-permute-done.11.rows_ref.behind_ref, ...), custom_call_target="tpu_custom_call" | custom-call | tf_op jit(solution)/shard_map/pallas_call | solution.py:437
  123.8 1.9 %collective-permute-start.15 = (bf16[128,2048]{1,0:T(8,128)(2,1)S(1)}, bf16[128,2048]{1,0:T(8,128)(2,1)S(1)}, u32[]{:S(2)}, u32[]{:S(2)}) collective-permute-start(bf16[128,2048]{1,0:T(8,128)(2,1)S(1)} %get-tuple-element.64), channel_id=1, source_target_pairs={{0,1},{1,0},{2,3},{3,2},{4,5},{5,4},{6,7},{7,6},{8,9},{9,8},{10,11... | collective-permute-start | bytes 1572872 | tf_op jit(solution)/shard_map/ppermute | solution.py:420
  125.8 1.9 %collective-permute-done.15.other_ref = bf16[128,2048]{1,0:T(8,128)(2,1)S(1)} collective-permute-done((bf16[128,2048]{1,0:T(8,128)(2,1)S(1)}, bf16[128,2048]{1,0:T(8,128)(2,1)S(1)}, u32[]{:S(2)}, u32[]{:S(2)}) %collective-permute-start.15) | collective-permute-done | bytes 524320 | tf_op jit(solution)/shard_map/ppermute | solution.py:420
  127.6 0.9 shard_map.193
  (4 shorter events, 0.1 us)
Async XLA Ops:
  3.1 27.3 %collective-permute-start.6 = (bf16[2048,768]{1,0:T(8,128)(2,1)S(1)}, bf16[2048,768]{1,0:T(8,128)(2,1)S(1)}, u32[]{:S(2)}, u32[]{:S(2)}) collective-permute-start(bf16[2048,768]{1,0:T(8,128)(2,1)S(1)} %get-tuple-element.37.refs_7_.refs_2_), channel_id=1, source_target_pairs={{0,1},{1,0},{2,3},{3,2},{4,5},{5,4},{6,7},{7,6},{8,9},{9,8},{10,11... | collective-permute-start | bytes 9437192 | tf_op jit(solution)/shard_map/ppermute | solution.py:420
  13.2 13.4 %collective-permute-start = (bf16[128,2048]{1,0:T(8,128)(2,1)S(1)}, bf16[128,2048]{1,0:T(8,128)(2,1)S(1)}, u32[]{:S(2)}, u32[]{:S(2)}) collective-permute-start(bf16[128,2048]{1,0:T(8,128)(2,1)S(1)} %get-tuple-element.35.refs_0_), channel_id=1, source_target_pairs={{0,2},{1,7},{2,4},{3,1},{4,6},{5,3},{6,0},{7,5},{8,10},{9,15},{10,... | collective-permute-start | bytes 1572872 | tf_op jit(solution)/shard_map/ppermute | solution.py:416
  15.1 15.3 %collective-permute-start.1 = (bf16[128,2048]{1,0:T(8,128)(2,1)S(1)}, bf16[128,2048]{1,0:T(8,128)(2,1)S(1)}, u32[]{:S(2)}, u32[]{:S(2)}) collective-permute-start(bf16[128,2048]{1,0:T(8,128)(2,1)S(1)} %get-tuple-element.35.refs_0_), channel_id=1, source_target_pairs={{0,6},{1,3},{2,0},{3,5},{4,2},{5,7},{6,4},{7,1},{8,14},{9,11},{10,... | collective-permute-start | bytes 1572872 | tf_op jit(solution)/shard_map/ppermute | solution.py:416
  18.5 1.3 %collective-permute-start.2 = (bf16[16,2048]{1,0:T(8,128)(2,1)S(1)}, bf16[16,2048]{1,0:T(8,128)(2,1)S(1)}, u32[]{:S(2)}, u32[]{:S(2)}) collective-permute-start(bf16[16,2048]{1,0:T(8,128)(2,1)S(1)} %get-tuple-element.36), channel_id=1, source_target_pairs={{7,8},{15,16},{23,24},{31,32},{39,40},{47,48},{55,56},{63,64},{71,... | collective-permute-start | bytes 196616 | tf_op jit(solution)/shard_map/ppermute | solution.py:400
  19.2 1.4 %collective-permute-start.3 = (bf16[16,2048]{1,0:T(8,128)(2,1)S(1)}, bf16[16,2048]{1,0:T(8,128)(2,1)S(1)}, u32[]{:S(2)}, u32[]{:S(2)}) collective-permute-start(bf16[16,2048]{1,0:T(8,128)(2,1)S(1)} %get-tuple-element.36), channel_id=1, source_target_pairs={{7,10},{15,18},{23,26},{31,34},{39,42},{47,50},{55,58},{63,66},{71... | collective-permute-start | bytes 196616 | tf_op jit(solution)/shard_map/ppermute | solution.py:400
  19.9 1.4 %collective-permute-start.4 = (bf16[16,2048]{1,0:T(8,128)(2,1)S(1)}, bf16[16,2048]{1,0:T(8,128)(2,1)S(1)}, u32[]{:S(2)}, u32[]{:S(2)}) collective-permute-start(bf16[16,2048]{1,0:T(8,128)(2,1)S(1)} %get-tuple-element.36), channel_id=1, source_target_pairs={{7,12},{15,20},{23,28},{31,36},{39,44},{47,52},{55,60},{63,68},{71... | collective-permute-start | bytes 196616 | tf_op jit(solution)/shard_map/ppermute | solution.py:400
  20.5 0.7 collective-permute-start.5
  33.1 21.7 %collective-permute-start.9 = (bf16[400,768]{1,0:T(8,128)(2,1)S(1)}, bf16[400,768]{1,0:T(8,128)(2,1)S(1)}, u32[]{:S(2)}, u32[]{:S(2)}) collective-permute-start(bf16[400,768]{1,0:T(8,128)(2,1)S(1)} %get-tuple-element.40), channel_id=1, source_target_pairs={{0,1},{1,0},{2,3},{3,2},{4,5},{5,4},{6,7},{7,6},{8,9},{9,8},{10,11... | collective-permute-start | bytes 1843208 | tf_op jit(solution)/shard_map/ppermute | solution.py:420
  35.1 7.4 %collective-permute-start.7 = (bf16[64,2048]{1,0:T(8,128)(2,1)S(1)}, bf16[64,2048]{1,0:T(8,128)(2,1)S(1)}, u32[]{:S(2)}, u32[]{:S(2)}) collective-permute-start(bf16[64,2048]{1,0:T(8,128)(2,1)S(1)} %shard_map.184), channel_id=1, source_target_pairs={{0,2},{1,7},{2,4},{3,1},{4,6},{5,3},{6,0},{7,5},{8,10},{9,15},{10,... | collective-permute-start | bytes 786440 | tf_op jit(solution)/shard_map/ppermute | solution.py:416
  37.2 9.9 %collective-permute-start.8 = (bf16[64,2048]{1,0:T(8,128)(2,1)S(1)}, bf16[64,2048]{1,0:T(8,128)(2,1)S(1)}, u32[]{:S(2)}, u32[]{:S(2)}) collective-permute-start(bf16[64,2048]{1,0:T(8,128)(2,1)S(1)} %shard_map.185), channel_id=1, source_target_pairs={{0,6},{1,3},{2,0},{3,5},{4,2},{5,7},{6,4},{7,1},{8,14},{9,11},{10,... | collective-permute-start | bytes 786440 | tf_op jit(solution)/shard_map/ppermute | solution.py:416
  48.2 6.6 %collective-permute-start.10 = (bf16[128,768]{1,0:T(8,128)(2,1)S(1)}, bf16[128,768]{1,0:T(8,128)(2,1)S(1)}, u32[]{:S(2)}, u32[]{:S(2)}) collective-permute-start(bf16[128,768]{1,0:T(8,128)(2,1)S(1)} %get-tuple-element.43), channel_id=1, source_target_pairs={{0,1},{1,0},{2,3},{3,2},{4,5},{5,4},{6,7},{7,6},{8,9},{9,8},{10,11... | collective-permute-start | bytes 589832 | tf_op jit(solution)/shard_map/ppermute | solution.py:420
  50.1 24.2 %collective-permute-start.11 = (bf16[256,2048]{1,0:T(8,128)(2,1)S(1)}, bf16[256,2048]{1,0:T(8,128)(2,1)S(1)}, u32[]{:S(2)}, u32[]{:S(2)}) collective-permute-start(bf16[256,2048]{1,0:T(8,128)(2,1)S(1)} %get-tuple-element.52.own_ref), channel_id=1, source_target_pairs={{0,2},{1,7},{2,4},{3,1},{4,6},{5,3},{6,0},{7,5},{8,10},{9,15},{10,... | collective-permute-start | bytes 3145736 | tf_op jit(solution)/shard_map/ppermute | solution.py:416
  54.8 49.0 %copy-start = (f32[128]{0:T(128)S(1)}, f32[128]{0:T(128)}, u32[]{:S(2)}) copy-start(f32[128]{0:T(128)} %param.33) | copy-start | bytes 1540
  72.3 21.7 %collective-permute-start.12 = (bf16[256,2048]{1,0:T(8,128)(2,1)S(1)}, bf16[256,2048]{1,0:T(8,128)(2,1)S(1)}, u32[]{:S(2)}, u32[]{:S(2)}) collective-permute-start(bf16[256,2048]{1,0:T(8,128)(2,1)S(1)} %get-tuple-element.52.own_ref), channel_id=1, source_target_pairs={{0,6},{1,3},{2,0},{3,5},{4,2},{5,7},{6,4},{7,1},{8,14},{9,11},{10,... | collective-permute-start | bytes 3145736 | tf_op jit(solution)/shard_map/ppermute | solution.py:416
  94.0 27.6 %collective-permute-start.13 = (bf16[128,2048]{1,0:T(8,128)(2,1)S(1)}, bf16[128,2048]{1,0:T(8,128)(2,1)S(1)}, u32[]{:S(2)}, u32[]{:S(2)}) collective-permute-start(bf16[128,2048]{1,0:T(8,128)(2,1)S(1)} %shard_map.190), channel_id=1, source_target_pairs={{0,2},{1,7},{2,4},{3,1},{4,6},{5,3},{6,0},{7,5},{8,10},{9,15},{10,... | collective-permute-start | bytes 1572872 | tf_op jit(solution)/shard_map/ppermute | solution.py:416
  101.9 19.8 %collective-permute-start.14 = (bf16[128,2048]{1,0:T(8,128)(2,1)S(1)}, bf16[128,2048]{1,0:T(8,128)(2,1)S(1)}, u32[]{:S(2)}, u32[]{:S(2)}) collective-permute-start(bf16[128,2048]{1,0:T(8,128)(2,1)S(1)} %shard_map.191), channel_id=1, source_target_pairs={{0,6},{1,3},{2,0},{3,5},{4,2},{5,7},{6,4},{7,1},{8,14},{9,11},{10,... | collective-permute-start | bytes 1572872 | tf_op jit(solution)/shard_map/ppermute | solution.py:416
  123.8 3.8 %collective-permute-start.15 = (bf16[128,2048]{1,0:T(8,128)(2,1)S(1)}, bf16[128,2048]{1,0:T(8,128)(2,1)S(1)}, u32[]{:S(2)}, u32[]{:S(2)}) collective-permute-start(bf16[128,2048]{1,0:T(8,128)(2,1)S(1)} %get-tuple-element.64), channel_id=1, source_target_pairs={{0,1},{1,0},{2,3},{3,2},{4,5},{5,4},{6,7},{7,6},{8,9},{9,8},{10,11... | collective-permute-start | bytes 1572872 | tf_op jit(solution)/shard_map/ppermute | solution.py:420

commit v4 on v2

--- a/solution.py
+++ b/solution.py
@@ -55,25 +55,20 @@
     read_hbm,
     pool_hbm,
     gate_hbm,
-    state_output_hbm,
-    pool_output_hbm,
     *refs,
 ):
-    small_hbm, (w_ref, output_ref, taps_ref, lanes_ref, pool_matrix_ref), small = (
+    small_hbm, (w_ref, taps_ref, lanes_ref, pool_matrix_ref), small = (
         refs[:9],
-        refs[9:14],
-        refs[14:23],
-    )
-    arrived = refs[23]
+        refs[9:13],
+        refs[13:22],
+    )
+    arrived = refs[22]
     step_ref, value_taps, write_taps, read_taps, bias_ref, pld_ref, rate_ref = small[:7]
     group_ref, channel_ref = small[7:]
-    count = state_output_hbm.shape[0]
     large = [
         (ref, w_ref.at[:, k * STATE : (k + 1) * STATE])
         for k, ref in enumerate((value_hbm, write_hbm, read_hbm, pool_hbm, gate_hbm))
     ]
-    large.append((state_output_hbm, output_ref.at[:count]))
-    large.append((pool_output_hbm, output_ref.at[count:]))
     fetch(large + list(zip(small_hbm, small)), arrived)
     rank = place_ref[1] * 2 + place_ref[2]
     heads, length = bias_ref.shape
@@ -113,6 +108,11 @@
         pool_matrix_ref[k * POOL_DIM : (k + 1) * POOL_DIM] = jnp.dot(
             group_ref[k], place, preferred_element_type=F32
         ).astype(BF16)
+
+
+def stack_kernel(state_hbm, pool_hbm, out_ref, arrived):
+    count = state_hbm.shape[0]
+    fetch(((state_hbm, out_ref.at[:count]), (pool_hbm, out_ref.at[count:])), arrived)
 
 
 def halves_kernel(prior_ref, next_ref, first_ref, second_ref):
@@ -337,11 +337,13 @@
     incoming = [
         pltpu.make_async_copy(w_ref.at[k], weights_ref.at[k], arrived.at[k]) for k in range(parts)
     ]
-    for copy in incoming:
+    for copy in incoming[:3]:
         copy.start()
     total = None
     for k in range(parts):
         incoming[k].wait()
+        if k + 3 < parts:
+            incoming[k + 3].start()
         part = jnp.dot(rows_ref[k], weights_ref[k], preferred_element_type=F32)
         total = part if total is None else total + part
     out_ref[...] = total.astype(BF16)
@@ -458,6 +460,14 @@
     following = around(normed, -1)
     found = rows_before(tail, ring)
     output_rows = state_output_matrix.shape[0] + pooling_output_matrix.shape[0]
+    (own_output,) = kernel_call(
+        stack_kernel,
+        [held((output_rows, width), BF16)],
+        Stored(state_output_matrix),
+        Stored(pooling_output_matrix),
+        scratch=[pltpu.SemaphoreType.DMA((2,))],
+    )
+    output_weights = lax.all_gather(own_output, TP, axis=0)
     small = [
         step_weight_matrix.T,
         value_filter_weight,
@@ -475,14 +485,11 @@
         read_weight_matrix,
         pooling_input_matrix,
         gate_weight_matrix,
-        state_output_matrix,
-        pooling_output_matrix,
     ]
-    weights, own_output, taps, lanes, pool_matrix = kernel_call(
+    weights, taps, lanes, pool_matrix = kernel_call(
         prepare_kernel,
         [
             held((width, 6 * STATE), BF16),
-            held((output_rows, width), BF16),
             held((8, 3 * STATE), F32),
             held((6 * blocks + 8, STATE), F32),
             held((STATE, STATE), BF16),
@@ -514,8 +521,6 @@
     own_near, send_near = project(normed, prior, following, *found)
     other_near = swapped(send_near)
     own_far, send_far = project(far_first, far_second)
-    own_far, own_output = lax.optimization_barrier((own_far, own_output))
-    output_weights = lax.all_gather(own_output, TP, axis=0)
     other_far = swapped(send_far)
 
     columns, inner = lax.axis_size("sp_0"), lax.axis_size("sp_1")

time: 146 us -> 145 us (level)
  waiting for transfers between devices: 16.1 us -> 27.7 us
  local copies, waits for them, and re-layouts: 8.16 us -> 0.01 us
  blocking collectives: 59.5 us -> 51.5 us
  Pallas kernels: 16.9 us -> 19.7 us
    ppermute x4, waiting for transfers between devices: 14.7 us -> 26.6 us  [around(): lax.ppermute(array, 'x', [(i, (i + away) % ring) for i in range(ring)])]
    unnamed x24 -> x2, local copies, waits for them, and re-layouts: 8.16 us -> 0.01 us
    all_to_all x1, blocking collectives: 21.3 us -> 15 us  [shards(): pieces = lax.all_to_all(packed, 'sp_1', 0, 0, tiled=True)]
    pallas_call x9 -> x10, Pallas kernels: 16.9 us -> 19.7 us  [kernel_call(): pl.pallas_call(body, grid=(1,), in_specs=[spec(array) for array in arrays...]
  transfers between devices with their start and end apart: 12 -> 12, of which waited for: 5 -> 5; matrix products, arithmetic and copies ran while one was open for 0% -> 0% of each run, Pallas kernels for 6% -> 8%
where the time goes in v4:
time: 145 us
  blocking collectives  51.5 us (36%)
  starting transfers between devices  32.3 us (22%)
  waiting for transfers between devices  27.7 us (19%)
  Pallas kernels  19.7 us (14%)
  between operations  13.6 us (9%)
    ppermute x4, waiting for transfers between devices, around(): lax.ppermute(array, 'x', [(i, (i + away) % ring) for i in range(ring)])  26.6 us
    all_to_all x1, blocking collectives, shards(): pieces = lax.all_to_all(packed, 'sp_0', 0, 0, tiled=True)  19.8 us
    pallas_call x10, Pallas kernels, kernel_call(): pl.pallas_call(body, grid=(1,), in_specs=[spec(array) for array in arrays...  19.7 us
    all_to_all x1, blocking collectives, shards(): lax.all_to_all(branches.reshape(members, own_rows, 2 * STATE), TP, 0, 0,...  16.6 us
    ppermute x3, starting transfers between devices, swapped(): return lax.ppermute(array, 'core', [(0, 1), (1, 0)])  16 us
    all_to_all x1, blocking collectives, shards(): pieces = lax.all_to_all(packed, 'sp_1', 0, 0, tiled=True)  15 us
    ppermute x4, starting transfers between devices, around(): lax.ppermute(array, 'x', [(i, (i + away) % ring) for i in range(ring)])  13.7 us
  transfers between devices with their start and end apart: 12, of which 5 were waited for; matrix products, arithmetic and copies ran while one was open for 0% of the time, Pallas kernels for 8%

profile of v4, /device:TPU:1, one launch (start us, length us, event | category | flops | bytes accessed | tf_op | source)
XLA Modules:
  0.0 144.9 jit_solution(11774607692499901541)
XLA Ops:
  6.5 0.0 all-gather.3.cloned.1.call-start
  6.5 2.3 %shard_map.189 = bf16[256,2048]{1,0:T(8,128)(2,1)} custom-call(bf16[128,2048]{1,0:T(8,128)(2,1)} %state_hbm.1, bf16[128,2048]{1,0:T(8,128)(2,1)} %pool_hbm.3), custom_call_target="tpu_custom_call" | custom-call | tf_op jit(solution)/shard_map/pallas_call | solution.py:403
  8.8 0.0 all-gather.3.cloned.1.call-update
  8.9 0.1 pad_add_fusion.place_ref
  8.9 2.7 %shard_map.182 = (bf16[2048,768]{1,0:T(8,128)(2,1)S(1)}, f32[8,384]{1,0:T(8,128)S(1)}, f32[56,128]{1,0:T(8,128)S(1)}, bf16[128,128]{1,0:T(8,128)(2,1)S(1)}) custom-call(s32[3]{0:T(128)S(1)} %pad_add_fusion.place_ref, bf16[2048,128]{1,0:T(8,128)(2,1)} %value_hbm.1, bf16[2048,128]{1,0:T(8,128)(2,1)} %write_hbm.1, bf16[2048,128]{1,0:T(8,128)(2,1)} %read_hbm.1, ...), custom_call_target="tpu_custom_call" | custom-call | tf_op jit(solution)/shard_map/pallas_call | solution.py:403
  11.7 8.7 %collective-permute-start.6 = (bf16[2048,768]{1,0:T(8,128)(2,1)S(1)}, bf16[2048,768]{1,0:T(8,128)(2,1)S(1)}, u32[]{:S(2)}, u32[]{:S(2)}) collective-permute-start(bf16[2048,768]{1,0:T(8,128)(2,1)S(1)} %get-tuple-element.27.refs_7_.refs_2_), channel_id=1, source_target_pairs={{0,1},{1,0},{2,3},{3,2},{4,5},{5,4},{6,7},{7,6},{8,9},{9,8},{10,11... | collective-permute-start | bytes 9437192 | tf_op jit(solution)/shard_map/ppermute | solution.py:386
  20.4 1.3 shard_map.181
  21.7 1.9 %collective-permute-start = (bf16[128,2048]{1,0:T(8,128)(2,1)S(1)}, bf16[128,2048]{1,0:T(8,128)(2,1)S(1)}, u32[]{:S(2)}, u32[]{:S(2)}) collective-permute-start(bf16[128,2048]{1,0:T(8,128)(2,1)S(1)} %get-tuple-element.25.refs_0_), channel_id=1, source_target_pairs={{0,2},{2,4},{4,6},{6,0},{1,3},{3,5},{5,7},{7,1},{8,10},{10,12},{12... | collective-permute-start | bytes 1572872 | tf_op jit(solution)/shard_map/ppermute | solution.py:382
  23.6 4.6 %collective-permute-start.1 = (bf16[128,2048]{1,0:T(8,128)(2,1)S(1)}, bf16[128,2048]{1,0:T(8,128)(2,1)S(1)}, u32[]{:S(2)}, u32[]{:S(2)}) collective-permute-start(bf16[128,2048]{1,0:T(8,128)(2,1)S(1)} %get-tuple-element.25.refs_0_), channel_id=1, source_target_pairs={{0,6},{2,0},{4,2},{6,4},{1,7},{3,1},{5,3},{7,5},{8,14},{10,8},{12,... | collective-permute-start | bytes 1572872 | tf_op jit(solution)/shard_map/ppermute | solution.py:382
  28.2 0.7 collective-permute-start.2
  28.9 0.7 collective-permute-start.3
  29.6 0.0 collective-permute-done.2.refs_3_
  29.6 0.7 collective-permute-start.4
  30.3 0.0 collective-permute-done.3.refs_4_
  30.3 0.7 collective-permute-start.5
  30.9 0.0 collective-permute-done.4.refs_5_
  31.0 0.0 collective-permute-done.5.refs_6_
  31.0 10.9 %collective-permute-done.refs_1_.prior_ref = bf16[128,2048]{1,0:T(8,128)(2,1)S(1)} collective-permute-done((bf16[128,2048]{1,0:T(8,128)(2,1)S(1)}, bf16[128,2048]{1,0:T(8,128)(2,1)S(1)}, u32[]{:S(2)}, u32[]{:S(2)}) %collective-permute-start) | collective-permute-done | bytes 524320 | tf_op jit(solution)/shard_map/ppermute | solution.py:382
  41.9 3.9 %collective-permute-done.1.refs_2_.next_ref = bf16[128,2048]{1,0:T(8,128)(2,1)S(1)} collective-permute-done((bf16[128,2048]{1,0:T(8,128)(2,1)S(1)}, bf16[128,2048]{1,0:T(8,128)(2,1)S(1)}, u32[]{:S(2)}, u32[]{:S(2)}) %collective-permute-start.1) | collective-permute-done | bytes 524320 | tf_op jit(solution)/shard_map/ppermute | solution.py:382
  45.9 0.0 collective-permute-done.6.refs_8_.refs_3_
  45.9 2.7 %shard_map.183 = (bf16[400,768]{1,0:T(8,128)(2,1)S(1)}, bf16[400,768]{1,0:T(8,128)(2,1)S(1)}) custom-call(bf16[128,2048]{1,0:T(8,128)(2,1)S(1)} %get-tuple-element.25.refs_0_, bf16[128,2048]{1,0:T(8,128)(2,1)S(1)} %collective-permute-done.refs_1_.prior_ref, bf16[128,2048]{1,0:T(8,128)(2,1)S(1)} %collective-permute-done.1.refs_2_.next_ref, ...), custom_call_target="tpu_custom_call" | custom-call | tf_op jit(solution)/shard_map/pallas_call | solution.py:403
  48.6 4.6 %collective-permute-start.9 = (bf16[400,768]{1,0:T(8,128)(2,1)S(1)}, bf16[400,768]{1,0:T(8,128)(2,1)S(1)}, u32[]{:S(2)}, u32[]{:S(2)}) collective-permute-start(bf16[400,768]{1,0:T(8,128)(2,1)S(1)} %get-tuple-element.32), channel_id=1, source_target_pairs={{0,1},{1,0},{2,3},{3,2},{4,5},{5,4},{6,7},{7,6},{8,9},{9,8},{10,11... | collective-permute-start | bytes 1843208 | tf_op jit(solution)/shard_map/ppermute | solution.py:386
  53.2 1.9 %collective-permute-start.7 = (bf16[64,2048]{1,0:T(8,128)(2,1)S(1)}, bf16[64,2048]{1,0:T(8,128)(2,1)S(1)}, u32[]{:S(2)}, u32[]{:S(2)}) collective-permute-start(bf16[64,2048]{1,0:T(8,128)(2,1)S(1)} %get-tuple-element.29), channel_id=1, source_target_pairs={{0,2},{2,4},{4,6},{6,0},{1,3},{3,5},{5,7},{7,1},{8,10},{10,12},{12... | collective-permute-start | bytes 786440 | tf_op jit(solution)/shard_map/ppermute | solution.py:382
  55.1 5.3 %collective-permute-start.8 = (bf16[64,2048]{1,0:T(8,128)(2,1)S(1)}, bf16[64,2048]{1,0:T(8,128)(2,1)S(1)}, u32[]{:S(2)}, u32[]{:S(2)}) collective-permute-start(bf16[64,2048]{1,0:T(8,128)(2,1)S(1)} %get-tuple-element.30), channel_id=1, source_target_pairs={{0,6},{2,0},{4,2},{6,4},{1,7},{3,1},{5,3},{7,5},{8,14},{10,8},{12,... | collective-permute-start | bytes 786440 | tf_op jit(solution)/shard_map/ppermute | solution.py:382
  60.4 10.7 %collective-permute-done.7.refs_0_ = bf16[64,2048]{1,0:T(8,128)(2,1)S(1)} collective-permute-done((bf16[64,2048]{1,0:T(8,128)(2,1)S(1)}, bf16[64,2048]{1,0:T(8,128)(2,1)S(1)}, u32[]{:S(2)}, u32[]{:S(2)}) %collective-permute-start.7) | collective-permute-done | bytes 262176 | tf_op jit(solution)/shard_map/ppermute | solution.py:382
  71.2 1.0 collective-permute-done.8.refs_1_
  72.2 1.0 shard_map.185
  73.2 0.0 copy-start
  73.2 2.6 %collective-permute-start.10 = (bf16[128,768]{1,0:T(8,128)(2,1)S(1)}, bf16[128,768]{1,0:T(8,128)(2,1)S(1)}, u32[]{:S(2)}, u32[]{:S(2)}) collective-permute-start(bf16[128,768]{1,0:T(8,128)(2,1)S(1)} %get-tuple-element.33), channel_id=1, source_target_pairs={{0,1},{1,0},{2,3},{3,2},{4,5},{5,4},{6,7},{7,6},{8,9},{9,8},{10,11... | collective-permute-start | bytes 589832 | tf_op jit(solution)/shard_map/ppermute | solution.py:386
  75.8 1.0 collective-permute-done.10.other_far_ref
  76.9 0.0 collective-permute-done.9.other_near_ref
  76.9 3.7 %shard_map.186 = (f32[1024,128]{1,0:T(8,128)S(1)}, bf16[1024,128]{1,0:T(8,128)(2,1)S(1)}, f32[1024,128]{1,0:T(8,128)S(1)}, f32[1024,128]{1,0:T(8,128)S(1)}, bf16...) custom-call(s32[3]{0:T(128)S(1)} %pad_add_fusion.place_ref, ...), custom_call_target="tpu_custom_call" | custom-call | tf_op jit(solution)/shard_map/pallas_call | solution.py:403
  80.6 15.0 %all_to_all.15.pieces_ref = bf16[8,144,128]{2,1,0:T(8,128)(2,1)S(1)} all-to-all(bf16[8,144,128]{2,1,0:T(8,128)(2,1)S(1)} %get-tuple-element.37), channel_id=1, replica_groups=mesh['sp_0'=8,'sp_1'=8,'x'=4,'core'=2] {'sp_1'}, dimensions={0} | all-to-all | bytes 589824 | tf_op jit(solution)/shard_map/all_to_all | solution.py:554
  95.6 0.1 shard_map.187
  95.7 19.8 %all_to_all.16.pieces_ref = bf16[8,144,128]{2,1,0:T(8,128)(2,1)S(1)} all-to-all(bf16[8,144,128]{2,1,0:T(8,128)(2,1)S(1)} %get-tuple-element.38), channel_id=1, replica_groups=mesh['sp_0'=8,'sp_1'=8,'x'=4,'core'=2] {'sp_0'}, dimensions={0} | all-to-all | bytes 589824 | tf_op jit(solution)/shard_map/all_to_all | solution.py:562
  115.5 0.0 copy-done
  115.5 0.5 shard_map.188
  116.0 16.6 %all_to_all.17.rows_ref = bf16[8,128,256]{2,1,0:T(8,128)(2,1)S(1)} all-to-all(bf16[8,128,256]{2,1,0:T(8,128)(2,1)S(1)} %bitcast.12), channel_id=1, replica_groups=mesh['sp_0'=8,'sp_1'=8,'x'=4,'core'=2] {'x','core'}, dimensions={0} | all-to-all | bytes 1048576 | tf_op jit(solution)/shard_map/all_to_all | solution.py:577
  132.6 0.0 all-gather.3.cloned.1.call-done
  132.6 5.4 %shard_map.190 = bf16[128,2048]{1,0:T(8,128)(2,1)} custom-call(bf16[8,128,256]{2,1,0:T(8,128)(2,1)S(1)} %all_to_all.17.rows_ref, bf16[8,256,2048]{2,1,0:T(8,128)(2,1)} %bitcast.14), custom_call_target="tpu_custom_call" | custom-call | tf_op jit(solution)/shard_map/pallas_call | solution.py:403
  (1 shorter events, 0.0 us)
Async XLA Ops:
  6.5 126.1 %all-gather.3.cloned.1.call-start = ((), (), s32[]{:S(2)}) async-start(), calls=%async_computation.3 | async-start | bytes 9437184 | tf_op jit(solution)/shard_map/all_gather | solution.py:470
  11.7 34.2 %collective-permute-start.6 = (bf16[2048,768]{1,0:T(8,128)(2,1)S(1)}, bf16[2048,768]{1,0:T(8,128)(2,1)S(1)}, u32[]{:S(2)}, u32[]{:S(2)}) collective-permute-start(bf16[2048,768]{1,0:T(8,128)(2,1)S(1)} %get-tuple-element.27.refs_7_.refs_2_), channel_id=1, source_target_pairs={{0,1},{1,0},{2,3},{3,2},{4,5},{5,4},{6,7},{7,6},{8,9},{9,8},{10,11... | collective-permute-start | bytes 9437192 | tf_op jit(solution)/shard_map/ppermute | solution.py:386
  21.7 20.2 %collective-permute-start = (bf16[128,2048]{1,0:T(8,128)(2,1)S(1)}, bf16[128,2048]{1,0:T(8,128)(2,1)S(1)}, u32[]{:S(2)}, u32[]{:S(2)}) collective-permute-start(bf16[128,2048]{1,0:T(8,128)(2,1)S(1)} %get-tuple-element.25.refs_0_), channel_id=1, source_target_pairs={{0,2},{2,4},{4,6},{6,0},{1,3},{3,5},{5,7},{7,1},{8,10},{10,12},{12... | collective-permute-start | bytes 1572872 | tf_op jit(solution)/shard_map/ppermute | solution.py:382
  23.6 22.2 %collective-permute-start.1 = (bf16[128,2048]{1,0:T(8,128)(2,1)S(1)}, bf16[128,2048]{1,0:T(8,128)(2,1)S(1)}, u32[]{:S(2)}, u32[]{:S(2)}) collective-permute-start(bf16[128,2048]{1,0:T(8,128)(2,1)S(1)} %get-tuple-element.25.refs_0_), channel_id=1, source_target_pairs={{0,6},{2,0},{4,2},{6,4},{1,7},{3,1},{5,3},{7,5},{8,14},{10,8},{12,... | collective-permute-start | bytes 1572872 | tf_op jit(solution)/shard_map/ppermute | solution.py:382
  28.2 1.3 collective-permute-start.2
  28.9 1.4 collective-permute-start.3
  29.6 1.4 collective-permute-start.4
  30.3 0.7 collective-permute-start.5
  48.6 28.3 %collective-permute-start.9 = (bf16[400,768]{1,0:T(8,128)(2,1)S(1)}, bf16[400,768]{1,0:T(8,128)(2,1)S(1)}, u32[]{:S(2)}, u32[]{:S(2)}) collective-permute-start(bf16[400,768]{1,0:T(8,128)(2,1)S(1)} %get-tuple-element.32), channel_id=1, source_target_pairs={{0,1},{1,0},{2,3},{3,2},{4,5},{5,4},{6,7},{7,6},{8,9},{9,8},{10,11... | collective-permute-start | bytes 1843208 | tf_op jit(solution)/shard_map/ppermute | solution.py:386
  53.2 18.0 %collective-permute-start.7 = (bf16[64,2048]{1,0:T(8,128)(2,1)S(1)}, bf16[64,2048]{1,0:T(8,128)(2,1)S(1)}, u32[]{:S(2)}, u32[]{:S(2)}) collective-permute-start(bf16[64,2048]{1,0:T(8,128)(2,1)S(1)} %get-tuple-element.29), channel_id=1, source_target_pairs={{0,2},{2,4},{4,6},{6,0},{1,3},{3,5},{5,7},{7,1},{8,10},{10,12},{12... | collective-permute-start | bytes 786440 | tf_op jit(solution)/shard_map/ppermute | solution.py:382
  55.1 17.1 %collective-permute-start.8 = (bf16[64,2048]{1,0:T(8,128)(2,1)S(1)}, bf16[64,2048]{1,0:T(8,128)(2,1)S(1)}, u32[]{:S(2)}, u32[]{:S(2)}) collective-permute-start(bf16[64,2048]{1,0:T(8,128)(2,1)S(1)} %get-tuple-element.30), channel_id=1, source_target_pairs={{0,6},{2,0},{4,2},{6,4},{1,7},{3,1},{5,3},{7,5},{8,14},{10,8},{12,... | collective-permute-start | bytes 786440 | tf_op jit(solution)/shard_map/ppermute | solution.py:382
  73.2 42.4 %copy-start = (f32[128]{0:T(128)S(1)}, f32[128]{0:T(128)}, u32[]{:S(2)}) copy-start(f32[128]{0:T(128)} %param.33) | copy-start | bytes 1540
  73.2 3.7 %collective-permute-start.10 = (bf16[128,768]{1,0:T(8,128)(2,1)S(1)}, bf16[128,768]{1,0:T(8,128)(2,1)S(1)}, u32[]{:S(2)}, u32[]{:S(2)}) collective-permute-start(bf16[128,768]{1,0:T(8,128)(2,1)S(1)} %get-tuple-element.33), channel_id=1, source_target_pairs={{0,1},{1,0},{2,3},{3,2},{4,5},{5,4},{6,7},{7,6},{8,9},{9,8},{10,11... | collective-permute-start | bytes 589832 | tf_op jit(solution)/shard_map/ppermute | solution.py:386
Sparse Core Ops, SparseCore 0:
  9.5 71.0 all-gather.2

commit v5 on v2

--- a/solution.py
+++ b/solution.py
@@ -122,7 +122,9 @@
 
 
 def project_kernel(*refs):
-    *row_refs, w_ref, other_ref, own_out, other_out, rows_ref = refs
+    *row_refs, w_ref, other_hbm, own_out, other_out, rows_ref, other_ref, arrived = refs
+    copy = pltpu.make_async_copy(other_hbm, other_ref, arrived)
+    copy.start()
     at = 0
     tails = [ref[...] for ref in row_refs if ref.shape[0] == HALO]
     for ref in row_refs:
@@ -136,6 +138,7 @@
         rows_ref[at:] = tail
     rows = rows_ref[...]
     own_out[...] = jnp.dot(rows, w_ref[...], preferred_element_type=F32).astype(BF16)
+    copy.wait()
     other_out[...] = jnp.dot(rows, other_ref[...], preferred_element_type=F32).astype(BF16)
 
 
@@ -495,6 +498,8 @@
     other_weights = swapped(weights)
     half = own_rows // 2
     far = kernel_call(halves_kernel, [held((half, width), BF16)] * 2, prior, following)
+    far, own_output = lax.optimization_barrier((far, own_output))
+    output_weights = lax.all_gather(own_output, TP, axis=0)
     far_first = around(far[0], 1)
     far_second = around(far[1], -1)
 
@@ -506,16 +511,18 @@
             [held((count, weights.shape[1]), BF16)] * 2,
             *pieces,
             weights,
-            other_weights,
-            scratch=[pltpu.VMEM((count, width), BF16)],
+            Stored(other_weights),
+            scratch=[
+                pltpu.VMEM((count, width), BF16),
+                pltpu.VMEM(weights.shape, BF16),
+                pltpu.SemaphoreType.DMA,
+            ],
             mebibytes=24,
         )
 
     own_near, send_near = project(normed, prior, following, *found)
     other_near = swapped(send_near)
     own_far, send_far = project(far_first, far_second)
-    own_far, own_output = lax.optimization_barrier((own_far, own_output))
-    output_weights = lax.all_gather(own_output, TP, axis=0)
     other_far = swapped(send_far)
 
     columns, inner = lax.axis_size("sp_0"), lax.axis_size("sp_1")

time: 146 us -> 152 us (1.041)
  Pallas kernels: 16.9 us -> 23.6 us
  local copies, waits for them, and re-layouts: 8.16 us -> 3.4 us
  waiting for transfers between devices: 16.1 us -> 18.6 us
    pallas_call x9, Pallas kernels: 16.9 us -> 23.6 us  [kernel_call(): pl.pallas_call(body, grid=(1,), in_specs=[spec(array) for array in arrays...]
    unnamed x24 -> x10, local copies, waits for them, and re-layouts: 8.16 us -> 3.4 us
    ppermute x4, starting transfers between devices: 13.7 us -> 16.1 us  [around(): lax.ppermute(array, 'x', [(i, (i + away) % ring) for i in range(ring)])]
    ppermute x3, waiting for transfers between devices: 1.41 us -> 3.53 us  [swapped(): return lax.ppermute(array, 'core', [(0, 1), (1, 0)])]
  transfers between devices with their start and end apart: 12 -> 12, of which waited for: 5 -> 6; matrix products, arithmetic and copies ran while one was open for 0% -> 0% of each run, Pallas kernels for 6% -> 10%
where the time goes in v5:
time: 152 us; the launch traced here: 151 us
  blocking collectives  59.3 us (39%)
  starting transfers between devices  32.3 us (21%)
  Pallas kernels  23.6 us (16%)
  waiting for transfers between devices  18.6 us (12%)
  between operations  13.6 us (9%)
  local copies, waits for them, and re-layouts  3.4 us (2%)
    pallas_call x9, Pallas kernels, kernel_call(): pl.pallas_call(body, grid=(1,), in_specs=[spec(array) for array in arrays...  23.6 us
    all_to_all x1, blocking collectives, shards(): pieces = lax.all_to_all(packed, 'sp_1', 0, 0, tiled=True)  21.2 us
    all_to_all x1, blocking collectives, shards(): pieces = lax.all_to_all(packed, 'sp_0', 0, 0, tiled=True)  21.1 us
    all_to_all x1, blocking collectives, shards(): lax.all_to_all(branches.reshape(members, own_rows, 2 * STATE), TP, 0, 0,...  17 us
    ppermute x4, starting transfers between devices, around(): lax.ppermute(array, 'x', [(i, (i + away) % ring) for i in range(ring)])  16.1 us
    ppermute x4, waiting for transfers between devices, around(): lax.ppermute(array, 'x', [(i, (i + away) % ring) for i in range(ring)])  15.1 us
    ppermute x3, starting transfers between devices, swapped(): return lax.ppermute(array, 'core', [(0, 1), (1, 0)])  13.4 us
    ppermute x3, waiting for transfers between devices, swapped(): return lax.ppermute(array, 'core', [(0, 1), (1, 0)])  3.53 us
  transfers between devices with their start and end apart: 12, of which 6 were waited for; matrix products, arithmetic and copies ran while one was open for 0% of the time, Pallas kernels for 10%

profile of v5, /device:TPU:1, one launch (start us, length us, event | category | flops | bytes accessed | tf_op | source)
XLA Modules:
  0.0 151.0 jit_solution(16891068343688759175)
XLA Ops:
  6.5 0.0 all-gather.3.cloned.1.call-start
  6.5 2.1 %shard_map.181 = (bf16[128,2048]{1,0:T(8,128)(2,1)}, bf16[16,2048]{1,0:T(8,128)(2,1)S(1)}) custom-call(bf16[128,2048]{1,0:T(8,128)(2,1)} %x_hbm.1, f32[1,2048]{1,0:T(1,128)} %bitcast.16), custom_call_target="tpu_custom_call" | custom-call | tf_op jit(solution)/shard_map/pallas_call | solution.py:404
  8.6 3.9 %collective-permute-start = (bf16[128,2048]{1,0:T(8,128)(2,1)}, bf16[128,2048]{1,0:T(8,128)(2,1)}, u32[]{:S(2)}, u32[]{:S(2)}) collective-permute-start(bf16[128,2048]{1,0:T(8,128)(2,1)} %get-tuple-element.29.refs_0_), channel_id=1, source_target_pairs={{0,2},{2,4},{4,6},{6,0},{1,3},{3,5},{5,7},{7,1},{8,10},{10,12},{12... | collective-permute-start | bytes 1572872 | tf_op jit(solution)/shard_map/ppermute | solution.py:383
  12.6 3.2 %collective-permute-start.1 = (bf16[128,2048]{1,0:T(8,128)(2,1)}, bf16[128,2048]{1,0:T(8,128)(2,1)}, u32[]{:S(2)}, u32[]{:S(2)}) collective-permute-start(bf16[128,2048]{1,0:T(8,128)(2,1)} %get-tuple-element.29.refs_0_), channel_id=1, source_target_pairs={{0,6},{2,0},{4,2},{6,4},{1,7},{3,1},{5,3},{7,5},{8,14},{10,8},{12,... | collective-permute-start | bytes 1572872 | tf_op jit(solution)/shard_map/ppermute | solution.py:383
  15.8 0.1 pad_add_fusion.place_ref
  15.9 3.1 %shard_map.182 = (bf16[2048,768]{1,0:T(8,128)(2,1)S(1)}, bf16[256,2048]{1,0:T(8,128)(2,1)S(1)}, f32[8,384]{1,0:T(8,128)S(1)}, f32[56,128]{1,0:T(8,128)S(1)}, bf16[128,128]{1,0:T(8,128)(2,1)S(1)}) custom-call(s32[3]{0:T(128)S(1)} %pad_add_fusion.place_ref, bf16[2048,128]{1,0:T(8,128)(2,1)} %value_hbm.1, bf16[2048,128]{1,0:T(8,128)(2,1)} %write_hbm.1, ...), custom_call_target="tpu_custom_call" | custom-call | tf_op jit(solution)/shard_map/pallas_call | solution.py:404
  18.9 0.0 copy-start
  18.9 1.0 copy-done
  19.9 0.8 collective-permute-done.refs_1_.prior_ref
  20.7 2.7 %collective-permute-done.1.refs_2_.next_ref = bf16[128,2048]{1,0:T(8,128)(2,1)} collective-permute-done((bf16[128,2048]{1,0:T(8,128)(2,1)}, bf16[128,2048]{1,0:T(8,128)(2,1)}, u32[]{:S(2)}, u32[]{:S(2)}) %collective-permute-start.1) | collective-permute-done | bytes 524320 | tf_op jit(solution)/shard_map/ppermute | solution.py:383
  23.4 1.2 shard_map.184
  24.7 0.0 copy-start.2
  24.7 0.7 copy-done.2
  25.4 0.0 all-gather.3.cloned.1.call-update
  25.4 8.0 %collective-permute-start.6 = (bf16[2048,768]{1,0:T(8,128)(2,1)S(1)}, bf16[2048,768]{1,0:T(8,128)(2,1)S(1)}, u32[]{:S(2)}, u32[]{:S(2)}) collective-permute-start(bf16[2048,768]{1,0:T(8,128)(2,1)S(1)} %get-tuple-element.31.refs_7_.refs_2_), channel_id=1, source_target_pairs={{0,1},{1,0},{2,3},{3,2},{4,5},{5,4},{6,7},{7,6},{8,9},{9,8},{10,11... | collective-permute-start | bytes 9437192 | tf_op jit(solution)/shard_map/ppermute | solution.py:387
  33.4 0.0 copy-start.3
  33.4 0.8 collective-permute-start.2
  34.2 0.7 collective-permute-start.3
  34.9 0.7 collective-permute-start.4
  35.6 0.7 collective-permute-start.5
  36.2 0.0 collective-permute-done.2.refs_3_
  36.3 0.0 collective-permute-done.3.refs_4_
  36.3 0.0 collective-permute-done.4.refs_5_
  36.3 0.0 collective-permute-done.5.refs_6_
  36.3 2.4 %collective-permute-done.6.refs_8_.refs_3_ = bf16[2048,768]{1,0:T(8,128)(2,1)S(1)} collective-permute-done((bf16[2048,768]{1,0:T(8,128)(2,1)S(1)}, bf16[2048,768]{1,0:T(8,128)(2,1)S(1)}, u32[]{:S(2)}, u32[]{:S(2)}) %collective-permute-start.6) | collective-permute-done | bytes 3145760 | tf_op jit(solution)/shard_map/ppermute | solution.py:387
  38.7 0.0 copy-start.4
  38.7 1.7 %copy-done.4 = bf16[2048,768]{1,0:T(8,128)(2,1)} copy-done((bf16[2048,768]{1,0:T(8,128)(2,1)}, bf16[2048,768]{1,0:T(8,128)(2,1)S(1)}, u32[]{:S(2)}) %copy-start.4) | copy-done | bytes 3145752
  40.4 5.1 %shard_map.183 = (bf16[400,768]{1,0:T(8,128)(2,1)S(1)}, bf16[400,768]{1,0:T(8,128)(2,1)S(1)}) custom-call(bf16[128,2048]{1,0:T(8,128)(2,1)} %get-tuple-element.29.refs_0_, bf16[128,2048]{1,0:T(8,128)(2,1)} %collective-permute-done.refs_1_.prior_ref, bf16[128,2048]{1,0:T(8,128)(2,1)} %collective-permute-done.1.refs_2_.next_ref, ...), custom_call_target="tpu_custom_call" | custom-call | tf_op jit(solution)/shard_map/pallas_call | solution.py:404
  45.5 2.3 %collective-permute-start.9 = (bf16[400,768]{1,0:T(8,128)(2,1)S(1)}, bf16[400,768]{1,0:T(8,128)(2,1)S(1)}, u32[]{:S(2)}, u32[]{:S(2)}) collective-permute-start(bf16[400,768]{1,0:T(8,128)(2,1)S(1)} %get-tuple-element.39), channel_id=1, source_target_pairs={{0,1},{1,0},{2,3},{3,2},{4,5},{5,4},{6,7},{7,6},{8,9},{9,8},{10,11... | collective-permute-start | bytes 1843208 | tf_op jit(solution)/shard_map/ppermute | solution.py:387
  47.8 0.0 copy-done.3
  47.8 2.7 %collective-permute-start.7 = (bf16[64,2048]{1,0:T(8,128)(2,1)S(1)}, bf16[64,2048]{1,0:T(8,128)(2,1)S(1)}, u32[]{:S(2)}, u32[]{:S(2)}) collective-permute-start(bf16[64,2048]{1,0:T(8,128)(2,1)S(1)} %copy-done.3), channel_id=1, source_target_pairs={{0,2},{2,4},{4,6},{6,0},{1,3},{3,5},{5,7},{7,1},{8,10},{10,12},{12... | collective-permute-start | bytes 786440 | tf_op jit(solution)/shard_map/ppermute | solution.py:383
  50.5 6.2 %collective-permute-start.8 = (bf16[64,2048]{1,0:T(8,128)(2,1)S(1)}, bf16[64,2048]{1,0:T(8,128)(2,1)S(1)}, u32[]{:S(2)}, u32[]{:S(2)}) collective-permute-start(bf16[64,2048]{1,0:T(8,128)(2,1)S(1)} %get-tuple-element.37), channel_id=1, source_target_pairs={{0,6},{2,0},{4,2},{6,4},{1,7},{3,1},{5,3},{7,5},{8,14},{10,8},{12,... | collective-permute-start | bytes 786440 | tf_op jit(solution)/shard_map/ppermute | solution.py:383
  56.8 10.3 %collective-permute-done.7.refs_0_ = bf16[64,2048]{1,0:T(8,128)(2,1)S(1)} collective-permute-done((bf16[64,2048]{1,0:T(8,128)(2,1)S(1)}, bf16[64,2048]{1,0:T(8,128)(2,1)S(1)}, u32[]{:S(2)}, u32[]{:S(2)}) %collective-permute-start.7) | collective-permute-done | bytes 262176 | tf_op jit(solution)/shard_map/ppermute | solution.py:383
  67.1 1.3 collective-permute-done.8.refs_1_
  68.3 3.3 %shard_map.185 = (bf16[128,768]{1,0:T(8,128)(2,1)S(1)}, bf16[128,768]{1,0:T(8,128)(2,1)S(1)}) custom-call(bf16[64,2048]{1,0:T(8,128)(2,1)S(1)} %collective-permute-done.7.refs_0_, bf16[64,2048]{1,0:T(8,128)(2,1)S(1)} %collective-permute-done.8.refs_1_, bf16[2048,768]{1,0:T(8,128)(2,1)S(1)} %get-tuple-element.31.refs_7_.refs_2_, bf16[2048,768]{1,0:T(8,128)(2,1)} %copy-done.4), custom_call_target="tpu_custom_call" | custom-call | tf_op jit(solution)/shard_map/pallas_call | solution.py:404
  71.7 0.0 copy-start.1
  71.7 3.1 %collective-permute-start.10 = (bf16[128,768]{1,0:T(8,128)(2,1)S(1)}, bf16[128,768]{1,0:T(8,128)(2,1)S(1)}, u32[]{:S(2)}, u32[]{:S(2)}) collective-permute-start(bf16[128,768]{1,0:T(8,128)(2,1)S(1)} %get-tuple-element.40), channel_id=1, source_target_pairs={{0,1},{1,0},{2,3},{3,2},{4,5},{5,4},{6,7},{7,6},{8,9},{9,8},{10,11... | collective-permute-start | bytes 589832 | tf_op jit(solution)/shard_map/ppermute | solution.py:387
  74.8 1.1 collective-permute-done.10.other_far_ref
  76.0 0.0 collective-permute-done.9.other_near_ref
  76.0 3.7 %shard_map.186 = (f32[1024,128]{1,0:T(8,128)S(1)}, bf16[1024,128]{1,0:T(8,128)(2,1)S(1)}, f32[1024,128]{1,0:T(8,128)S(1)}, f32[1024,128]{1,0:T(8,128)S(1)}, bf16...) custom-call(s32[3]{0:T(128)S(1)} %pad_add_fusion.place_ref, ...), custom_call_target="tpu_custom_call" | custom-call | tf_op jit(solution)/shard_map/pallas_call | solution.py:404
  79.7 21.2 %all_to_all.15.pieces_ref = bf16[8,144,128]{2,1,0:T(8,128)(2,1)S(1)} all-to-all(bf16[8,144,128]{2,1,0:T(8,128)(2,1)S(1)} %get-tuple-element.44), channel_id=1, replica_groups=mesh['sp_0'=8,'sp_1'=8,'x'=4,'core'=2] {'sp_1'}, dimensions={0} | all-to-all | bytes 589824 | tf_op jit(solution)/shard_map/all_to_all | solution.py:556
  100.8 0.1 shard_map.187
  100.9 21.1 %all_to_all.16.pieces_ref = bf16[8,144,128]{2,1,0:T(8,128)(2,1)S(1)} all-to-all(bf16[8,144,128]{2,1,0:T(8,128)(2,1)S(1)} %get-tuple-element.45), channel_id=1, replica_groups=mesh['sp_0'=8,'sp_1'=8,'x'=4,'core'=2] {'sp_0'}, dimensions={0} | all-to-all | bytes 589824 | tf_op jit(solution)/shard_map/all_to_all | solution.py:564
  122.0 0.0 copy-done.1
  122.0 0.5 shard_map.188
  122.5 17.0 %all_to_all.17.rows_ref = bf16[8,128,256]{2,1,0:T(8,128)(2,1)S(1)} all-to-all(bf16[8,128,256]{2,1,0:T(8,128)(2,1)S(1)} %bitcast.12), channel_id=1, replica_groups=mesh['sp_0'=8,'sp_1'=8,'x'=4,'core'=2] {'x','core'}, dimensions={0} | all-to-all | bytes 1048576 | tf_op jit(solution)/shard_map/all_to_all | solution.py:579
  139.5 0.0 all-gather.3.cloned.1.call-done
  139.5 4.6 %shard_map.189 = bf16[128,2048]{1,0:T(8,128)(2,1)} custom-call(bf16[8,128,256]{2,1,0:T(8,128)(2,1)S(1)} %all_to_all.17.rows_ref, bf16[8,256,2048]{2,1,0:T(8,128)(2,1)} %bitcast.14), custom_call_target="tpu_custom_call" | custom-call | tf_op jit(solution)/shard_map/pallas_call | solution.py:404
Async XLA Ops:
  6.5 133.0 %all-gather.3.cloned.1.call-start = ((), (), s32[]{:S(2)}) async-start(), calls=%async_computation.3 | async-start | bytes 9437184 | tf_op jit(solution)/shard_map/all_gather | solution.py:502
  8.6 12.1 %collective-permute-start = (bf16[128,2048]{1,0:T(8,128)(2,1)}, bf16[128,2048]{1,0:T(8,128)(2,1)}, u32[]{:S(2)}, u32[]{:S(2)}) collective-permute-start(bf16[128,2048]{1,0:T(8,128)(2,1)} %get-tuple-element.29.refs_0_), channel_id=1, source_target_pairs={{0,2},{2,4},{4,6},{6,0},{1,3},{3,5},{5,7},{7,1},{8,10},{10,12},{12... | collective-permute-start | bytes 1572872 | tf_op jit(solution)/shard_map/ppermute | solution.py:383
  12.6 10.9 %collective-permute-start.1 = (bf16[128,2048]{1,0:T(8,128)(2,1)}, bf16[128,2048]{1,0:T(8,128)(2,1)}, u32[]{:S(2)}, u32[]{:S(2)}) collective-permute-start(bf16[128,2048]{1,0:T(8,128)(2,1)} %get-tuple-element.29.refs_0_), channel_id=1, source_target_pairs={{0,6},{2,0},{4,2},{6,4},{1,7},{3,1},{5,3},{7,5},{8,14},{10,8},{12,... | collective-permute-start | bytes 1572872 | tf_op jit(solution)/shard_map/ppermute | solution.py:383
  18.9 1.0 copy-start
  24.7 0.7 copy-start.2
  25.4 13.3 %collective-permute-start.6 = (bf16[2048,768]{1,0:T(8,128)(2,1)S(1)}, bf16[2048,768]{1,0:T(8,128)(2,1)S(1)}, u32[]{:S(2)}, u32[]{:S(2)}) collective-permute-start(bf16[2048,768]{1,0:T(8,128)(2,1)S(1)} %get-tuple-element.31.refs_7_.refs_2_), channel_id=1, source_target_pairs={{0,1},{1,0},{2,3},{3,2},{4,5},{5,4},{6,7},{7,6},{8,9},{9,8},{10,11... | collective-permute-start | bytes 9437192 | tf_op jit(solution)/shard_map/ppermute | solution.py:387
  33.4 14.4 %copy-start.3 = (bf16[64,2048]{1,0:T(8,128)(2,1)S(1)}, bf16[64,2048]{1,0:T(8,128)(2,1)}, u32[]{:S(2)}) copy-start(bf16[64,2048]{1,0:T(8,128)(2,1)} %copy-done.2) | copy-start | bytes 786436
  33.4 2.8 %collective-permute-start.2 = (bf16[16,2048]{1,0:T(8,128)(2,1)S(1)}, bf16[16,2048]{1,0:T(8,128)(2,1)S(1)}, u32[]{:S(2)}, u32[]{:S(2)}) collective-permute-start(bf16[16,2048]{1,0:T(8,128)(2,1)S(1)} %get-tuple-element.30), channel_id=1, source_target_pairs={{7,8},{15,16},{23,24},{31,32},{39,40},{47,48},{55,56},{63,64},{71,... | collective-permute-start | bytes 196616 | tf_op jit(solution)/shard_map/ppermute | solution.py:372
  34.2 2.0 %collective-permute-start.3 = (bf16[16,2048]{1,0:T(8,128)(2,1)S(1)}, bf16[16,2048]{1,0:T(8,128)(2,1)S(1)}, u32[]{:S(2)}, u32[]{:S(2)}) collective-permute-start(bf16[16,2048]{1,0:T(8,128)(2,1)S(1)} %get-tuple-element.30), channel_id=1, source_target_pairs={{7,10},{15,18},{23,26},{31,34},{39,42},{47,50},{55,58},{63,66},{71... | collective-permute-start | bytes 196616 | tf_op jit(solution)/shard_map/ppermute | solution.py:372
  34.9 1.4 collective-permute-start.4
  35.6 0.7 collective-permute-start.5
  38.7 1.7 %copy-start.4 = (bf16[2048,768]{1,0:T(8,128)(2,1)}, bf16[2048,768]{1,0:T(8,128)(2,1)S(1)}, u32[]{:S(2)}) copy-start(bf16[2048,768]{1,0:T(8,128)(2,1)S(1)} %collective-permute-done.6.refs_8_.refs_3_) | copy-start | bytes 9437188
  45.5 30.5 %collective-permute-start.9 = (bf16[400,768]{1,0:T(8,128)(2,1)S(1)}, bf16[400,768]{1,0:T(8,128)(2,1)S(1)}, u32[]{:S(2)}, u32[]{:S(2)}) collective-permute-start(bf16[400,768]{1,0:T(8,128)(2,1)S(1)} %get-tuple-element.39), channel_id=1, source_target_pairs={{0,1},{1,0},{2,3},{3,2},{4,5},{5,4},{6,7},{7,6},{8,9},{9,8},{10,11... | collective-permute-start | bytes 1843208 | tf_op jit(solution)/shard_map/ppermute | solution.py:387
  47.8 19.3 %collective-permute-start.7 = (bf16[64,2048]{1,0:T(8,128)(2,1)S(1)}, bf16[64,2048]{1,0:T(8,128)(2,1)S(1)}, u32[]{:S(2)}, u32[]{:S(2)}) collective-permute-start(bf16[64,2048]{1,0:T(8,128)(2,1)S(1)} %copy-done.3), channel_id=1, source_target_pairs={{0,2},{2,4},{4,6},{6,0},{1,3},{3,5},{5,7},{7,1},{8,10},{10,12},{12... | collective-permute-start | bytes 786440 | tf_op jit(solution)/shard_map/ppermute | solution.py:383
  50.5 17.8 %collective-permute-start.8 = (bf16[64,2048]{1,0:T(8,128)(2,1)S(1)}, bf16[64,2048]{1,0:T(8,128)(2,1)S(1)}, u32[]{:S(2)}, u32[]{:S(2)}) collective-permute-start(bf16[64,2048]{1,0:T(8,128)(2,1)S(1)} %get-tuple-element.37), channel_id=1, source_target_pairs={{0,6},{2,0},{4,2},{6,4},{1,7},{3,1},{5,3},{7,5},{8,14},{10,8},{12,... | collective-permute-start | bytes 786440 | tf_op jit(solution)/shard_map/ppermute | solution.py:383
  71.7 50.3 %copy-start.1 = (f32[128]{0:T(128)S(1)}, f32[128]{0:T(128)}, u32[]{:S(2)}) copy-start(f32[128]{0:T(128)} %param.33) | copy-start | bytes 1540
  71.7 4.3 %collective-permute-start.10 = (bf16[128,768]{1,0:T(8,128)(2,1)S(1)}, bf16[128,768]{1,0:T(8,128)(2,1)S(1)}, u32[]{:S(2)}, u32[]{:S(2)}) collective-permute-start(bf16[128,768]{1,0:T(8,128)(2,1)S(1)} %get-tuple-element.40), channel_id=1, source_target_pairs={{0,1},{1,0},{2,3},{3,2},{4,5},{5,4},{6,7},{7,6},{8,9},{9,8},{10,11... | collective-permute-start | bytes 589832 | tf_op jit(solution)/shard_map/ppermute | solution.py:387
Sparse Core Ops, SparseCore 0:
  25.5 70.5 all-gather.2
